TPU v7x, 256 devices: a 4x2x16 block of a 4x16x16 slice. The times are simulated.
256 devices in a mesh: grp: 2 (over y), sp: 16 (over z), tp: 4 (over x), dp: 2 (over core).
Axes of the slice: x: 4, y: 2, z: 16, core: 2. Of those that a mesh axis runs over, the one named last changes fastest.
The devices are a block of a 4x16x16 slice.
Arguments:
- latent: bfloat16 [24576, 4096], P(('grp', 'sp', 'dp')), parts along dimension 0, may hold values from -6 to 6
- context: bfloat16 [1024, 4096], P(('grp', 'sp')), parts along dimension 0, may hold values from -6 to 6
- condition: bfloat16 [8192], P('grp'), parts along dimension 0, may hold values from -6 to 6
- context_condition: bfloat16 [4096], replicated, may hold values from -6 to 6
- shift_weight: bfloat16 [4096, 4096], P('sp', ('tp', 'dp')), may hold values from -0.09375 to 0.09375
- scale_weight: bfloat16 [4096, 4096], P('sp', ('tp', 'dp')), may hold values from -0.09375 to 0.09375
- gate_weight: bfloat16 [4096, 4096], P('sp', ('tp', 'dp')), may hold values from -0.09375 to 0.09375
- norm_gain: float32 [4096], replicated, may hold values from 0.1 to 1.9
- out_gate_weight: bfloat16 [4096, 2048], P(None, ('tp', 'dp')), may hold values from -0.09375 to 0.09375
- signal_weight: bfloat16 [4096, 2048], P(None, ('tp', 'dp')), may hold values from -0.09375 to 0.09375
- writer_weight: bfloat16 [4096, 1024], P(None, ('tp', 'dp')), may hold values from -0.09375 to 0.09375
- reader_matrix: bfloat16 [4096, 1024], P(None, ('tp', 'dp')), may hold values from -0.09375 to 0.09375
- step_weight: bfloat16 [2, 4096, 32], P(None, None, ('tp', 'dp')), may hold values from -0.09375 to 0.09375
- signal_taps: float32 [3, 2048], P(None, ('tp', 'dp')), may hold values from -3.5 to 3.5
- writer_taps: float32 [3, 1024], P(None, ('tp', 'dp')), may hold values from -3.5 to 3.5
- reader_taps: float32 [3, 1024], P(None, ('tp', 'dp')), may hold values from -3.5 to 3.5
- step_bias: float32 [2, 32], P(None, ('tp', 'dp')), may hold values from -4.5 to -2.5
- decay_log: float32 [2, 32], P(None, ('tp', 'dp')), may hold values from -12 to 1
- decay_extra: float32 [2, 32, 24576], P(None, ('tp', 'dp'), ('grp', 'sp')), parts along dimension 2, may hold values from -3 to 0
- group_gain: float32 [2048], P(('tp', 'dp')), may hold values from 0.1 to 1.9
- output_weight: bfloat16 [2048, 4096], P(None, ('tp', 'dp')), may hold values from -0.125 to 0.125
Outputs:
- updated: bfloat16 [24576, 4096], P(('grp', 'sp'), ('tp', 'dp')), parts along dimension 0
There are 2 independent parts, one for each index of `grp`. A program takes and returns all parts, laid end to end along the dimension named above; an argument that names none is the same for every part. Nothing has to cross between parts.
All inputs are finite; a program needn't handle non-finite values.
Results may differ from a plain program's by a relative error of at most 0.007.
Values may be sent and summed in bfloat16 or wider, within the bound.
No kernel may reach another device: no remote copies, remote signals or barrier semaphores. Data moves between devices by JAX's collectives and lax.ppermute only.
A program may use at most 128 MiB of HBM per device.

v0:
```python
import jax
import jax.numpy as jnp
from jax import lax
from jax.sharding import PartitionSpec as P

STATE = 128
BLOCK = 128


EPSILON = 1e-06


def copy_for_each(x, axis):
    copies = jnp.broadcast_to(x, (lax.axis_size(axis), *x.shape))
    return lax.all_to_all(copies, axis, split_axis=0, concat_axis=0, tiled=True)


def of_everyone(x, axis):
    everything = copy_for_each(x, axis)
    return jnp.sum(everything, axis=0)


def in_one(arrays, axis):
    ends = [0]
    for a in arrays:
        ends.append(ends[-1] + a.size)
    subtotal = of_everyone(jnp.concatenate([a.ravel() for a in arrays]), axis)
    return tuple((subtotal[b:e].reshape(a.shape) for a, b, e in zip(arrays, ends, ends[1:])))


def side_by_side(arrays, axis, dim, along):
    ends, at = ([], 0)
    for a in arrays[:-1]:
        at += a.shape[along]
        ends.append(at)
    both = jnp.concatenate(arrays, axis=along)
    return tuple(jnp.split(lax.all_gather(both, axis, axis=dim, tiled=True), ends, axis=along))


def rows_first(arrays, axis, dims):
    turned = [jnp.moveaxis(a, dim, 0) for a, dim in zip(arrays, dims)]
    widths = [t[0].size for t in turned]
    both = jnp.concatenate([t.reshape(-1, w) for t, w in zip(turned, widths)], axis=1)
    out = lax.all_gather(both, axis, axis=0, tiled=True)
    tiles = jnp.split(out, [sum(widths[:k]) for k in range(1, len(widths))], axis=1)
    return tuple(
        (
            jnp.moveaxis(b.reshape(-1, *t.shape[1:]), 0, dim)
            for b, t, dim in zip(tiles, turned, dims)
        )
    )


def extended(cells, sides, width):
    for axis, dim in sides:
        count = lax.axis_size(axis)
        ends = count - 1
        head = lax.slice_in_dim(cells, 0, width, axis=dim)
        tail = lax.slice_in_dim(cells, cells.shape[dim] - width, cells.shape[dim], axis=dim)
        cells = jnp.concatenate(
            [
                lax.ppermute(tail, axis, [(i, (i + 1) % count) for i in range(ends)]),
                cells,
                lax.ppermute(head, axis, [((i + 1) % count, i) for i in range(ends)]),
            ],
            axis=dim,
        )
    return cells


def entering(x, axis, combine, identity, reverse):
    devices, position = (lax.axis_size(axis), lax.axis_index(axis))
    everything = jax.tree.map(lambda part: lax.all_gather(part, axis), x)
    start = jax.tree.map(
        lambda part, zero: jnp.broadcast_to(jnp.asarray(zero, part.dtype), part.shape), x, identity
    )

    def turn(k, before):
        at = devices - 1 - k if reverse else k
        reached = at > position if reverse else at < position
        new = combine(before, jax.tree.map(lambda part: part[at], everything))
        return jax.tree.map(lambda a, b: jnp.where(reached, a, b), new, before)

    return lax.fori_loop(0, devices, turn, start)


def modulate(rows, norm_gain, shift_vec, scale_vec):
    values = rows.astype(jnp.float32)
    normed = (
        values * lax.rsqrt(jnp.mean(values * values, axis=-1, keepdims=True) + EPSILON) * norm_gain
    )
    return (normed * (1.0 + scale_vec) + shift_vec).astype(jnp.bfloat16)


def centred_conv(padded, conv_taps, length):
    running = jnp.zeros((length, padded.shape[1]), jnp.float32)
    for offset in range(conv_taps.shape[0]):
        running = running + conv_taps[offset] * padded[offset : offset + length].astype(jnp.float32)
    return jax.nn.silu(running)


def project_rows(hidden, signal_weight, writer_weight, reader_matrix, step_weight):
    raw_cols = jnp.concatenate(
        [
            jnp.dot(hidden, signal_weight, preferred_element_type=jnp.float32),
            jnp.dot(hidden, writer_weight, preferred_element_type=jnp.float32),
            jnp.dot(hidden, reader_matrix, preferred_element_type=jnp.float32),
        ],
        axis=1,
    ).astype(jnp.bfloat16)
    step_in = jnp.stack(
        [
            jnp.dot(hidden, step_weight[0], preferred_element_type=jnp.float32),
            jnp.dot(hidden, step_weight[1], preferred_element_type=jnp.float32),
        ]
    ).astype(jnp.bfloat16)
    return (raw_cols, step_in)


def split_mixed(conv_out, head_count, head_width, group_count, state_width):
    length = conv_out.shape[0]
    signal_end = head_count * head_width
    writer_end = signal_end + group_count * state_width
    signal = conv_out[:, :signal_end].reshape(length, head_count, head_width)
    writer = conv_out[:, signal_end:writer_end].reshape(length, group_count, state_width)
    reader = conv_out[:, writer_end:].reshape(length, group_count, state_width)
    return (signal, writer, reader)


def state_span(signal, step_size, log_decay, writer, reader, start_state, block):
    length, head_count, head_width = signal.shape
    group_count, state_width = (writer.shape[1], writer.shape[2])
    per_group = head_count // group_count
    blocks = length // block
    scaled = (signal * step_size[..., None]).reshape(
        blocks, block, group_count, per_group, head_width
    )
    cum_log = jnp.cumsum(log_decay.reshape(blocks, block, group_count, per_group), axis=1)
    writer_blk = writer.reshape(blocks, block, group_count, state_width)
    reader_blk = reader.reshape(blocks, block, group_count, state_width)
    inner_dot = jnp.einsum("bign,bjgn->bgij", reader_blk, writer_blk)
    moved = jnp.moveaxis(cum_log, 1, -1)
    gap_logs = moved[..., :, None] - moved[..., None, :]
    lower_mask = jnp.tril(jnp.ones((block, block), dtype=bool))
    weights = jnp.exp(jnp.where(lower_mask, gap_logs, -jnp.inf))
    in_block = jnp.einsum("bgij,bgeij,bjgep->bigep", inner_dot, weights, scaled)
    to_end = jnp.exp(cum_log[:, -1:] - cum_log)
    states = jnp.einsum("bjgn,bjge,bjgep->bgepn", writer_blk, to_end, scaled)
    block_decay = jnp.exp(cum_log[:, -1])

    def advance(running, block_item):
        state_add, decay_now = block_item
        return (running * decay_now[..., None, None] + state_add, running)

    last_state, before = lax.scan(
        advance,
        start_state.reshape(group_count, per_group, head_width, state_width),
        (states, block_decay),
    )
    carried = jnp.einsum("bign,bgepn,bige->bigep", reader_blk, before, jnp.exp(cum_log))
    result = (in_block + carried).reshape(length, head_count, head_width)
    return (result, last_state.reshape(head_count, head_width, state_width))


def context_state(signal, row_weights, writer):
    length, head_count, head_width = signal.shape
    group_count, state_width = (writer.shape[1], writer.shape[2])
    per_group = head_count // group_count
    grouped = signal.reshape(length, group_count, per_group, head_width)
    weights = row_weights.reshape(length, group_count, per_group)
    summed = jnp.einsum("tgn,tge,tgep->gepn", writer, weights, grouped)
    return summed.reshape(head_count, head_width, state_width)


def group_norm(gated, group_count, group_gain):
    length = gated.shape[0]
    grouped = gated.reshape(length, group_count, -1)
    normed = grouped * lax.rsqrt(jnp.mean(grouped * grouped, axis=-1, keepdims=True) + EPSILON)
    return (normed.reshape(length, -1) * group_gain).astype(jnp.bfloat16)


def chain_step(preceding_entries, later):
    return (
        preceding_entries[0] + later[0],
        jnp.exp(later[0])[:, None, None] * preceding_entries[1] + later[1],
    )


def on_device(
    latent,
    context,
    condition,
    context_condition,
    shift_weight,
    scale_weight,
    gate_weight,
    norm_gain,
    out_gate_weight,
    signal_weight,
    writer_weight,
    reader_matrix,
    step_weight,
    signal_taps,
    writer_taps,
    reader_taps,
    step_bias,
    decay_log,
    decay_extra,
    group_gain,
    output_weight,
):
    rows_here = shift_weight.shape[0]
    cond_act = jax.nn.silu(jnp.stack([condition, context_condition]).astype(jnp.float32)).astype(
        jnp.bfloat16
    )
    own_rows = lax.dynamic_slice_in_dim(cond_act, lax.axis_index("sp") * rows_here, rows_here, 1)
    shift_part = jnp.dot(own_rows, shift_weight, preferred_element_type=jnp.float32)
    scale_part = jnp.dot(own_rows, scale_weight, preferred_element_type=jnp.float32)
    gate_part = jnp.dot(own_rows[:1], gate_weight, preferred_element_type=jnp.float32)
    shift_sum, scale_sum, gate_sum = in_one((shift_part, scale_part, gate_part), "sp")
    shift_vec, scale_vec = side_by_side((shift_sum, scale_sum), ("tp", "dp"), 1, 0)
    gate_vec = gate_sum[0]
    full_rows = lax.all_gather(latent, "dp", axis=0, tiled=True)
    length = full_rows.shape[0]
    hidden = modulate(full_rows, norm_gain, shift_vec[0], scale_vec[0])
    ctx_hidden = modulate(context, norm_gain, shift_vec[1], scale_vec[1])
    conv_taps = jnp.concatenate([signal_taps, writer_taps, reader_taps], axis=1)
    decay_rates = -jnp.exp(decay_log)[:, None, :]
    head_count = step_bias.shape[1]
    head_width = signal_weight.shape[1] // head_count
    group_count = writer_weight.shape[1] // STATE
    per_group = head_count // group_count
    ctx_raw, ctx_step_in = project_rows(
        ctx_hidden, signal_weight, writer_weight, reader_matrix, step_weight
    )
    every_raw, every_step = rows_first((ctx_raw, ctx_step_in), "sp", (0, 1))
    ctx_len = every_raw.shape[0]
    ctx_conv = centred_conv(jnp.pad(every_raw, ((1, 1), (0, 0))), conv_taps, ctx_len)
    ctx_signal, ctx_writer, _ = split_mixed(ctx_conv, head_count, head_width, group_count, STATE)
    prefix_stride_length = jax.nn.softplus(every_step.astype(jnp.float32) + step_bias[:, None, :])
    ctx_decay = decay_rates * prefix_stride_length
    cum_log = jnp.cumsum(ctx_decay, axis=1)
    ctx_forward = context_state(
        ctx_signal, jnp.exp(cum_log[0, -1:] - cum_log[0]) * prefix_stride_length[0], ctx_writer
    )
    ctx_backward = context_state(
        ctx_signal, jnp.exp(cum_log[1] - ctx_decay[1]) * prefix_stride_length[1], ctx_writer
    )
    gate_in = jnp.dot(hidden, out_gate_weight, preferred_element_type=jnp.float32).astype(
        jnp.bfloat16
    )
    raw_cols, step_in = project_rows(
        hidden, signal_weight, writer_weight, reader_matrix, step_weight
    )
    padded = extended(raw_cols, (("sp", 0),), 1)
    signal, writer, reader = split_mixed(
        centred_conv(padded, conv_taps, length), head_count, head_width, group_count, STATE
    )
    step_size = jax.nn.softplus(step_in.astype(jnp.float32) + step_bias[:, None, :])
    log_decay = decay_rates * step_size + jnp.swapaxes(decay_extra, 1, 2)
    zero_state = jnp.zeros((head_count, head_width, STATE), jnp.float32)
    forward_out, forward_last = state_span(
        signal, step_size[0], log_decay[0], writer, reader, zero_state, BLOCK
    )
    back_signal = jnp.flip(signal, 0)
    back_reader = jnp.flip(reader, 0)
    back_decay = jnp.flip(log_decay[1], 0)
    backward_out, backward_last = state_span(
        back_signal,
        jnp.flip(step_size[1], 0),
        back_decay,
        jnp.flip(writer, 0),
        back_reader,
        zero_state,
        BLOCK,
    )
    cum_forward = jnp.cumsum(log_decay[0], axis=0)
    cumulative_backward = jnp.cumsum(back_decay, axis=0)
    identity = (jnp.zeros((head_count,), jnp.float32), zero_state)
    onward_inflow = entering((cum_forward[-1], forward_last), "sp", chain_step, identity, False)
    enter_bwd = entering((cumulative_backward[-1], backward_last), "sp", chain_step, identity, True)
    start_fwd = jnp.exp(onward_inflow[0])[:, None, None] * ctx_forward + onward_inflow[1]
    start_bwd = jnp.exp(enter_bwd[0])[:, None, None] * ctx_backward + enter_bwd[1]
    reader_head_rows = jnp.repeat(reader, per_group, axis=1)
    back_heads = jnp.repeat(back_reader, per_group, axis=1)
    forward_out = (
        forward_out
        + jnp.einsum("thn,hpn->thp", reader_head_rows, start_fwd) * jnp.exp(cum_forward)[..., None]
    )
    backward_out = (
        backward_out
        + jnp.einsum("thn,hpn->thp", back_heads, start_bwd)
        * jnp.exp(cumulative_backward)[..., None]
    )
    both = (forward_out + jnp.flip(backward_out, 0)).reshape(length, -1)
    gated = both * jax.nn.silu(gate_in.astype(jnp.float32))
    normed = group_norm(gated, group_count, group_gain)
    mix = jnp.dot(
        lax.all_gather(normed, ("tp", "dp"), axis=1, tiled=True),
        output_weight,
        preferred_element_type=jnp.float32,
    )
    out_start = lax.axis_index(("tp", "dp")) * output_weight.shape[1]
    residual = lax.dynamic_slice_in_dim(full_rows, out_start, output_weight.shape[1], 1).astype(
        jnp.float32
    )
    return (residual + gate_vec * mix).astype(jnp.bfloat16)


def solution(mesh):
    in_specs = (
        P(("grp", "sp", "dp"), None),
        P(("grp", "sp"), None),
        P("grp"),
        P(),
        P("sp", ("tp", "dp")),
        P("sp", ("tp", "dp")),
        P("sp", ("tp", "dp")),
        P(),
        P(None, ("tp", "dp")),
        P(None, ("tp", "dp")),
        P(None, ("tp", "dp")),
        P(None, ("tp", "dp")),
        P(None, None, ("tp", "dp")),
        P(None, ("tp", "dp")),
        P(None, ("tp", "dp")),
        P(None, ("tp", "dp")),
        P(None, ("tp", "dp")),
        P(None, ("tp", "dp")),
        P(None, ("tp", "dp"), ("grp", "sp")),
        P(("tp", "dp")),
        P(None, ("tp", "dp")),
    )
    out_specs = P(("grp", "sp"), ("tp", "dp"))
    return jax.shard_map(
        on_device, mesh=mesh, in_specs=in_specs, out_specs=out_specs, check_vma=False
    )
```

profile of v0, /device:TPU:33, one launch (start us, length us, event | category | flops | bytes accessed | tf_op | source)
XLA Modules:
  0.0 478.3 jit_solution(13487710746028656442)
XLA Ops:
  8.9 24.5 %all-to-all-start = ((f32[16,1,2560]{2,1,0:T(1,128)}), f32[16,1,2560]{2,1,0:T(1,128)S(1)}, u32[]{:S(2)}, u32[]{:S(2)}) async-start(f32[16,1,2560]{2,1,0:T(1,128)} %broadcast_in_dim.34), calls=%async_computation | async-start | bytes 327680 | tf_op jit(solution)/shard_map/all_to_all | solution.py:15
  34.5 10.9 %all-to-all-done = f32[16,1,2560]{2,1,0:T(1,128)S(1)} async-done(((f32[16,1,2560]{2,1,0:T(1,128)}), f32[16,1,2560]{2,1,0:T(1,128)S(1)}, u32[]{:S(2)}, u32[]{:S(2)}) %all-to-all-start) | async-done | bytes 163872 | tf_op jit(solution)/shard_map/all_to_all | solution.py:15
  45.6 17.6 %all_gather.25 = f32[4,4096]{1,0:T(4,128)S(1)} all-gather(f32[4,512]{1,0:T(4,128)S(1)} %pad_maximum_fusion.9), channel_id=1, replica_groups=mesh['grp'=2,'sp'=16,'tp'=4,'dp'=2] {'tp','dp'}, dimensions={1}, use_global_device_ids=true | all-gather | bytes 73728 | tf_op jit(solution)/shard_map/all_gather | solution.py:37
  63.9 1.7 convolution_convert_fusion.5
  65.6 1.5 convolution_convert_fusion.6
  67.6 25.9 %all_gather.28 = bf16[512,520]{1,0:T(8,128)(2,1)S(1)} all-gather(bf16[32,520]{1,0:T(8,128)(2,1)S(1)} %pad_maximum_fusion.7), channel_id=1, replica_groups=mesh['grp'=2,'sp'=16,'tp'=4,'dp'=2] {'sp'}, dimensions={0}, use_global_device_ids=true | all-gather | bytes 565760 | tf_op jit(solution)/shard_map/all_gather | solution.py:44
  96.4 2.4 reduce-window.24
  101.1 4.2 fusion.4
  105.7 3.1 fusion.8
  108.9 2.2 convolution_convert_fusion.2
  111.1 2.2 convolution_convert_fusion.3
  113.4 2.0 convolution_convert_fusion.1
  115.4 1.7 fusion.38
  117.1 2.0 fusion.37
  119.9 1.3 collective-permute-start.1
  121.2 4.7 collective-permute-start
  128.5 3.3 rev.19
  133.3 1.1 reduce-window.26
  136.2 1.7 copy.341
  137.9 1.3 fusion.111
  140.5 1.3 reshape.370
  141.8 2.2 reduce-window.20
  144.8 1.4 reduce-window.21
  148.3 1.7 fusion.107
  150.0 1.7 fusion.106
  151.7 1.8 copy.329
  153.5 1.7 copy.326
  155.2 1.2 copy.309
  156.4 1.3 mul.352
  158.5 1.3 copy.311
  159.8 1.7 copy.306
  161.5 20.6 %all-gather.1 = f32[16,1,4]{2,1,0:T(1,128)} all-gather(f32[1,1,4]{2,1,0:T(1,128)} %bitcast.351), channel_id=1, replica_groups=mesh['grp'=2,'sp'=16,'tp'=4,'dp'=2] {'sp'}, dimensions={0}, use_global_device_ids=true | all-gather | bytes 272 | tf_op jit(solution)/shard_map/all_gather | solution.py:73
  182.1 21.8 %all-gather = f32[16,1,4]{2,1,0:T(1,128)} all-gather(f32[1,1,4]{2,1,0:T(1,128)} %bitcast.352), channel_id=1, replica_groups=mesh['grp'=2,'sp'=16,'tp'=4,'dp'=2] {'sp'}, dimensions={0}, use_global_device_ids=true | all-gather | bytes 272 | tf_op jit(solution)/shard_map/all_gather | solution.py:73
  204.0 4.9 %divide_multiply_fusion = f32[768,512]{0,1:T(8,128)S(1)} fusion(bf16[1,512]{0,1:T(8,128)(2,1)S(1)} %collective-permute-done.1, bf16[768,128]{0,1:T(8,128)(2,1)S(1)} %copy-done.15, bf16[768,128]{0,1:T(8,128)(2,1)S(1)} %copy-done.17, bf16[768,256]{0,1:T(8,128)(2,1)} %copy-done.23, bf16[1,512]{0,1:T(8,128)(2,1)} %collective-permute-done, f32[512]{0:T(512)} %bitcast.339, ...), kind=kLoop, calls=%fused_computation.35 | loop fusion | flops 12189696 | bytes 2367488 | tf_op jit(solution)/shard_map/jit(silu)/mul | solution.py:99
  209.8 3.8 reverse.6
  213.5 1.8 copy.303
  215.3 3.8 reverse.7
  219.0 1.7 copy.304
  220.8 1.8 copy.323
  222.5 1.7 copy.324
  224.2 1.1 reshape.367
  225.3 2.4 rev.18
  227.8 1.2 broadcast_multiply_fusion.3
  229.0 1.1 reshape.381
  230.1 1.4 broadcast_multiply_fusion
  232.5 8.2 %while.62 = (s32[]{:T(128)}, f32[1,4,64,128]{3,2,1,0:T(8,128)S(1)}, bf16[6,1,4,64,128]{4,3,2,1,0:T(8,128)(2,1)}, f32[6,1,4]{2,1,0:T(1,128)}, f32[6,1,4,64,128]{4,3,2,1,0:T(8,128)S(1)}, /*index=5*/s32[]{:T(128)}, s32[]{:T(128)}) while((s32[]{:T(128)}, f32[1,4,64,128]{3,2,1,0:T(8,128)S(1)}, ...), condition=%wide.region_14.15_spmd.clone, body=%wide.region_13.14_spmd.clone.sunk | while | flops 131075 | bytes 589980 | solution.py:155
  241.5 1.3 fusion.114
  242.8 2.0 fusion.113
  248.0 1.1 convolution_bitcast_fusion.1
  249.6 1.1 reshape.383
  250.7 2.8 fusion.19
  253.6 10.1 %while.60 = (s32[]{:T(128)}, f32[1,4,64,128]{3,2,1,0:T(8,128)S(1)}, bf16[6,1,4,64,128]{4,3,2,1,0:T(8,128)(2,1)S(1)}, f32[6,1,4]{2,1,0:T(1,128)}, f32[6,1,4,64,128]{4,3,2,1,0:T(8,128)}, /*index=5*/s32[]{:T(128)}, s32[]{:T(128)}) while((s32[]{:T(128)}, f32[1,4,64,128]{3,2,1,0:T(8,128)S(1)}, ...), condition=%wide.region_4.5_spmd.clone, body=%wide.region_3.4_spmd.clone.sunk | while | flops 131075 | bytes 589980 | solution.py:155
  263.7 1.4 fusion.32
  265.7 1.1 reshape.369
  266.9 52.0 %all-gather.11.cloned.1.call-done = f32[16,4,64,128]{3,2,1,0:T(8,128)} async-done(((f32[1,4,64,128]{3,2,1,0:T(8,128)}), f32[16,4,64,128]{3,2,1,0:T(8,128)}) %all-gather.11.cloned.1.call-update) | async-done | bytes 2097168 | tf_op jit(solution)/shard_map/all_gather | solution.py:73
  318.9 27.4 %while.63 = (s32[]{:T(128)}, f32[4]{0:T(128)S(1)}, f32[4,64,128]{2,1,0:T(8,128)S(1)}, s32[]{:T(128)}, f32[16,4]{1,0:T(8,128)}, /*index=5*/f32[16,4,64,128]{3,2,1...) while((s32[]{:T(128)}, f32[4]{0:T(128)S(1)}, f32[4,64,128]{2,1,0:T(8,128)S(1)}, ...), condition=%wide.region_18.19_spmd.clone, body=%wide.region_17.18_spmd.clone.sunk | while | flops 131092 | bytes 393481 | solution.py:84
  346.4 2.7 fusion.29
  349.1 4.5 rev.20
  353.6 35.5 %all-gather.9.cloned.1.call-done = f32[16,4,64,128]{3,2,1,0:T(8,128)} async-done(((f32[1,4,64,128]{3,2,1,0:T(8,128)}), f32[16,4,64,128]{3,2,1,0:T(8,128)}) %all-gather.9.cloned.1.call-update) | async-done | bytes 2097168 | tf_op jit(solution)/shard_map/all_gather | solution.py:73
  389.1 27.4 %while.61 = (s32[]{:T(128)}, f32[4]{0:T(128)S(1)}, f32[4,64,128]{2,1,0:T(8,128)S(1)}, s32[]{:T(128)}, f32[16,4]{1,0:T(8,128)}, /*index=5*/f32[16,4,64,128]{3,2,1,0:T(8,128)}, s32[]{:T(128)}, s32[]{:T(128)}) while((s32[]{:T(128)}, f32[4]{0:T(128)S(1)}, f32[4,64,128]{2,1,0:T(8,128)S(1)}, s32[]{:T(128)}, f32[16,4]{1,0:T(8,128)}, ...), condition=%wide.region_8.9_spmd.clone, body=%wide.region_7.8_spmd.clone.sunk | while | flops 131088 | bytes 393419 | solution.py:84
  416.5 2.9 fusion.27
  419.4 5.5 %multiply_reduce_fusion = (f32[768]{0:T(1024)S(1)}, f32[768,256]{0,1:T(8,128)S(1)}) fusion(bf16[768,4096]{1,0:T(8,128)(2,1)} %copy-done.1, bf16[4096,256]{1,0:T(8,128)(2,1)} %param.37, f32[768,4,64]{0,2,1:T(8,128)} %fusion.27), kind=kOutput, calls=%fused_computation.95 | convolution fusion | flops 1612381440 | bytes 9964544 | tf_op jit(solution)/shard_map/dot_general | solution.py:249
  425.9 41.1 %all-gather.13.cloned.1.call-done = bf16[768,2048]{0,1:T(8,128)(2,1)} async-done(((bf16[768,256]{0,1:T(8,128)(2,1)}), bf16[768,2048]{0,1:T(8,128)(2,1)}) %all-gather.13.cloned.1.call-update) | async-done | bytes 3145744 | tf_op jit(solution)/shard_map/all_gather | solution.py:299
  467.0 4.8 add_convert_fusion
  (324 shorter events, 101.4 us)
Async XLA Ops:
  6.5 460.5 %copy-start = (bf16[2048,512]{1,0:T(8,128)(2,1)S(1)}, bf16[2048,512]{1,0:T(8,128)(2,1)}, u32[]{:S(2)}) copy-start(bf16[2048,512]{1,0:T(8,128)(2,1)} %param.49) | copy-start | bytes 6291460
  6.6 0.9 copy-start.49
  6.6 0.9 copy-start.50
  6.6 1.1 copy-start.25
  6.6 1.3 copy-start.26
  6.6 1.4 copy-start.27
  6.6 27.5 %copy-start.51 = (f32[3,256]{1,0:T(4,128)S(1)}, f32[3,256]{1,0:T(4,128)}, u32[]{:S(2)}) copy-start(f32[3,256]{1,0:T(4,128)} %param.42) | copy-start | bytes 9220
  6.6 27.5 %copy-start.52 = (f32[3,128]{1,0:T(4,128)S(1)}, f32[3,128]{1,0:T(4,128)}, u32[]{:S(2)}) copy-start(f32[3,128]{1,0:T(4,128)} %param.43) | copy-start | bytes 4612
  6.6 27.5 %copy-start.54 = (f32[2,4]{1,0:T(2,128)S(1)}, f32[2,4]{1,0:T(2,128)}, u32[]{:S(2)}) copy-start(f32[2,4]{1,0:T(2,128)} %param.46) | copy-start | bytes 100
  6.6 27.6 %copy-start.53 = (f32[3,128]{1,0:T(4,128)S(1)}, f32[3,128]{1,0:T(4,128)}, u32[]{:S(2)}) copy-start(f32[3,128]{1,0:T(4,128)} %param.44) | copy-start | bytes 4612
  6.6 27.6 %copy-start.24 = (bf16[32,4096]{1,0:T(8,128)(2,1)S(1)}, bf16[32,4096]{1,0:T(8,128)(2,1)}, u32[]{:S(2)}) copy-start(bf16[32,4096]{1,0:T(8,128)(2,1)} %param.30) | copy-start | bytes 786436
  6.6 94.5 %all-gather.7.cloned.1.call-start = ((), (), s32[]{:S(2)}) async-start(), calls=%async_computation.1 | async-start | bytes 9437184 | tf_op jit(solution)/shard_map/all_gather | solution.py:223
  7.4 55.8 %copy-start.31 = (f32[4096]{0:T(1024)S(1)}, f32[4096]{0:T(1024)}, u32[]{:S(2)}) copy-start(f32[4096]{0:T(1024)} %param.36) | copy-start | bytes 49156
  7.4 56.0 %copy-start.28 = (bf16[2,4096,4]{1,2,0:T(4,128)(2,1)S(1)}, bf16[2,4096,4]{1,2,0:T(4,128)(2,1)}, u32[]{:S(2)}) copy-start(bf16[2,4096,4]{1,2,0:T(4,128)(2,1)} %param.41) | copy-start | bytes 196612
  8.9 36.5 %all-to-all-start = ((f32[16,1,2560]{2,1,0:T(1,128)}), f32[16,1,2560]{2,1,0:T(1,128)S(1)}, u32[]{:S(2)}, u32[]{:S(2)}) async-start(f32[16,1,2560]{2,1,0:T(1,128)} %broadcast_in_dim.34), calls=%async_computation | async-start | bytes 327680 | tf_op jit(solution)/shard_map/all_to_all | solution.py:15
  33.4 285.4 %all-gather.11.cloned.1.call-start = ((), (), s32[]{:S(2)}) async-start(), calls=%async_computation.3 | async-start | bytes 2228224 | tf_op jit(solution)/shard_map/all_gather | solution.py:73
  34.4 59.1 %copy-start.41 = (f32[1,512]{1,0:T(1,128)}, f32[1,512]{1,0:T(1,128)S(1)}, u32[]{:S(2)}) copy-start(f32[1,512]{1,0:T(1,128)S(1)} %get-tuple-element.663) | copy-start | bytes 6148
  34.5 59.1 %copy-start.42 = (f32[1,512]{1,0:T(1,128)}, f32[1,512]{1,0:T(1,128)S(1)}, u32[]{:S(2)}) copy-start(f32[1,512]{1,0:T(1,128)S(1)} %get-tuple-element.664) | copy-start | bytes 6148
  34.5 59.1 %copy-start.43 = (f32[1,512]{1,0:T(1,128)}, f32[1,512]{1,0:T(1,128)S(1)}, u32[]{:S(2)}) copy-start(f32[1,512]{1,0:T(1,128)S(1)} %get-tuple-element.665) | copy-start | bytes 6148
  45.5 17.7 %copy-start.37 = (f32[2560]{0:T(1024)}, f32[2560]{0:T(1024)S(1)}, u32[]{:S(2)}) copy-start(f32[2560]{0:T(1024)S(1)} %reduce_sum.36) | copy-start | bytes 30724
  63.9 3.2 copy-start.18
  93.6 2.7 copy-start.48
  94.1 1.0 copy-start.8
  101.1 4.6 copy-start.2
  105.7 3.1 copy-start.6
  108.8 8.3 %copy-start.1 = (bf16[768,4096]{1,0:T(8,128)(2,1)}, bf16[768,4096]{1,0:T(8,128)(2,1)S(1)}, u32[]{:S(2)}) copy-start(bf16[768,4096]{1,0:T(8,128)(2,1)S(1)} %fusion.8) | copy-start | bytes 18874372
  108.8 2.2 copy-start.7
  111.1 8.0 %copy-start.14 = (bf16[768,128]{0,1:T(8,128)(2,1)}, bf16[768,128]{0,1:T(8,128)(2,1)S(1)}, u32[]{:S(2)}) copy-start(bf16[768,128]{0,1:T(8,128)(2,1)S(1)} %convolution_convert_fusion.2) | copy-start | bytes 589828
  111.1 2.3 copy-start.19
  113.4 5.7 %copy-start.16 = (bf16[768,128]{0,1:T(8,128)(2,1)}, bf16[768,128]{0,1:T(8,128)(2,1)S(1)}, u32[]{:S(2)}) copy-start(bf16[768,128]{0,1:T(8,128)(2,1)S(1)} %convolution_convert_fusion.3) | copy-start | bytes 589828
  115.4 3.7 copy-start.23
  119.1 6.8 %copy-start.40 = (f32[2,4,768]{2,1,0:T(4,128)S(1)}, f32[2,4,768]{2,1,0:T(4,128)}, u32[]{:S(2)}) copy-start(f32[2,4,768]{2,1,0:T(4,128)} %param.47) | copy-start | bytes 73732
  119.9 84.0 %collective-permute-start.1 = (bf16[1,512]{0,1:T(8,128)(2,1)}, bf16[1,512]{0,1:T(8,128)(2,1)S(1)}, u32[]{:S(2)}, u32[]{:S(2)}) collective-permute-start(bf16[1,512]{0,1:T(8,128)(2,1)} %get-tuple-element.645), channel_id=1, source_target_pairs={{8,0},{16,8},{24,16},{32,24},{40,32},{48,40},{56,48},{64,56},{72,6... | collective-permute-start | bytes 3080 | tf_op jit(solution)/shard_map/ppermute | solution.py:64
  121.2 82.7 %collective-permute-start = (bf16[1,512]{0,1:T(8,128)(2,1)}, bf16[1,512]{0,1:T(8,128)(2,1)}, u32[]{:S(2)}, u32[]{:S(2)}) collective-permute-start(bf16[1,512]{0,1:T(8,128)(2,1)} %get-tuple-element.644), channel_id=1, source_target_pairs={{0,8},{8,16},{16,24},{24,32},{32,40},{40,48},{48,56},{56,64},{64,7... | collective-permute-start | bytes 3080 | tf_op jit(solution)/shard_map/ppermute | solution.py:62
  150.0 53.9 %copy-start.15 = (bf16[768,128]{0,1:T(8,128)(2,1)S(1)}, bf16[768,128]{0,1:T(8,128)(2,1)}, u32[]{:S(2)}) copy-start(bf16[768,128]{0,1:T(8,128)(2,1)} %copy-done.14) | copy-start | bytes 589828
  150.0 53.9 %copy-start.17 = (bf16[768,128]{0,1:T(8,128)(2,1)S(1)}, bf16[768,128]{0,1:T(8,128)(2,1)}, u32[]{:S(2)}) copy-start(bf16[768,128]{0,1:T(8,128)(2,1)} %copy-done.16) | copy-start | bytes 589828
  224.2 3.5 copy-start.34
  227.8 2.3 copy-start.29
  230.1 1.4 copy-start.21
  240.7 0.7 copy-start.4
  240.7 4.1 copy-start.10
  240.8 4.1 copy-start.44
  240.8 4.1 copy-start.47
  241.5 147.6 %all-gather.9.cloned.1.call-start = ((), (), s32[]{:S(2)}) async-start(), calls=%async_computation.2 | async-start | bytes 2228224 | tf_op jit(solution)/shard_map/all_gather | solution.py:73
  244.9 1.2 copy-start.9
  244.9 1.2 copy-start.30
  246.1 1.0 copy-start.13
  246.1 1.1 copy-start.22
  246.1 1.1 copy-start.33
  247.1 1.0 copy-start.20
  253.6 10.1 %copy-start.11 = (bf16[768,128]{1,0:T(8,128)(2,1)S(1)}, bf16[768,128]{1,0:T(8,128)(2,1)}, u32[]{:S(2)}) copy-start(bf16[768,128]{1,0:T(8,128)(2,1)} %copy.303) | copy-start | bytes 589828
  253.6 10.1 %copy-start.32 = (f32[6,128,4]{1,2,0:T(4,128)S(1)}, f32[6,128,4]{1,2,0:T(4,128)}, u32[]{:S(2)}) copy-start(f32[6,128,4]{1,2,0:T(4,128)} %copy.306) | copy-start | bytes 36868
  263.7 2.0 copy-start.3
  265.2 53.7 %copy-start.46 = (f32[4]{0:T(128)S(1)}, f32[4]{0:T(128)}, u32[]{:S(2)}) copy-start(f32[4]{0:T(128)} %custom-call.4) | copy-start | bytes 52
  266.8 79.6 %copy-start.5 = (f32[512,256]{0,1:T(8,128)S(1)}, f32[512,256]{0,1:T(8,128)}, u32[]{:S(2)}) copy-start(f32[512,256]{0,1:T(8,128)} %copy.318) | copy-start | bytes 1572868
  266.8 79.6 %copy-start.36 = (f32[768,4]{0,1:T(4,128)S(1)}, f32[768,4]{0,1:T(4,128)}, u32[]{:S(2)}) copy-start(f32[768,4]{0,1:T(4,128)} %get-tuple-element.636) | copy-start | bytes 36868
  266.8 79.6 %copy-start.39 = (f32[512,4]{0,1:T(4,128)S(1)}, f32[512,4]{0,1:T(4,128)}, u32[]{:S(2)}) copy-start(f32[512,4]{0,1:T(4,128)} %fusion.94) | copy-start | bytes 24580
  266.8 200.2 %all-gather.13.cloned.1.call-start = ((), (), s32[]{:S(2)}) async-start(), calls=%async_computation.4 | async-start | bytes 3538944 | tf_op jit(solution)/shard_map/all_gather | solution.py:299
  346.4 42.7 %copy-start.45 = (f32[4]{0:T(128)S(1)}, f32[4]{0:T(128)}, u32[]{:S(2)}) copy-start(f32[4]{0:T(128)} %custom-call.1) | copy-start | bytes 52
  349.1 67.4 %copy-start.12 = (bf16[768,128]{1,0:T(8,128)(2,1)S(1)}, bf16[768,128]{1,0:T(8,128)(2,1)}, u32[]{:S(2)}) copy-start(bf16[768,128]{1,0:T(8,128)(2,1)} %copy.303) | copy-start | bytes 589828
  349.1 67.4 %copy-start.35 = (f32[768,4]{0,1:T(4,128)S(1)}, f32[768,4]{0,1:T(4,128)}, u32[]{:S(2)}) copy-start(f32[768,4]{0,1:T(4,128)} %get-tuple-element.632) | copy-start | bytes 36868
  349.1 67.4 %copy-start.38 = (f32[512,4]{0,1:T(4,128)S(1)}, f32[512,4]{0,1:T(4,128)}, u32[]{:S(2)}) copy-start(f32[512,4]{0,1:T(4,128)} %fusion.95) | copy-start | bytes 24580
  419.4 5.6 %copy-start.55 = (f32[256]{0:T(256)S(1)}, f32[256]{0:T(256)}, u32[]{:S(2)}) copy-start(f32[256]{0:T(256)} %param.48) | copy-start | bytes 3076
  424.9 42.1 %slice-start = ((f32[2560]{0:T(1024)}), f32[512]{0:T(512)S(1)}, s32[]{:S(2)}) async-start(f32[2560]{0:T(1024)} %copy-done.37), calls=%async_computation.5 | async-start | bytes 4096 | tf_op jit(solution)/shard_map/slice | solution.py:28
Sparse Core Ops, SparseCore 0:
  9.3 41.3 all-gather.6
  241.6 77.2 all-gather.10
  320.7 68.3 all-gather.8
  426.0 40.9 all-gather.12
where the time goes:
time: 482 us; the launch traced here: 478 us
  waiting for transfers between devices  140 us (29%)
  other arithmetic  98.2 us (20%)
  blocking collectives  85.9 us (18%)
  local copies, waits for them, and re-layouts  67.5 us (14%)
  matrix products  40.4 us (8%)
  starting transfers between devices  30.8 us (6%)
  between operations  14.2 us (3%)
    all_gather x2, waiting for transfers between devices, entering(): everything = jax.tree.map(lambda part: lax.all_gather(part, axis), x)  87.5 us
    all_gather x2, blocking collectives, entering(): everything = jax.tree.map(lambda part: lax.all_gather(part, axis), x)  42.4 us
    all_gather x1, waiting for transfers between devices, on_device(): lax.all_gather(normed, ('tp', 'dp'), axis=1, tiled=True)  41.1 us
    select_n x32, other arithmetic, turn(): return jax.tree.map(lambda a, b: jnp.where(reached, a, b), new, before)  31.6 us
    all_gather x1, blocking collectives, rows_first(): out = lax.all_gather(both, axis, axis=0, tiled=True)  25.9 us
    all_to_all x1, starting transfers between devices, copy_for_each(): return lax.all_to_all(copies, axis, split_axis=0, concat_axis=0, tiled=True)  24.5 us
    exp x32, other arithmetic, chain_step(): jnp.exp(later[0])[:, None, None] * preceding_entries[1] + later[1]  22.3 us
    all_gather x1, blocking collectives, side_by_side(): lax.all_gather(both, axis, axis=dim, tiled=True)  17.6 us
  transfers between devices with their start and end apart: 7, of which 4 were waited for; matrix products, arithmetic and copies ran while one was open for 22% of the time, Pallas kernels for 0%

commit v1 on v0

v1 whole, which is shorter than its diff:
```python
import functools
import jax
import jax.numpy as jnp
from jax import lax
from jax.experimental import pallas as pl
from jax.experimental.pallas import tpu as pltpu
from jax.sharding import PartitionSpec as P

STATE = 128
EPSILON = 1e-06
F32 = jnp.float32
BF16 = jnp.bfloat16
LANES = 128
I_TILE = 128
KINDS = 4
PIECES = 2
EDGES = 16
MIB = 2**20


def shifted(x, axis, by):
    n = lax.axis_size(axis)
    return lax.ppermute(x, axis, [(i, (i + by) % n) for i in range(n)])


def rounded(x):
    return x.astype(BF16).astype(F32)


def silu(x):
    return x / (1.0 + jnp.exp(-x))


def per_head(cols, base, heads, width):
    lane = lax.broadcasted_iota(jnp.int32, (cols.shape[0], LANES), 1)
    per_tile = LANES // width
    tiles = []
    for t in range(heads // per_tile):
        tile = jnp.broadcast_to(cols[:, base + t * per_tile : base + t * per_tile + 1], lane.shape)
        for e in range(1, per_tile):
            at = base + t * per_tile + e
            tile = jnp.where(lane >= e * width, cols[:, at : at + 1], tile)
        tiles.append(tile)
    return jnp.concatenate(tiles, axis=1)


def running_sums(values):
    n = values.shape[1]
    lane = lax.broadcasted_iota(jnp.int32, values.shape, 1)
    ahead, behind, k = values, values, 1
    while k < n:
        ahead = ahead + jnp.where(lane >= k, pltpu.roll(ahead, k, 1), 0.0)
        behind = behind + jnp.where(lane < n - k, pltpu.roll(behind, n - k, 1), 0.0)
        k *= 2
    return ahead, behind


def condense_body(cond, shift, scale, gate, out):
    n = out.shape[0]
    parts = jnp.concatenate(
        [
            jnp.dot(cond[...], shift[...], preferred_element_type=F32),
            jnp.dot(cond[...], scale[...], preferred_element_type=F32),
            jnp.dot(cond[...], gate[...], preferred_element_type=F32),
        ],
        axis=0,
    )
    for i in range(n):
        out[i] = parts[: out.shape[1], :]


def fold_body(got, out, gate):
    total = got[0]
    for i in range(1, got.shape[0]):
        total = total + got[i]
    for i in range(out.shape[0]):
        out[i] = total[: out.shape[1], :]
    gate[...] = total[out.shape[1] :, :]


def project_body(
    flags, own, oth, ctx, same, crossed, gain, vectors, w_gate, w_sig, w_wri, w_rea, w_step,
    taps, bias, dlog, extra,
    gate_out, sig_out, wri_out, rea_out, rows_out, cols_out, payload,
    acc, hidden, squares, pad, cpad, stpad,
    *, heads,
):
    k = pl.program_id(0)
    half = own.shape[0]
    length = 2 * half
    ctx_len = ctx.shape[0]
    n_sig = w_sig.shape[1]
    n_gate = w_gate.shape[1]
    n_state = w_wri.shape[1]
    width = n_sig // heads
    conv_w = n_sig + 2 * n_state
    dp = flags[0]

    @pl.when(k == 0)
    def _():
        acc[...] = jnp.zeros_like(acc)
        squares[...] = jnp.zeros_like(squares)

    w = jnp.concatenate([w_gate[...], w_sig[...], w_wri[...], w_rea[...], w_step[...]], axis=1)
    g0, b0 = gain[...] * (1.0 + vectors[0, 2:3, :]), vectors[0, 0:1, :]
    g1, b1 = gain[...] * (1.0 + vectors[0, 3:4, :]), vectors[0, 1:2, :]

    def take(values, scale, at):
        n = values.shape[0]
        hidden[at : at + n, :] = (values * scale).astype(BF16)
        part = values[:, :LANES] * values[:, :LANES]
        for t in range(1, values.shape[1] // LANES):
            tile = values[:, t * LANES : (t + 1) * LANES]
            part = part + tile * tile
        squares[at : at + n, :] += part

    first = dp == 0
    edges_before = jnp.where(first, crossed[...].astype(F32), same[...].astype(F32))
    edges_after = jnp.where(first, same[...].astype(F32), crossed[...].astype(F32))
    row = lax.broadcasted_iota(jnp.int32, (EDGES, own.shape[1]), 0)
    tile = jnp.zeros(row.shape, F32)
    for r, value in enumerate(
        (edges_before[1:2], edges_after[1:2], edges_before[0:1], edges_after[0:1])
    ):
        tile = jnp.where(row == r, value, tile)
    take(tile, jnp.where(row < 2, g1, g0), length + ctx_len)
    tile = jnp.zeros(row.shape, F32)
    for r, value in enumerate((b0, b0 - rounded(b0), b1, b1 - rounded(b1))):
        tile = jnp.where(row == r, value, tile)
    at = length + ctx_len + EDGES
    hidden[at : at + EDGES, :] = tile.astype(BF16)
    take(ctx[...].astype(F32), g1, length)
    take(own[...].astype(F32), g0, 0)
    take(oth[...].astype(F32), g0, half)
    acc[...] += jnp.dot(hidden[...], w, preferred_element_type=F32)

    @pl.when(k == pl.num_programs(0) - 1)
    def _():
        c0, c1 = n_gate, n_gate + conv_w
        d_model = own.shape[1] * pl.num_programs(0)
        prev_ok = jnp.where(flags[1] > 0, 0.0, 1.0)
        next_ok = jnp.where(flags[2] > 0, 0.0, 1.0)
        base = length + ctx_len + EDGES
        lat_add = acc[base : base + 1, :] + acc[base + 1 : base + 2, :]
        ctx_add = acc[base + 2 : base + 3, :] + acc[base + 3 : base + 4, :]
        scale = lax.rsqrt(
            jnp.sum(squares[...], axis=1, keepdims=True) * (1.0 / d_model) + EPSILON
        )

        def values(lo, n, cols, add):
            return rounded(acc[lo : lo + n, cols] * scale[lo : lo + n, :] + add[:, cols])

        conv_cols, step_cols = slice(c0, c1), slice(c1, c1 + 2 * heads)
        for lo, off in ((0, dp * half), (half, (1 - dp) * half)):
            off = pl.multiple_of(off, half)
            gate_out[pl.ds(off, half), :] = values(lo, half, slice(0, c0), lat_add).astype(BF16)
            pad[pl.ds(off + 8, half), :] = values(lo, half, conv_cols, lat_add)
            stpad[pl.ds(off, half), : 2 * heads] = values(lo, half, step_cols, lat_add)
        base = length + ctx_len
        pad[7:8, :] = values(base + 2, 1, conv_cols, lat_add) * prev_ok
        pad[8 + length : 9 + length, :] = values(base + 3, 1, conv_cols, lat_add) * next_ok
        cpad[8 : 8 + ctx_len, :] = values(length, ctx_len, conv_cols, ctx_add)
        cpad[7:8, :] = values(base, 1, conv_cols, ctx_add) * prev_ok
        cpad[8 + ctx_len : 9 + ctx_len, :] = values(base + 1, 1, conv_cols, ctx_add) * next_ok
        stpad[length : length + ctx_len, : 2 * heads] = values(length, ctx_len, step_cols, ctx_add)
        t0, t1, t2 = taps[0:1, :], taps[1:2, :], taps[2:3, :]
        conv = silu(
            t0 * pad[7 : 7 + length, :] + t1 * pad[8 : 8 + length, :] + t2 * pad[9 : 9 + length, :]
        )
        cconv = silu(
            t0 * cpad[7 : 7 + ctx_len, :]
            + t1 * cpad[8 : 8 + ctx_len, :]
            + t2 * cpad[9 : 9 + ctx_len, :]
        )
        sig, wri, rea = (
            conv[:, :n_sig],
            conv[:, n_sig : n_sig + n_state].astype(BF16),
            conv[:, n_sig + n_state :].astype(BF16),
        )
        sig_out[...] = sig.astype(BF16)
        wri_out[...] = wri
        rea_out[...] = rea
        csig, cwri = cconv[:, :n_sig], cconv[:, n_sig : n_sig + n_state].astype(BF16)

        both = 2 * heads
        turned = stpad[...].T[:both, :]
        lane = lax.broadcasted_iota(jnp.int32, turned.shape, 1)
        z = jnp.where(lane < length + ctx_len, turned, 0.0) + bias[...]
        step = jnp.maximum(z, 0.0) + jnp.log1p(jnp.exp(-jnp.abs(z)))
        more = jnp.concatenate([extra[...], jnp.zeros((both, LANES), F32)], axis=1)
        logs = -jnp.exp(dlog[...]) * step + more
        logs = jnp.where(lane < length + ctx_len, logs, 0.0)
        lat_step, lat_log = step[:, :length], logs[:, :length]
        ctx_step, ctx_log = step[:, length:], logs[:, length:]
        forward = lax.broadcasted_iota(jnp.int32, (both, 1), 0) < heads
        ahead, behind = running_sums(lat_log)
        cum = jnp.where(forward, ahead, behind)
        total = ahead[:, length - 1 :]
        lat_w = jnp.exp(total - cum) * lat_step
        c_ahead, _ = running_sums(ctx_log)
        c_total = c_ahead[:, LANES - 1 :]
        ctx_w = jnp.exp(jnp.where(forward, c_total - c_ahead, c_ahead - ctx_log)) * ctx_step
        rows_out[:both, :] = cum
        rows_out[both:, :] = lat_step
        cols = jnp.concatenate([cum, lat_w, jnp.zeros((LANES - 2 * both, length), F32)], axis=0).T
        ctx_cols = jnp.concatenate([ctx_w, jnp.zeros((LANES - both, LANES), F32)], axis=0).T
        cols_out[...] = cols
        contract = (((0,), (0,)), ((), ()))
        for direction in range(2):
            lhs = (sig * per_head(cols, both + direction * heads, heads, width)).astype(BF16)
            state = lax.dot_general(lhs, wri, contract, preferred_element_type=F32)
            part = n_sig // payload.shape[0]
            kind = direction * part
            payload[:, kind : kind + part, :] = state.reshape(-1, part, n_state).astype(BF16)
            lhs = csig * per_head(ctx_cols[:ctx_len, :], direction * heads, heads, width)
            state = lax.dot_general(lhs.astype(BF16), cwri, contract, preferred_element_type=F32)
            kind = (2 + direction) * part
            payload[:, kind : kind + part, :] = state.reshape(-1, part, n_state).astype(BF16)
        tail = payload.shape[1] - KINDS * part
        row = lax.broadcasted_iota(jnp.int32, (tail, LANES), 0)
        pieces = []
        for value in (total, c_total):
            high = rounded(value)
            pieces.append((high, value - high))
        per_slice = payload.shape[0] // heads
        for h in range(heads):
            tile = jnp.zeros((tail, LANES), F32)
            for kind in range(KINDS):
                at = (kind % 2) * heads + h
                for piece in range(PIECES):
                    value = pieces[kind // 2][piece][at : at + 1, :]
                    tile = jnp.where(row == kind * PIECES + piece, value, tile)
            for e in range(per_slice):
                payload[h * per_slice + e, KINDS * part :, :] = tile.astype(BF16)


def chain_body(got, out, *, part):
    spans = got.shape[0]

    def decay(i, kind):
        at = KINDS * part + kind * PIECES
        value = got[i, at : at + 1, :].astype(F32)
        for piece in range(1, PIECES):
            value = value + got[i, at + piece : at + piece + 1, :].astype(F32)
        return jnp.exp(value)

    def added(i, kind):
        return got[i, kind * part : (kind + 1) * part, :].astype(F32)

    for direction, order in ((0, range(spans)), (1, range(spans - 1, -1, -1))):
        state = jnp.zeros((part, got.shape[2]), F32)
        for i in order:
            state = decay(i, 2 + direction) * state + added(i, 2 + direction)
        for i in order:
            out[i, direction * part : (direction + 1) * part, :] = state.astype(BF16)
            state = decay(i, direction) * state + added(i, direction)


def inside_body(rea, wri, sig, rows, cols, out, *, heads):
    length = wri.shape[0]
    width = sig.shape[1] // heads
    block = rea.shape[0]
    start = pl.program_id(0) * block
    score = lax.dot_general(
        rea[...], wri[...], (((1,), (1,)), ((), ())), preferred_element_type=F32
    )
    i = start + lax.broadcasted_iota(jnp.int32, (block, length), 0)
    j = lax.broadcasted_iota(jnp.int32, (block, length), 1)
    below = i >= j
    above = i <= j
    for h in range(heads):
        b = heads + h
        gap = jnp.where(
            below, cols[:, h : h + 1] - rows[h : h + 1, :], cols[:, b : b + 1] - rows[b : b + 1, :]
        )
        size = jnp.where(below, rows[2 * heads + h : 2 * heads + h + 1, :], 0.0) + jnp.where(
            above, rows[2 * heads + b : 2 * heads + b + 1, :], 0.0
        )
        weights = (jnp.exp(gap) * size * score).astype(BF16)
        out[:, h * width : (h + 1) * width] = jnp.dot(
            weights, sig[:, h * width : (h + 1) * width], preferred_element_type=F32
        )


def finish_body(starts, rea, cols, inside, gate, gain, out, *, heads):
    spans, rows, state = starts.shape
    part = rows // 2
    n_sig = inside.shape[1]
    width = n_sig // heads
    contract = (((1,), (1,)), ((), ()))
    mixed = inside[...]
    decays = jnp.exp(cols[...])
    for direction in range(2):
        begin = starts[:, direction * part : (direction + 1) * part, :].reshape(n_sig, state)
        carried = lax.dot_general(rea[...], begin, contract, preferred_element_type=F32)
        mixed = mixed + carried * per_head(decays, direction * heads, heads, width)
    gated = mixed * silu(gate[...].astype(F32))
    scale = lax.rsqrt(jnp.mean(gated * gated, axis=-1, keepdims=True) + EPSILON)
    out[...] = (gated * scale * gain[...]).astype(BF16)


def output_body(where, *refs, count):
    blocks, (weight, own, oth, gate), out = refs[:count], refs[count : count + 4], refs[-1]
    n = blocks[0].shape[1]
    total = None
    for b, block in enumerate(blocks):
        at = pl.multiple_of(where[2 + b] * n, n)
        term = jnp.dot(block[...], weight[pl.ds(at, n), :], preferred_element_type=F32)
        total = term if total is None else total + term
    tiles = pl.num_programs(0) // 2
    mine = jnp.where(pl.program_id(0) // tiles == where[0], 1.0, 0.0)
    rest = own[...].astype(F32) * mine + oth[...].astype(F32) * (1.0 - mine)
    out[...] = (rest + gate[...] * total).astype(BF16)


def whole(shape):
    return pl.BlockSpec(shape, lambda *_: (0,) * len(shape))


def shaped(shape, dtype):
    return pltpu.HBM(shape, dtype)


def placed(*arrays):
    return [pltpu.with_memory_space_constraint(a, pltpu.HBM) for a in arrays]


def in_vmem(*arrays):
    return [pltpu.with_memory_space_constraint(a, pltpu.VMEM) for a in arrays]


def on_device(
    latent, context, condition, context_condition, shift_weight, scale_weight, gate_weight,
    norm_gain, out_gate_weight, signal_weight, writer_weight, reader_matrix, step_weight,
    signal_taps, writer_taps, reader_taps, step_bias, decay_log, decay_extra, group_gain,
    output_weight,
):
    sp, tp, dp = lax.axis_index("sp"), lax.axis_index("tp"), lax.axis_index("dp")
    n_sp, n_tp, n_dp = lax.axis_size("sp"), lax.axis_size("tp"), lax.axis_size("dp")
    half, d_model = latent.shape
    length = half * n_dp
    ctx_len = context.shape[0]
    heads = step_bias.shape[1]
    n_sig = signal_weight.shape[1]
    n_gate = out_gate_weight.shape[1]
    n_state = writer_weight.shape[1]
    n_out = output_weight.shape[1]

    rows_here, cols_here = shift_weight.shape
    cond_act = jax.nn.silu(jnp.stack([condition, context_condition]).astype(F32)).astype(BF16)
    own_rows = lax.dynamic_slice_in_dim(cond_act, sp * rows_here, rows_here, 1)
    parts = pl.pallas_call(
        condense_body,
        out_shape=shaped((n_sp, 5, cols_here), F32),
        compiler_params=pltpu.CompilerParams(vmem_limit_bytes=8 * MIB),
        name="condense",
    )(own_rows, *placed(shift_weight, scale_weight, gate_weight))
    latent, context, sent = lax.optimization_barrier((latent, context, parts))
    sums = lax.all_to_all(sent, "sp", split_axis=0, concat_axis=0, tiled=True)
    vectors, gate_vec = pl.pallas_call(
        fold_body,
        out_shape=(
            shaped((n_tp * n_dp, 4, cols_here), F32),
            shaped((1, cols_here), F32),
        ),
        compiler_params=pltpu.CompilerParams(vmem_limit_bytes=8 * MIB),
        name="fold",
    )(sums)
    vectors = lax.all_to_all(vectors, ("tp", "dp"), split_axis=0, concat_axis=0, tiled=True)

    oth = shifted(latent, "dp", 1)
    edge = jnp.where(
        dp == 1,
        jnp.concatenate([latent[-1:], context[-1:]]),
        jnp.concatenate([latent[:1], context[:1]]),
    )
    pairs = {0: [], 1: []}
    for s in range(n_sp):
        for flip in pairs:
            if s + 1 < n_sp:
                pairs[flip].append((2 * s + 1, 2 * (s + 1) + 1 - flip))
            if s:
                pairs[flip].append((2 * s, 2 * (s - 1) + flip))
    same = lax.ppermute(edge, ("sp", "dp"), pairs[0])
    crossed = lax.ppermute(edge, ("sp", "dp"), pairs[1])

    flags = jnp.stack([dp, sp == 0, sp == n_sp - 1]).astype(jnp.int32)
    taps = jnp.concatenate([signal_taps, writer_taps, reader_taps], axis=1)
    steps = jnp.moveaxis(step_weight, 0, 1).reshape(d_model, 2 * heads)
    extra = decay_extra.reshape(2 * heads, length)
    n_all = n_gate + n_sig + 2 * n_state + 2 * heads
    n_rows = length + ctx_len + 2 * EDGES
    part = n_sig // n_sp
    tail = KINDS * PIECES
    conv_w = n_sig + 2 * n_state
    tile = lambda rows: pl.BlockSpec((rows, cols_here), lambda k, *_: (0, k))
    down = lambda cols: pl.BlockSpec((cols_here, cols), lambda k, *_: (k, 0))
    outs = (
        shaped((length, n_gate), BF16),
        shaped((length, n_sig), BF16),
        shaped((length, n_state), BF16),
        shaped((length, n_state), BF16),
        shaped((4 * heads, length), F32),
        shaped((length, LANES), F32),
        shaped((n_sp, KINDS * part + tail, n_state), BF16),
    )
    gate_in, signal, writer, reader, rows, cols, payload = pl.pallas_call(
        functools.partial(project_body, heads=heads),
        out_shape=outs,
        grid_spec=pltpu.PrefetchScalarGridSpec(
            num_scalar_prefetch=1,
            grid=(d_model // cols_here,),
            in_specs=[
                tile(half), tile(half), tile(ctx_len), tile(2), tile(2), tile(1),
                pl.BlockSpec((1, 4, cols_here), lambda k, *_: (k, 0, 0)),
                down(n_gate), down(n_sig), down(n_state), down(n_state), down(2 * heads),
                whole((3, conv_w)), whole((2 * heads, 1)), whole((2 * heads, 1)),
                whole((2 * heads, length)),
            ],
            out_specs=[whole(o.shape) for o in outs],
            scratch_shapes=[
                pltpu.VMEM((n_rows, n_all), F32),
                pltpu.VMEM((n_rows, cols_here), BF16),
                pltpu.VMEM((n_rows, LANES), F32),
                pltpu.VMEM((length + 16, conv_w), F32),
                pltpu.VMEM((ctx_len + 16, conv_w), F32),
                pltpu.VMEM((length + LANES, LANES), F32),
            ],
        ),
        compiler_params=pltpu.CompilerParams(
            dimension_semantics=("arbitrary",), vmem_limit_bytes=28 * MIB
        ),
        cost_estimate=pl.CostEstimate(
            flops=2 * n_rows * d_model * n_all, transcendentals=0,
            bytes_accessed=2 * d_model * (n_rows + n_all),
        ),
        name="project",
    )(
        flags, *placed(latent), oth, *placed(context), same, crossed, norm_gain.reshape(1, -1), vectors,
        *placed(out_gate_weight, signal_weight, writer_weight, reader_matrix, steps),
        taps, step_bias.reshape(-1, 1), decay_log.reshape(-1, 1), extra,
    )

    got = lax.all_to_all(payload, "sp", split_axis=0, concat_axis=0, tiled=True)
    row_block = lambda cols_: pl.BlockSpec((I_TILE, cols_), lambda i: (i, 0))
    inside = pl.pallas_call(
        functools.partial(inside_body, heads=heads),
        out_shape=shaped((length, n_sig), F32),
        grid=(length // I_TILE,),
        in_specs=[
            row_block(n_state), whole((length, n_state)), whole((length, n_sig)),
            whole((4 * heads, length)), row_block(LANES),
        ],
        out_specs=row_block(n_sig),
        compiler_params=pltpu.CompilerParams(vmem_limit_bytes=16 * MIB),
        cost_estimate=pl.CostEstimate(
            flops=2 * length * length * (n_state + 4 * n_sig),
            transcendentals=heads * length * length,
            bytes_accessed=4 * length * n_sig,
        ),
        name="inside",
    )(*placed(reader, writer, signal, rows, cols))
    starts = pl.pallas_call(
        functools.partial(chain_body, part=part),
        out_shape=shaped((n_sp, 2 * part, n_state), BF16),
        compiler_params=pltpu.CompilerParams(vmem_limit_bytes=4 * MIB),
        name="chain",
    )(got)
    starts = lax.all_to_all(starts, "sp", split_axis=0, concat_axis=0, tiled=True)
    normed = pl.pallas_call(
        functools.partial(finish_body, heads=heads),
        out_shape=pltpu.VMEM((length, n_sig), BF16),
        compiler_params=pltpu.CompilerParams(vmem_limit_bytes=12 * MIB),
        name="finish",
    )(*in_vmem(starts), *placed(reader, cols, inside, gate_in), group_gain.reshape(1, -1))
    at = tp * n_dp + dp
    blocks, places = [normed], [at]
    for by in (*range(2, n_tp - 1), n_tp - 1, 1):
        blocks.append(shifted(normed, "tp", by))
        places.append((tp + n_tp - by) % n_tp * n_dp + dp)
    for one, place in list(zip(blocks, places)):
        blocks.append(shifted(one, "dp", 1))
        places.append(place - dp + 1 - dp)
    where = jnp.stack([dp, at, *places]).astype(jnp.int32)
    count = len(blocks)
    rows_out = half // 2
    return pl.pallas_call(
        functools.partial(output_body, count=count),
        out_shape=shaped((length, n_out), BF16),
        grid_spec=pltpu.PrefetchScalarGridSpec(
            num_scalar_prefetch=1,
            grid=(length // rows_out,),
            in_specs=[pl.BlockSpec((rows_out, n_sig), lambda i, w: (i, 0))] * count
            + [
                whole(output_weight.shape),
                pl.BlockSpec((rows_out, n_out), lambda i, w: (i % 2, w[1])),
                pl.BlockSpec((rows_out, n_out), lambda i, w: (i % 2, w[1])),
                whole((1, n_out)),
            ],
            out_specs=pl.BlockSpec((rows_out, n_out), lambda i, w: (i, 0)),
        ),
        compiler_params=pltpu.CompilerParams(vmem_limit_bytes=14 * MIB),
        cost_estimate=pl.CostEstimate(
            flops=2 * length * n_sig * count * n_out, transcendentals=0,
            bytes_accessed=2 * count * n_sig * (length + n_out),
        ),
        name="output",
    )(where, *in_vmem(*blocks), *placed(output_weight, latent), oth, gate_vec)


def solution(mesh):
    tensor = ("tp", "dp")
    in_specs = (
        P(("grp", "sp", "dp"), None), P(("grp", "sp"), None), P("grp"), P(),
        P("sp", tensor), P("sp", tensor), P("sp", tensor), P(),
        P(None, tensor), P(None, tensor), P(None, tensor), P(None, tensor),
        P(None, None, tensor), P(None, tensor), P(None, tensor), P(None, tensor),
        P(None, tensor), P(None, tensor), P(None, tensor, ("grp", "sp")), P(tensor),
        P(None, tensor),
    )
    return jax.shard_map(
        on_device, mesh=mesh, in_specs=in_specs, out_specs=P(("grp", "sp"), tensor),
        check_vma=False,
    )
```

time: 482 us -> 154 us (0.32)
  waiting for transfers between devices: 140 us -> 11 us
  other arithmetic: 98.2 us -> 0.94 us
  blocking collectives: 85.9 us -> 18.4 us
  local copies, waits for them, and re-layouts: 67.5 us -> 8.53 us
  starting transfers between devices: 30.8 us -> 77 us
  matrix products: 40.4 us -> 0 us
  Pallas kernels: 0 us -> 36.8 us
  between operations: 14.2 us -> 0.13 us
    all_gather x4 -> x0, waiting for transfers between devices: 129 us -> none  [the longest x2 87.5 us: entering(): everything = jax.tree.map(lambda part: lax.all_gather(part, axis), x)]
    all_gather x4 -> x0, blocking collectives: 85.9 us -> none  [the longest x2 42.4 us: entering(): everything = jax.tree.map(lambda part: lax.all_gather(part, axis), x)]
    ppermute x2 -> x10, starting transfers between devices: 5.99 us -> 49.4 us  [the longest x8 42.8 us: shifted(): return lax.ppermute(x, axis, [(i, (i + by) % n) for i in range(n)])]
    dot_general x25 -> x0, matrix products: 40.4 us -> none  [the longest x1 5.52 us: on_device(): jnp.dot(hidden, out_gate_weight, preferred_element_type=jnp.float32)]
    pallas_call x0 -> x7, Pallas kernels: none -> 36.8 us  [the longest x1 15.9 us: on_device(): pl.pallas_call(functools.partial(project_body, heads=heads), out_shape=ou...]
    select_n x33 -> x1, other arithmetic: 31.7 us -> 0.08 us  [on_device(): jnp.where(dp == 1, jnp.concatenate([latent[-1:], context[-1:]]), jnp.conc...]
    exp x34 -> x0, other arithmetic: 25.8 us -> none  [the longest x32 22.3 us: chain_step(): jnp.exp(later[0])[:, None, None] * preceding_entries[1] + later[1]]
    all_to_all x0 -> x1, blocking collectives: none -> 18.4 us  [on_device(): got = lax.all_to_all(payload, 'sp', split_axis=0, concat_axis=0, tiled=True)]
  transfers between devices with their start and end apart: 7 -> 13, of which waited for: 4 -> 4; matrix products, arithmetic and copies ran while one was open for 22% -> 4% of each run, Pallas kernels for 0% -> 6%
where the time goes in v1:
time: 154 us; the launch traced here: 153 us
  starting transfers between devices  77 us (50%)
  Pallas kernels  36.8 us (24%)
  blocking collectives  18.4 us (12%)
  waiting for transfers between devices  11 us (7%)
  local copies, waits for them, and re-layouts  8.53 us (6%)
    ppermute x8, starting transfers between devices, shifted(): return lax.ppermute(x, axis, [(i, (i + by) % n) for i in range(n)])  42.8 us
    all_to_all x1, blocking collectives, on_device(): got = lax.all_to_all(payload, 'sp', split_axis=0, concat_axis=0, tiled=True)  18.4 us
    pallas_call x1, Pallas kernels, on_device(): pl.pallas_call(functools.partial(project_body, heads=heads), out_shape=ou...  15.9 us
    all_to_all x1, starting transfers between devices, on_device(): lax.all_to_all(starts, 'sp', split_axis=0, concat_axis=0, tiled=True)  11.6 us
    all_to_all x1, starting transfers between devices, on_device(): lax.all_to_all(vectors, ('tp', 'dp'), split_axis=0, concat_axis=0, tiled=...  11.3 us
    pallas_call x1, Pallas kernels, on_device(): pl.pallas_call(functools.partial(inside_body, heads=heads), out_shape=sha...  8.32 us
    pallas_call x1, Pallas kernels, on_device(): pl.pallas_call(functools.partial(output_body, count=count), out_shape=sha...  6.4 us
    all_to_all x1, waiting for transfers between devices, on_device(): sums = lax.all_to_all(sent, 'sp', split_axis=0, concat_axis=0, tiled=True)  5.65 us
  transfers between devices with their start and end apart: 13, of which 4 were waited for; matrix products, arithmetic and copies ran while one was open for 4% of the time, Pallas kernels for 6%

profile of v1, /device:TPU:33, one launch (start us, length us, event | category | flops | bytes accessed | tf_op | source)
XLA Modules:
  0.0 152.8 jit_solution(7338865261207560028)
XLA Ops:
  0.0 0.0 copy-start.4
  0.0 0.7 stack.71
  0.7 0.7 stack.72
  1.5 2.1 %condense.1 = f32[16,5,512]{2,1,0:T(8,128)} custom-call(bf16[2,256]{1,0:T(2,128)(2,1)S(1)} %fusion.cond, bf16[256,512]{1,0:T(8,128)(2,1)} %shift.1, bf16[256,512]{1,0:T(8,128)(2,1)} %scale.1, bf16[256,512]{1,0:T(8,128)(2,1)} %gate.1), custom_call_target="tpu_custom_call" | custom-call | tf_op jit(solution)/shard_map/condense/pallas_call | solution.py:352
  3.6 20.4 %collective-permute-start = (bf16[384,4096]{1,0:T(8,128)(2,1)}, bf16[384,4096]{1,0:T(8,128)(2,1)S(1)}, u32[]{:S(2)}, u32[]{:S(2)}) collective-permute-start(bf16[384,4096]{1,0:T(8,128)(2,1)} %refs_9_), channel_id=1, source_target_pairs={{0,1},{1,0},{2,3},{3,2},{4,5},{5,4},{6,7},{7,6},{8,9},{9,8},{10,11... | collective-permute-start | bytes 9437192 | tf_op jit(solution)/shard_map/ppermute | solution.py:23
  24.0 4.7 %all-to-all-start = ((f32[16,5,512]{2,1,0:T(8,128)}), f32[16,5,512]{2,1,0:T(8,128)S(1)}, u32[]{:S(2)}, u32[]{:S(2)}) async-start(f32[16,5,512]{2,1,0:T(8,128)} %condense.1), calls=%async_computation | async-start | bytes 524288 | tf_op jit(solution)/shard_map/all_to_all | solution.py:359
  28.7 1.0 fusion.1
  29.7 0.1 broadcast_select_fusion
  29.8 3.5 %collective-permute-start.2 = (bf16[2,4096]{1,0:T(2,128)(2,1)S(1)}, bf16[2,4096]{1,0:T(2,128)(2,1)S(1)}, u32[]{:S(2)}, u32[]{:S(2)}) collective-permute-start(bf16[2,4096]{1,0:T(2,128)(2,1)S(1)} %broadcast_select_fusion), channel_id=1, source_target_pairs={{1,8},{9,16},{8,1},{17,24},{16,9},{25,32},{24,17},{33,40},{32,25},... | collective-permute-start | bytes 49160 | tf_op jit(solution)/shard_map/ppermute | solution.py:385
  33.3 3.1 %collective-permute-start.1 = (bf16[2,4096]{1,0:T(2,128)(2,1)S(1)}, bf16[2,4096]{1,0:T(2,128)(2,1)S(1)}, u32[]{:S(2)}, u32[]{:S(2)}) collective-permute-start(bf16[2,4096]{1,0:T(2,128)(2,1)S(1)} %broadcast_select_fusion), channel_id=1, source_target_pairs={{1,9},{9,17},{8,0},{17,25},{16,8},{25,33},{24,16},{33,41},{32,24},... | collective-permute-start | bytes 49160 | tf_op jit(solution)/shard_map/ppermute | solution.py:384
  36.5 0.7 pad_maximum_fusion.taps
  37.2 5.6 %all-to-all-done.got = f32[16,5,512]{2,1,0:T(8,128)S(1)} async-done(((f32[16,5,512]{2,1,0:T(8,128)}), f32[16,5,512]{2,1,0:T(8,128)S(1)}, u32[]{:S(2)}, u32[]{:S(2)}) %all-to-all-start) | async-done | bytes 163872 | tf_op jit(solution)/shard_map/all_to_all | solution.py:359
  42.8 0.7 fold.1
  43.5 11.3 %all-to-all-start.1 = ((f32[8,4,512]{2,1,0:T(4,128)}), f32[8,4,512]{2,1,0:T(4,128)S(1)}, u32[]{:S(2)}, u32[]{:S(2)}) async-start(f32[8,4,512]{2,1,0:T(4,128)} %get-tuple-element.20), calls=%async_computation.1 | async-start | bytes 131072 | tf_op jit(solution)/shard_map/all_to_all | solution.py:369
  54.8 0.1 pad_add_fusion.flags
  54.9 0.8 reshape.26.bias
  55.6 0.8 reshape.27.dlog
  56.4 0.8 reshape.22.extra
  57.2 0.9 reshape.19
  58.0 1.3 copy.25.w_step
  59.4 0.0 collective-permute-done.2.crossed
  59.4 0.0 collective-permute-done.1.same
  59.4 0.3 all-to-all-done.1.vectors
  59.7 0.0 collective-permute-done.oth.refs_10_
  59.7 0.0 copy-done.4
  59.7 15.9 %project.1 = (bf16[768,256]{1,0:T(8,128)(2,1)}, bf16[768,256]{1,0:T(8,128)(2,1)}, bf16[768,128]{1,0:T(8,128)(2,1)}, bf16[768,128]{1,0:T(8,128)(2,1)}, f32[16,768...) custom-call(s32[3]{0:T(128)S(1)} %pad_add_fusion.flags, bf16[384,4096]{1,0:T(8,128)(2,1)} %refs_9_, ...), custom_call_target="tpu_custom_call" | custom-call | flops 5289017344 | bytes 13172736 | tf_op jit(solution)/shard_map/project/pallas_call | solution.py:407
  75.6 0.0 copy-start.3
  75.6 18.4 %all_to_all.20.got = bf16[16,72,128]{2,1,0:T(8,128)(2,1)S(1)} all-to-all(bf16[16,72,128]{2,1,0:T(8,128)(2,1)} %get-tuple-element.21), channel_id=1, replica_groups=mesh['grp'=2,'sp'=16,'tp'=4,'dp'=2] {'sp'}, dimensions={0} | all-to-all | bytes 589824 | tf_op jit(solution)/shard_map/all_to_all | solution.py:444
  94.0 0.8 chain.1
  94.8 11.6 %all-to-all-start.3 = ((bf16[16,32,128]{2,1,0:T(8,128)(2,1)}), bf16[16,32,128]{2,1,0:T(8,128)(2,1)S(1)}, u32[]{:S(2)}, u32[]{:S(2)}) async-start(bf16[16,32,128]{2,1,0:T(8,128)(2,1)} %chain.1), calls=%async_computation.3 | async-start | bytes 262144 | tf_op jit(solution)/shard_map/all_to_all | solution.py:469
  106.3 0.0 copy-start.2
  106.3 8.3 %inside.1 = f32[768,256]{1,0:T(8,128)} custom-call(bf16[768,128]{1,0:T(8,128)(2,1)} %get-tuple-element.22.rea, bf16[768,128]{1,0:T(8,128)(2,1)} %get-tuple-element.24.wri, bf16[768,256]{1,0:T(8,128)(2,1)} %get-tuple-element.25.sig, f32[16,768]{1,0:T(8,128)} %get-tuple-element.26.rows, f32[768,128]{1,0:T(8,128)} %get-tuple-element.23.cols), custom_call_target="tpu_custom_call" | custom-call | flops 1358954496 | bytes 786432 | tf_op jit(solution)/shard_map/inside/pallas_call | solution.py:446
  114.7 3.4 %all-to-all-done.3.starts = bf16[16,32,128]{2,1,0:T(8,128)(2,1)S(1)} async-done(((bf16[16,32,128]{2,1,0:T(8,128)(2,1)}), bf16[16,32,128]{2,1,0:T(8,128)(2,1)S(1)}, u32[]{:S(2)}, u32[]{:S(2)}) %all-to-all-start.3) | async-done | bytes 131104 | tf_op jit(solution)/shard_map/all_to_all | solution.py:469
  118.1 0.0 copy-start
  118.1 0.6 copy-done
  118.7 0.0 copy-done.3
  118.7 0.0 copy-start.1
  118.7 0.9 copy-done.1
  119.6 2.6 %finish.1.refs_0_ = bf16[768,256]{1,0:T(8,128)(2,1)S(1)} custom-call(bf16[16,32,128]{2,1,0:T(8,128)(2,1)S(1)} %copy-done.1, bf16[768,128]{1,0:T(8,128)(2,1)} %get-tuple-element.22.rea, f32[768,128]{1,0:T(8,128)} %get-tuple-element.23.cols, f32[768,256]{1,0:T(8,128)} %inside.1, bf16[768,256]{1,0:T(8,128)(2,1)} %get-tuple-element.27.gate, f32[1,256]{1,0:T(1,128)S(1)} %bitcast.16), custom_call_target="tpu_custom_call" | custom-call | tf_op jit(solution)/shard_map/finish/pallas_call | solution.py:470
  122.3 1.4 collective-permute-start.5
  123.7 1.4 collective-permute-start.4
  125.1 1.6 %collective-permute-start.3 = (bf16[768,256]{1,0:T(8,128)(2,1)S(1)}, bf16[768,256]{1,0:T(8,128)(2,1)}, u32[]{:S(2)}, u32[]{:S(2)}) collective-permute-start(bf16[768,256]{1,0:T(8,128)(2,1)S(1)} %finish.1.refs_0_), channel_id=1, source_target_pairs={{0,4},{2,6},{4,0},{6,2},{1,5},{3,7},{5,1},{7,3},{8,12},{10,14},{12... | collective-permute-start | bytes 1179656 | tf_op jit(solution)/shard_map/ppermute | solution.py:23
  126.6 4.6 %collective-permute-start.6 = (bf16[768,256]{1,0:T(8,128)(2,1)S(1)}, bf16[768,256]{1,0:T(8,128)(2,1)}, u32[]{:S(2)}, u32[]{:S(2)}) collective-permute-start(bf16[768,256]{1,0:T(8,128)(2,1)S(1)} %finish.1.refs_0_), channel_id=1, source_target_pairs={{0,1},{1,0},{2,3},{3,2},{4,5},{5,4},{6,7},{7,6},{8,9},{9,8},{10,11... | collective-permute-start | bytes 1179656 | tf_op jit(solution)/shard_map/ppermute | solution.py:23
  131.2 0.0 collective-permute-done.5.refs_3_
  131.2 7.3 %collective-permute-start.9 = (bf16[768,256]{1,0:T(8,128)(2,1)}, bf16[768,256]{1,0:T(8,128)(2,1)}, u32[]{:S(2)}, u32[]{:S(2)}) collective-permute-start(bf16[768,256]{1,0:T(8,128)(2,1)} %collective-permute-done.5.refs_3_), channel_id=1, source_target_pairs={{0,1},{1,0},{2,3},{3,2},{4,5},{5,4},{6,7},{7,6},{8,9},{9,8},{10,11... | collective-permute-start | bytes 1179656 | tf_op jit(solution)/shard_map/ppermute | solution.py:23
  138.5 0.0 collective-permute-done.4.refs_2_
  138.5 4.3 %collective-permute-start.8 = (bf16[768,256]{1,0:T(8,128)(2,1)}, bf16[768,256]{1,0:T(8,128)(2,1)}, u32[]{:S(2)}, u32[]{:S(2)}) collective-permute-start(bf16[768,256]{1,0:T(8,128)(2,1)} %collective-permute-done.4.refs_2_), channel_id=1, source_target_pairs={{0,1},{1,0},{2,3},{3,2},{4,5},{5,4},{6,7},{7,6},{8,9},{9,8},{10,11... | collective-permute-start | bytes 1179656 | tf_op jit(solution)/shard_map/ppermute | solution.py:23
  142.9 0.0 collective-permute-done.3.refs_1_
  142.9 1.8 %collective-permute-start.7 = (bf16[768,256]{1,0:T(8,128)(2,1)}, bf16[768,256]{1,0:T(8,128)(2,1)}, u32[]{:S(2)}, u32[]{:S(2)}) collective-permute-start(bf16[768,256]{1,0:T(8,128)(2,1)} %collective-permute-done.3.refs_1_), channel_id=1, source_target_pairs={{0,1},{1,0},{2,3},{3,2},{4,5},{5,4},{6,7},{7,6},{8,9},{9,8},{10,11... | collective-permute-start | bytes 1179656 | tf_op jit(solution)/shard_map/ppermute | solution.py:23
  144.7 0.1 stack.65.where
  144.7 0.0 collective-permute-done.6.refs_4_
  144.7 0.0 collective-permute-done.9.refs_7_
  144.8 0.0 collective-permute-done.8.refs_6_
  144.8 1.6 %collective-permute-done.7.refs_5_ = bf16[768,256]{1,0:T(8,128)(2,1)} collective-permute-done((bf16[768,256]{1,0:T(8,128)(2,1)}, bf16[768,256]{1,0:T(8,128)(2,1)}, u32[]{:S(2)}, u32[]{:S(2)}) %collective-permute-start.7) | collective-permute-done | bytes 393248 | tf_op jit(solution)/shard_map/ppermute | solution.py:23
  146.3 0.0 copy-done.2
  146.3 6.4 %output.1 = bf16[768,512]{1,0:T(8,128)(2,1)} custom-call(s32[10]{0:T(128)S(1)} %stack.65.where, bf16[768,256]{1,0:T(8,128)(2,1)S(1)} %finish.1.refs_0_, bf16[768,256]{1,0:T(8,128)(2,1)} %collective-permute-done.3.refs_1_, bf16[768,256]{1,0:T(8,128)(2,1)} %collective-permute-done.4.refs_2_, bf16[768,256]{1,0:T(8,128)(2,1)} %collective-permute-done.5.refs_3_, ...), custom_call_target="tpu_custom_call" | custom-call | flops 1610612736 | bytes 5242880 | tf_op jit(solution)/shard_map/output/pallas_call | solution.py:487
  (2 shorter events, 0.1 us)
Async XLA Ops:
  0.0 59.7 %copy-start.4 = (f32[4096]{0:T(1024)S(1)}, f32[4096]{0:T(1024)}, u32[]{:S(2)}) copy-start(f32[4096]{0:T(1024)} %param.28) | copy-start | bytes 49156
  3.6 56.1 %collective-permute-start = (bf16[384,4096]{1,0:T(8,128)(2,1)}, bf16[384,4096]{1,0:T(8,128)(2,1)S(1)}, u32[]{:S(2)}, u32[]{:S(2)}) collective-permute-start(bf16[384,4096]{1,0:T(8,128)(2,1)} %refs_9_), channel_id=1, source_target_pairs={{0,1},{1,0},{2,3},{3,2},{4,5},{5,4},{6,7},{7,6},{8,9},{9,8},{10,11... | collective-permute-start | bytes 9437192 | tf_op jit(solution)/shard_map/ppermute | solution.py:23
  24.0 18.9 %all-to-all-start = ((f32[16,5,512]{2,1,0:T(8,128)}), f32[16,5,512]{2,1,0:T(8,128)S(1)}, u32[]{:S(2)}, u32[]{:S(2)}) async-start(f32[16,5,512]{2,1,0:T(8,128)} %condense.1), calls=%async_computation | async-start | bytes 524288 | tf_op jit(solution)/shard_map/all_to_all | solution.py:359
  29.8 29.6 %collective-permute-start.2 = (bf16[2,4096]{1,0:T(2,128)(2,1)S(1)}, bf16[2,4096]{1,0:T(2,128)(2,1)S(1)}, u32[]{:S(2)}, u32[]{:S(2)}) collective-permute-start(bf16[2,4096]{1,0:T(2,128)(2,1)S(1)} %broadcast_select_fusion), channel_id=1, source_target_pairs={{1,8},{9,16},{8,1},{17,24},{16,9},{25,32},{24,17},{33,40},{32,25},... | collective-permute-start | bytes 49160 | tf_op jit(solution)/shard_map/ppermute | solution.py:385
  33.3 26.0 %collective-permute-start.1 = (bf16[2,4096]{1,0:T(2,128)(2,1)S(1)}, bf16[2,4096]{1,0:T(2,128)(2,1)S(1)}, u32[]{:S(2)}, u32[]{:S(2)}) collective-permute-start(bf16[2,4096]{1,0:T(2,128)(2,1)S(1)} %broadcast_select_fusion), channel_id=1, source_target_pairs={{1,9},{9,17},{8,0},{17,25},{16,8},{25,33},{24,16},{33,41},{32,24},... | collective-permute-start | bytes 49160 | tf_op jit(solution)/shard_map/ppermute | solution.py:384
  43.5 16.2 %all-to-all-start.1 = ((f32[8,4,512]{2,1,0:T(4,128)}), f32[8,4,512]{2,1,0:T(4,128)S(1)}, u32[]{:S(2)}, u32[]{:S(2)}) async-start(f32[8,4,512]{2,1,0:T(4,128)} %get-tuple-element.20), calls=%async_computation.1 | async-start | bytes 131072 | tf_op jit(solution)/shard_map/all_to_all | solution.py:369
  75.6 43.1 %copy-start.3 = (f32[256]{0:T(256)S(1)}, f32[256]{0:T(256)}, u32[]{:S(2)}) copy-start(f32[256]{0:T(256)} %param.40) | copy-start | bytes 3076
  94.8 23.3 %all-to-all-start.3 = ((bf16[16,32,128]{2,1,0:T(8,128)(2,1)}), bf16[16,32,128]{2,1,0:T(8,128)(2,1)S(1)}, u32[]{:S(2)}, u32[]{:S(2)}) async-start(bf16[16,32,128]{2,1,0:T(8,128)(2,1)} %chain.1), calls=%async_computation.3 | async-start | bytes 262144 | tf_op jit(solution)/shard_map/all_to_all | solution.py:469
  106.3 40.0 %copy-start.2 = (f32[1,512]{1,0:T(1,128)S(1)}, f32[1,512]{1,0:T(1,128)}, u32[]{:S(2)}) copy-start(f32[1,512]{1,0:T(1,128)} %get-tuple-element.28.refs_11_) | copy-start | bytes 6148
  118.1 0.6 copy-start
  118.7 0.9 copy-start.1
  122.3 8.9 %collective-permute-start.5 = (bf16[768,256]{1,0:T(8,128)(2,1)S(1)}, bf16[768,256]{1,0:T(8,128)(2,1)}, u32[]{:S(2)}, u32[]{:S(2)}) collective-permute-start(bf16[768,256]{1,0:T(8,128)(2,1)S(1)} %finish.1.refs_0_), channel_id=1, source_target_pairs={{0,2},{2,4},{4,6},{6,0},{1,3},{3,5},{5,7},{7,1},{8,10},{10,12},{12... | collective-permute-start | bytes 1179656 | tf_op jit(solution)/shard_map/ppermute | solution.py:23
  123.7 14.9 %collective-permute-start.4 = (bf16[768,256]{1,0:T(8,128)(2,1)S(1)}, bf16[768,256]{1,0:T(8,128)(2,1)}, u32[]{:S(2)}, u32[]{:S(2)}) collective-permute-start(bf16[768,256]{1,0:T(8,128)(2,1)S(1)} %finish.1.refs_0_), channel_id=1, source_target_pairs={{0,6},{2,0},{4,2},{6,4},{1,7},{3,1},{5,3},{7,5},{8,14},{10,8},{12,... | collective-permute-start | bytes 1179656 | tf_op jit(solution)/shard_map/ppermute | solution.py:23
  125.1 17.8 %collective-permute-start.3 = (bf16[768,256]{1,0:T(8,128)(2,1)S(1)}, bf16[768,256]{1,0:T(8,128)(2,1)}, u32[]{:S(2)}, u32[]{:S(2)}) collective-permute-start(bf16[768,256]{1,0:T(8,128)(2,1)S(1)} %finish.1.refs_0_), channel_id=1, source_target_pairs={{0,4},{2,6},{4,0},{6,2},{1,5},{3,7},{5,1},{7,3},{8,12},{10,14},{12... | collective-permute-start | bytes 1179656 | tf_op jit(solution)/shard_map/ppermute | solution.py:23
  126.6 18.1 %collective-permute-start.6 = (bf16[768,256]{1,0:T(8,128)(2,1)S(1)}, bf16[768,256]{1,0:T(8,128)(2,1)}, u32[]{:S(2)}, u32[]{:S(2)}) collective-permute-start(bf16[768,256]{1,0:T(8,128)(2,1)S(1)} %finish.1.refs_0_), channel_id=1, source_target_pairs={{0,1},{1,0},{2,3},{3,2},{4,5},{5,4},{6,7},{7,6},{8,9},{9,8},{10,11... | collective-permute-start | bytes 1179656 | tf_op jit(solution)/shard_map/ppermute | solution.py:23
  131.2 13.5 %collective-permute-start.9 = (bf16[768,256]{1,0:T(8,128)(2,1)}, bf16[768,256]{1,0:T(8,128)(2,1)}, u32[]{:S(2)}, u32[]{:S(2)}) collective-permute-start(bf16[768,256]{1,0:T(8,128)(2,1)} %collective-permute-done.5.refs_3_), channel_id=1, source_target_pairs={{0,1},{1,0},{2,3},{3,2},{4,5},{5,4},{6,7},{7,6},{8,9},{9,8},{10,11... | collective-permute-start | bytes 1179656 | tf_op jit(solution)/shard_map/ppermute | solution.py:23
  138.5 6.2 %collective-permute-start.8 = (bf16[768,256]{1,0:T(8,128)(2,1)}, bf16[768,256]{1,0:T(8,128)(2,1)}, u32[]{:S(2)}, u32[]{:S(2)}) collective-permute-start(bf16[768,256]{1,0:T(8,128)(2,1)} %collective-permute-done.4.refs_2_), channel_id=1, source_target_pairs={{0,1},{1,0},{2,3},{3,2},{4,5},{5,4},{6,7},{7,6},{8,9},{9,8},{10,11... | collective-permute-start | bytes 1179656 | tf_op jit(solution)/shard_map/ppermute | solution.py:23
  142.9 3.5 %collective-permute-start.7 = (bf16[768,256]{1,0:T(8,128)(2,1)}, bf16[768,256]{1,0:T(8,128)(2,1)}, u32[]{:S(2)}, u32[]{:S(2)}) collective-permute-start(bf16[768,256]{1,0:T(8,128)(2,1)} %collective-permute-done.3.refs_1_), channel_id=1, source_target_pairs={{0,1},{1,0},{2,3},{3,2},{4,5},{5,4},{6,7},{7,6},{8,9},{9,8},{10,11... | collective-permute-start | bytes 1179656 | tf_op jit(solution)/shard_map/ppermute | solution.py:23

commit v2 on v1

--- a/solution.py
+++ b/solution.py
@@ -15,6 +15,7 @@
 KINDS = 4
 PIECES = 2
 EDGES = 16
+CHUNKS = 2
 MIB = 2**20
 
 
@@ -55,18 +56,26 @@
     return ahead, behind
 
 
-def condense_body(cond, shift, scale, gate, out):
-    n = out.shape[0]
+def condense_body(where, cond, ctx_cond, shift, scale, gate, out, wide):
+    rows = shift.shape[0] // LANES
+    acts = []
+    for c, ref in enumerate((cond, ctx_cond)):
+        n = ref.shape[0]
+        wide[c * n : (c + 1) * n, :] = silu(ref[...].astype(F32))
+        picked = [wide[pl.ds(c * n + where[0] * rows + r, 1), :] for r in range(rows)]
+        acts.append(jnp.concatenate(picked, axis=1))
+    row = lax.broadcasted_iota(jnp.int32, (8, shift.shape[0]), 0)
+    acts = jnp.where(row == 0, acts[0], jnp.where(row == 1, acts[1], 0.0)).astype(BF16)
     parts = jnp.concatenate(
         [
-            jnp.dot(cond[...], shift[...], preferred_element_type=F32),
-            jnp.dot(cond[...], scale[...], preferred_element_type=F32),
-            jnp.dot(cond[...], gate[...], preferred_element_type=F32),
+            jnp.dot(acts, shift[...], preferred_element_type=F32)[:2, :],
+            jnp.dot(acts, scale[...], preferred_element_type=F32)[:2, :],
+            jnp.dot(acts, gate[...], preferred_element_type=F32)[:1, :],
         ],
         axis=0,
     )
-    for i in range(n):
-        out[i] = parts[: out.shape[1], :]
+    for i in range(out.shape[0]):
+        out[i] = parts
 
 
 def fold_body(got, out, gate):
@@ -79,11 +88,11 @@
 
 
 def project_body(
-    flags, own, oth, ctx, same, crossed, gain, vectors, w_gate, w_sig, w_wri, w_rea, w_step,
-    taps, bias, dlog, extra,
+    flags, own, oth, ctx, same, crossed, gain, vectors, w_gate, w_sig, w_wri, w_rea,
+    w_step, taps, bias, dlog, extra,
     gate_out, sig_out, wri_out, rea_out, rows_out, cols_out, payload,
-    acc, hidden, squares, pad, cpad, stpad,
-    *, heads,
+    acc, squares, pad, cpad, stpad, *hiddens,
+    heads,
 ):
     k = pl.program_id(0)
     half = own.shape[0]
@@ -95,17 +104,15 @@
     width = n_sig // heads
     conv_w = n_sig + 2 * n_state
     dp = flags[0]
+    first = dp == 0
+    wide = hiddens[0].shape[1]
 
     @pl.when(k == 0)
     def _():
         acc[...] = jnp.zeros_like(acc)
         squares[...] = jnp.zeros_like(squares)
 
-    w = jnp.concatenate([w_gate[...], w_sig[...], w_wri[...], w_rea[...], w_step[...]], axis=1)
-    g0, b0 = gain[...] * (1.0 + vectors[0, 2:3, :]), vectors[0, 0:1, :]
-    g1, b1 = gain[...] * (1.0 + vectors[0, 3:4, :]), vectors[0, 1:2, :]
-
-    def take(values, scale, at):
+    def take(hidden, values, scale, at):
         n = values.shape[0]
         hidden[at : at + n, :] = (values * scale).astype(BF16)
         part = values[:, :LANES] * values[:, :LANES]
@@ -114,25 +121,30 @@
             part = part + tile * tile
         squares[at : at + n, :] += part
 
-    first = dp == 0
-    edges_before = jnp.where(first, crossed[...].astype(F32), same[...].astype(F32))
-    edges_after = jnp.where(first, same[...].astype(F32), crossed[...].astype(F32))
-    row = lax.broadcasted_iota(jnp.int32, (EDGES, own.shape[1]), 0)
-    tile = jnp.zeros(row.shape, F32)
-    for r, value in enumerate(
-        (edges_before[1:2], edges_after[1:2], edges_before[0:1], edges_after[0:1])
-    ):
-        tile = jnp.where(row == r, value, tile)
-    take(tile, jnp.where(row < 2, g1, g0), length + ctx_len)
-    tile = jnp.zeros(row.shape, F32)
-    for r, value in enumerate((b0, b0 - rounded(b0), b1, b1 - rounded(b1))):
-        tile = jnp.where(row == r, value, tile)
-    at = length + ctx_len + EDGES
-    hidden[at : at + EDGES, :] = tile.astype(BF16)
-    take(ctx[...].astype(F32), g1, length)
-    take(own[...].astype(F32), g0, 0)
-    take(oth[...].astype(F32), g0, half)
-    acc[...] += jnp.dot(hidden[...], w, preferred_element_type=F32)
+    for c, hidden in enumerate(hiddens):
+        cut = slice(c * wide, (c + 1) * wide)
+        w = jnp.concatenate([r[cut, :] for r in (w_gate, w_sig, w_wri, w_rea, w_step)], axis=1)
+        g0, b0 = gain[:, cut] * (1.0 + vectors[c, 2:3, :]), vectors[c, 0:1, :]
+        g1, b1 = gain[:, cut] * (1.0 + vectors[c, 3:4, :]), vectors[c, 1:2, :]
+        edges = [same[:, cut].astype(F32), crossed[:, cut].astype(F32)]
+        edges_before = jnp.where(first, edges[1], edges[0])
+        edges_after = jnp.where(first, edges[0], edges[1])
+        row = lax.broadcasted_iota(jnp.int32, (EDGES, wide), 0)
+        tile = jnp.zeros(row.shape, F32)
+        for r, value in enumerate(
+            (edges_before[1:2], edges_after[1:2], edges_before[0:1], edges_after[0:1])
+        ):
+            tile = jnp.where(row == r, value, tile)
+        at = length + ctx_len
+        take(hidden, tile, jnp.where(row < 2, g1, g0), at)
+        tile = jnp.zeros(row.shape, F32)
+        for r, value in enumerate((b0, b0 - rounded(b0), b1, b1 - rounded(b1))):
+            tile = jnp.where(row == r, value, tile)
+        hidden[at + EDGES : at + 2 * EDGES, :] = tile.astype(BF16)
+        take(hidden, ctx[:, cut].astype(F32), g1, length)
+        take(hidden, own[:, cut].astype(F32), g0, 0)
+        take(hidden, oth[:, cut].astype(F32), g0, half)
+        acc[...] += jnp.dot(hidden[...], w, preferred_element_type=F32)
 
     @pl.when(k == pl.num_programs(0) - 1)
     def _():
@@ -300,17 +312,47 @@
 
 
 def output_body(where, *refs, count):
-    blocks, (weight, own, oth, gate), out = refs[:count], refs[count : count + 4], refs[-1]
-    n = blocks[0].shape[1]
-    total = None
-    for b, block in enumerate(blocks):
+    blocks, (weight, own, oth, gate, out) = refs[:count], refs[count : count + 5]
+    left, right, rest, done, sems = refs[count + 5 :]
+    length, n = blocks[0].shape
+    n_out = out.shape[1]
+    half = own.shape[0]
+    parts = length // half
+    column = pl.multiple_of(where[1] * n_out, n_out)
+    copies = []
+
+    def start(source, target):
+        copies.append(pltpu.make_async_copy(source, target, sems.at[len(copies)]))
+        copies[-1].start()
+
+    for b in range(count):
         at = pl.multiple_of(where[2 + b] * n, n)
-        term = jnp.dot(block[...], weight[pl.ds(at, n), :], preferred_element_type=F32)
-        total = term if total is None else total + term
-    tiles = pl.num_programs(0) // 2
-    mine = jnp.where(pl.program_id(0) // tiles == where[0], 1.0, 0.0)
-    rest = own[...].astype(F32) * mine + oth[...].astype(F32) * (1.0 - mine)
-    out[...] = (rest + gate[...] * total).astype(BF16)
+        start(weight.at[pl.ds(at, n), :], right.at[b * n : (b + 1) * n, :])
+        start(blocks[b].at[:half, :], left.at[:half, b * n : (b + 1) * n])
+    start(own.at[:, pl.ds(column, n_out)], rest.at[0])
+    start(oth.at[:, pl.ds(column, n_out)], rest.at[1])
+    for p in range(1, parts):
+        for b in range(count):
+            start(
+                blocks[b].at[p * half : (p + 1) * half, :],
+                left.at[p * half : (p + 1) * half, b * n : (b + 1) * n],
+            )
+    first = 2 * count + 2
+    for copy in copies[:first]:
+        copy.wait()
+    writes = []
+    for p in range(parts):
+        for copy in copies[first + (p - 1) * count : first + p * count] if p else []:
+            copy.wait()
+        rows = slice(p * half, (p + 1) * half)
+        total = jnp.dot(left[rows, :], right[...], preferred_element_type=F32)
+        mine = jnp.where(where[0] == p, 1.0, 0.0)
+        base = rest[0].astype(F32) * mine + rest[1].astype(F32) * (1.0 - mine)
+        done[rows, :] = (base + gate[...] * total).astype(BF16)
+        writes.append(pltpu.make_async_copy(done.at[rows, :], out.at[rows, :], sems.at[p]))
+        writes[-1].start()
+    for write in writes:
+        write.wait()
 
 
 def whole(shape):
@@ -346,17 +388,34 @@
     n_state = writer_weight.shape[1]
     n_out = output_weight.shape[1]
 
-    rows_here, cols_here = shift_weight.shape
-    cond_act = jax.nn.silu(jnp.stack([condition, context_condition]).astype(F32)).astype(BF16)
-    own_rows = lax.dynamic_slice_in_dim(cond_act, sp * rows_here, rows_here, 1)
+    cols_here = shift_weight.shape[1]
+    small = lambda n: pltpu.CompilerParams(vmem_limit_bytes=n * MIB)
     parts = pl.pallas_call(
         condense_body,
         out_shape=shaped((n_sp, 5, cols_here), F32),
-        compiler_params=pltpu.CompilerParams(vmem_limit_bytes=8 * MIB),
+        grid_spec=pltpu.PrefetchScalarGridSpec(
+            num_scalar_prefetch=1,
+            grid=(1,),
+            in_specs=[whole((d_model // LANES, LANES))] * 2 + [whole(shift_weight.shape)] * 3,
+            out_specs=whole((n_sp, 5, cols_here)),
+            scratch_shapes=[pltpu.VMEM((2 * d_model // LANES, LANES), F32)],
+        ),
+        compiler_params=small(8),
         name="condense",
-    )(own_rows, *placed(shift_weight, scale_weight, gate_weight))
+    )(
+        sp.astype(jnp.int32)[None],
+        *placed(condition.reshape(-1, LANES), context_condition.reshape(-1, LANES)),
+        *placed(shift_weight, scale_weight, gate_weight),
+    )
     latent, context, sent = lax.optimization_barrier((latent, context, parts))
     sums = lax.all_to_all(sent, "sp", split_axis=0, concat_axis=0, tiled=True)
+    taps = jnp.concatenate([signal_taps, writer_taps, reader_taps], axis=1)
+    steps = jnp.moveaxis(step_weight, 0, 1).reshape(d_model, 2 * heads)
+    extra = decay_extra.reshape(2 * heads, length)
+    bias, rates = step_bias.reshape(-1, 1), decay_log.reshape(-1, 1)
+    sums, taps, steps, extra, bias, rates = lax.optimization_barrier(
+        (sums, taps, steps, extra, bias, rates)
+    )
     vectors, gate_vec = pl.pallas_call(
         fold_body,
         out_shape=(
@@ -385,16 +444,14 @@
     crossed = lax.ppermute(edge, ("sp", "dp"), pairs[1])
 
     flags = jnp.stack([dp, sp == 0, sp == n_sp - 1]).astype(jnp.int32)
-    taps = jnp.concatenate([signal_taps, writer_taps, reader_taps], axis=1)
-    steps = jnp.moveaxis(step_weight, 0, 1).reshape(d_model, 2 * heads)
-    extra = decay_extra.reshape(2 * heads, length)
     n_all = n_gate + n_sig + 2 * n_state + 2 * heads
     n_rows = length + ctx_len + 2 * EDGES
     part = n_sig // n_sp
     tail = KINDS * PIECES
     conv_w = n_sig + 2 * n_state
-    tile = lambda rows: pl.BlockSpec((rows, cols_here), lambda k, *_: (0, k))
-    down = lambda cols: pl.BlockSpec((cols_here, cols), lambda k, *_: (k, 0))
+    k_tile = CHUNKS * cols_here
+    tile = lambda rows: pl.BlockSpec((rows, k_tile), lambda k, *_: (0, k))
+    down = lambda cols: pl.BlockSpec((k_tile, cols), lambda k, *_: (k, 0))
     outs = (
         shaped((length, n_gate), BF16),
         shaped((length, n_sig), BF16),
@@ -409,10 +466,11 @@
         out_shape=outs,
         grid_spec=pltpu.PrefetchScalarGridSpec(
             num_scalar_prefetch=1,
-            grid=(d_model // cols_here,),
+            grid=(d_model // k_tile,),
             in_specs=[
-                tile(half), tile(half), tile(ctx_len), tile(2), tile(2), tile(1),
-                pl.BlockSpec((1, 4, cols_here), lambda k, *_: (k, 0, 0)),
+                tile(half), tile(half), tile(ctx_len), tile(2), tile(2),
+                tile(1),
+                pl.BlockSpec((CHUNKS, 4, cols_here), lambda k, *_: (k, 0, 0)),
                 down(n_gate), down(n_sig), down(n_state), down(n_state), down(2 * heads),
                 whole((3, conv_w)), whole((2 * heads, 1)), whole((2 * heads, 1)),
                 whole((2 * heads, length)),
@@ -420,12 +478,12 @@
             out_specs=[whole(o.shape) for o in outs],
             scratch_shapes=[
                 pltpu.VMEM((n_rows, n_all), F32),
-                pltpu.VMEM((n_rows, cols_here), BF16),
                 pltpu.VMEM((n_rows, LANES), F32),
                 pltpu.VMEM((length + 16, conv_w), F32),
                 pltpu.VMEM((ctx_len + 16, conv_w), F32),
                 pltpu.VMEM((length + LANES, LANES), F32),
-            ],
+            ]
+            + [pltpu.VMEM((n_rows, cols_here), BF16)] * CHUNKS,
         ),
         compiler_params=pltpu.CompilerParams(
             dimension_semantics=("arbitrary",), vmem_limit_bytes=28 * MIB
@@ -438,7 +496,7 @@
     )(
         flags, *placed(latent), oth, *placed(context), same, crossed, norm_gain.reshape(1, -1), vectors,
         *placed(out_gate_weight, signal_weight, writer_weight, reader_matrix, steps),
-        taps, step_bias.reshape(-1, 1), decay_log.reshape(-1, 1), extra,
+        taps, bias, rates, extra,
     )
 
     got = lax.all_to_all(payload, "sp", split_axis=0, concat_axis=0, tiled=True)
@@ -460,6 +518,7 @@
         ),
         name="inside",
     )(*placed(reader, writer, signal, rows, cols))
+    got, inside = lax.optimization_barrier((got, inside))
     starts = pl.pallas_call(
         functools.partial(chain_body, part=part),
         out_shape=shaped((n_sp, 2 * part, n_state), BF16),
@@ -469,13 +528,13 @@
     starts = lax.all_to_all(starts, "sp", split_axis=0, concat_axis=0, tiled=True)
     normed = pl.pallas_call(
         functools.partial(finish_body, heads=heads),
-        out_shape=pltpu.VMEM((length, n_sig), BF16),
+        out_shape=shaped((length, n_sig), BF16),
         compiler_params=pltpu.CompilerParams(vmem_limit_bytes=12 * MIB),
         name="finish",
-    )(*in_vmem(starts), *placed(reader, cols, inside, gate_in), group_gain.reshape(1, -1))
+    )(starts, *placed(reader, cols, inside, gate_in), group_gain.reshape(1, -1))
     at = tp * n_dp + dp
-    blocks, places = [normed], [at]
-    for by in (*range(2, n_tp - 1), n_tp - 1, 1):
+    blocks, places = placed(normed), [at]
+    for by in (n_tp - 1, 1, *range(2, n_tp - 1)):
         blocks.append(shifted(normed, "tp", by))
         places.append((tp + n_tp - by) % n_tp * n_dp + dp)
     for one, place in list(zip(blocks, places)):
@@ -483,29 +542,26 @@
         places.append(place - dp + 1 - dp)
     where = jnp.stack([dp, at, *places]).astype(jnp.int32)
     count = len(blocks)
-    rows_out = half // 2
+    anywhere = pl.BlockSpec(memory_space=pl.ANY)
     return pl.pallas_call(
         functools.partial(output_body, count=count),
         out_shape=shaped((length, n_out), BF16),
         grid_spec=pltpu.PrefetchScalarGridSpec(
             num_scalar_prefetch=1,
-            grid=(length // rows_out,),
-            in_specs=[pl.BlockSpec((rows_out, n_sig), lambda i, w: (i, 0))] * count
-            + [
-                whole(output_weight.shape),
-                pl.BlockSpec((rows_out, n_out), lambda i, w: (i % 2, w[1])),
-                pl.BlockSpec((rows_out, n_out), lambda i, w: (i % 2, w[1])),
-                whole((1, n_out)),
+            grid=(1,),
+            in_specs=[anywhere] * (count + 3) + [whole((1, n_out))],
+            out_specs=anywhere,
+            scratch_shapes=[
+                pltpu.VMEM((length, n_sig * count), BF16),
+                pltpu.VMEM((n_sig * count, n_out), BF16),
+                pltpu.VMEM((2, half, n_out), BF16),
+                pltpu.VMEM((length, n_out), BF16),
+                pltpu.SemaphoreType.DMA((n_dp * (count + 1) + count + 1,)),
             ],
-            out_specs=pl.BlockSpec((rows_out, n_out), lambda i, w: (i, 0)),
-        ),
-        compiler_params=pltpu.CompilerParams(vmem_limit_bytes=14 * MIB),
-        cost_estimate=pl.CostEstimate(
-            flops=2 * length * n_sig * count * n_out, transcendentals=0,
-            bytes_accessed=2 * count * n_sig * (length + n_out),
-        ),
+        ),
+        compiler_params=small(24),
         name="output",
-    )(where, *in_vmem(*blocks), *placed(output_weight, latent), oth, gate_vec)
+    )(where, *placed(*blocks), *placed(output_weight, latent), oth, gate_vec)
 
 
 def solution(mesh):

time: 154 us -> 150 us (0.974)
  starting transfers between devices: 77 us -> 65.7 us
  blocking collectives: 18.4 us -> 23.3 us
  waiting for transfers between devices: 11 us -> 14.2 us
    all_to_all x1, starting transfers between devices: 11.6 us -> 4.44 us  [on_device(): got = lax.all_to_all(payload, 'sp', split_axis=0, concat_axis=0, tiled=True)]
    all_to_all x1, blocking collectives: 18.4 us -> 23.3 us  [on_device(): lax.all_to_all(starts, 'sp', split_axis=0, concat_axis=0, tiled=True)]
    all_to_all x1, waiting for transfers between devices: 5.65 us -> 0.83 us  [on_device(): sums = lax.all_to_all(sent, 'sp', split_axis=0, concat_axis=0, tiled=True)]
    ppermute x8, starting transfers between devices: 42.8 us -> 38.6 us  [shifted(): return lax.ppermute(x, axis, [(i, (i + by) % n) for i in range(n)])]
    ppermute x8, waiting for transfers between devices: 1.6 us -> 5.76 us  [shifted(): return lax.ppermute(x, axis, [(i, (i + by) % n) for i in range(n)])]
    optimization_barrier x0 -> x3, local copies, waits for them, and re-layouts: none -> 2.78 us  [on_device(): lax.optimization_barrier((sums, taps, steps, extra, bias, rates))]
    all_to_all x1, waiting for transfers between devices: 3.44 us -> 5.58 us  [on_device(): got = lax.all_to_all(payload, 'sp', split_axis=0, concat_axis=0, tiled=True)]
    all_to_all x1, waiting for transfers between devices: 0.3 us -> 1.98 us  [on_device(): lax.all_to_all(vectors, ('tp', 'dp'), split_axis=0, concat_axis=0, tiled=...]
  transfers between devices with their start and end apart: 13 -> 13, of which waited for: 4 -> 7; matrix products, arithmetic and copies ran while one was open for 4% -> 6% of each run, Pallas kernels for 6% -> 6%
where the time goes in v2:
time: 150 us; the launch traced here: 149 us
  starting transfers between devices  65.7 us (44%)
  Pallas kernels  36 us (24%)
  blocking collectives  23.3 us (16%)
  waiting for transfers between devices  14.2 us (9%)
  local copies, waits for them, and re-layouts  8.12 us (5%)
    ppermute x8, starting transfers between devices, shifted(): return lax.ppermute(x, axis, [(i, (i + by) % n) for i in range(n)])  38.6 us
    all_to_all x1, blocking collectives, on_device(): lax.all_to_all(starts, 'sp', split_axis=0, concat_axis=0, tiled=True)  23.3 us
    pallas_call x1, Pallas kernels, on_device(): pl.pallas_call(functools.partial(project_body, heads=heads), out_shape=ou...  15.1 us
    all_to_all x1, starting transfers between devices, on_device(): lax.all_to_all(vectors, ('tp', 'dp'), split_axis=0, concat_axis=0, tiled=...  11.3 us
    pallas_call x1, Pallas kernels, on_device(): pl.pallas_call(functools.partial(inside_body, heads=heads), out_shape=sha...  8.32 us
    ppermute x8, waiting for transfers between devices, shifted(): return lax.ppermute(x, axis, [(i, (i + by) % n) for i in range(n)])  5.76 us
    pallas_call x1, Pallas kernels, on_device(): pl.pallas_call(functools.partial(output_body, count=count), out_shape=sha...  5.68 us
    all_to_all x1, waiting for transfers between devices, on_device(): got = lax.all_to_all(payload, 'sp', split_axis=0, concat_axis=0, tiled=True)  5.58 us
  transfers between devices with their start and end apart: 13, of which 7 were waited for; matrix products, arithmetic and copies ran while one was open for 6% of the time, Pallas kernels for 6%

profile of v2, /device:TPU:33, one launch (start us, length us, event | category | flops | bytes accessed | tf_op | source)
XLA Modules:
  0.0 149.0 jit_solution(3909164546734267876)
XLA Ops:
  0.0 0.0 copy-start.2
  0.0 2.1 %condense.1 = f32[16,5,512]{2,1,0:T(8,128)} custom-call(s32[1]{0:T(128)} %bitcast.11.where, bf16[32,128]{1,0:T(8,128)(2,1)} %bitcast.22, bf16[32,128]{1,0:T(8,128)(2,1)} %bitcast.23, bf16[256,512]{1,0:T(8,128)(2,1)} %shift.1, bf16[256,512]{1,0:T(8,128)(2,1)} %scale.1, bf16[256,512]{1,0:T(8,128)(2,1)} %gate.1), custom_call_target="tpu_custom_call" | custom-call | tf_op jit(solution)/shard_map/condense/pallas_call | solution.py:393
  2.1 20.4 %collective-permute-start = (bf16[384,4096]{1,0:T(8,128)(2,1)}, bf16[384,4096]{1,0:T(8,128)(2,1)S(1)}, u32[]{:S(2)}, u32[]{:S(2)}) collective-permute-start(bf16[384,4096]{1,0:T(8,128)(2,1)} %refs_9_), channel_id=1, source_target_pairs={{0,1},{1,0},{2,3},{3,2},{4,5},{5,4},{6,7},{7,6},{8,9},{9,8},{10,11... | collective-permute-start | bytes 9437192 | tf_op jit(solution)/shard_map/ppermute | solution.py:24
  22.5 4.7 %all-to-all-start = ((f32[16,5,512]{2,1,0:T(8,128)}), f32[16,5,512]{2,1,0:T(8,128)S(1)}, u32[]{:S(2)}, u32[]{:S(2)}) async-start(f32[16,5,512]{2,1,0:T(8,128)} %condense.1), calls=%async_computation | async-start | bytes 524288 | tf_op jit(solution)/shard_map/all_to_all | solution.py:411
  27.2 1.0 fusion
  28.2 0.7 broadcast_select_fusion
  28.9 3.5 %collective-permute-start.2 = (bf16[2,4096]{1,0:T(2,128)(2,1)}, bf16[2,4096]{1,0:T(2,128)(2,1)S(1)}, u32[]{:S(2)}, u32[]{:S(2)}) collective-permute-start(bf16[2,4096]{1,0:T(2,128)(2,1)} %broadcast_select_fusion), channel_id=1, source_target_pairs={{1,8},{9,16},{8,1},{17,24},{16,9},{25,32},{24,17},{33,40},{32,25},... | collective-permute-start | bytes 49160 | tf_op jit(solution)/shard_map/ppermute | solution.py:444
  32.5 3.1 %collective-permute-start.1 = (bf16[2,4096]{1,0:T(2,128)(2,1)}, bf16[2,4096]{1,0:T(2,128)(2,1)S(1)}, u32[]{:S(2)}, u32[]{:S(2)}) collective-permute-start(bf16[2,4096]{1,0:T(2,128)(2,1)} %broadcast_select_fusion), channel_id=1, source_target_pairs={{1,9},{9,17},{8,0},{17,25},{16,8},{25,33},{24,16},{33,41},{32,24},... | collective-permute-start | bytes 49160 | tf_op jit(solution)/shard_map/ppermute | solution.py:443
  35.6 1.3 reshape.29
  36.9 1.3 reshape.30
  38.2 0.7 reshape.28.extra
  39.0 0.9 reshape.27
  39.8 0.7 pad_maximum_fusion.taps
  40.6 0.8 all-to-all-done.got
  41.4 0.7 fold.1
  42.0 11.3 %all-to-all-start.1 = ((f32[8,4,512]{2,1,0:T(4,128)}), f32[8,4,512]{2,1,0:T(4,128)S(1)}, u32[]{:S(2)}, u32[]{:S(2)}) async-start(f32[8,4,512]{2,1,0:T(4,128)} %get-tuple-element.29), calls=%async_computation.1 | async-start | bytes 131072 | tf_op jit(solution)/shard_map/all_to_all | solution.py:428
  53.3 0.1 pad_add_fusion.flags
  53.4 0.7 copy.26.bias
  54.1 0.8 copy.27.dlog
  54.9 1.3 copy.25.w_step
  56.2 0.0 collective-permute-done.2.crossed
  56.2 0.0 collective-permute-done.1.same
  56.2 2.0 %all-to-all-done.1.vectors = f32[8,4,512]{2,1,0:T(4,128)S(1)} async-done(((f32[8,4,512]{2,1,0:T(4,128)}), f32[8,4,512]{2,1,0:T(4,128)S(1)}, u32[]{:S(2)}, u32[]{:S(2)}) %all-to-all-start.1) | async-done | bytes 65568 | tf_op jit(solution)/shard_map/all_to_all | solution.py:428
  58.2 0.0 collective-permute-done.oth.refs_10_
  58.2 0.0 copy-done.2
  58.2 15.1 %project.1 = (bf16[768,256]{1,0:T(8,128)(2,1)}, bf16[768,256]{1,0:T(8,128)(2,1)}, bf16[768,128]{1,0:T(8,128)(2,1)}, bf16[768,128]{1,0:T(8,128)(2,1)}, f32[16,768...) custom-call(s32[3]{0:T(128)S(1)} %pad_add_fusion.flags, bf16[384,4096]{1,0:T(8,128)(2,1)} %refs_9_, ...), custom_call_target="tpu_custom_call" | custom-call | flops 5289017344 | bytes 13172736 | tf_op jit(solution)/shard_map/project/pallas_call | solution.py:464
  73.3 0.0 copy-start.1
  73.3 4.4 %all-to-all-start.2 = ((bf16[16,72,128]{2,1,0:T(8,128)(2,1)}), bf16[16,72,128]{2,1,0:T(8,128)(2,1)S(1)}, u32[]{:S(2)}, u32[]{:S(2)}) async-start(bf16[16,72,128]{2,1,0:T(8,128)(2,1)} %get-tuple-element.35), calls=%async_computation.2 | async-start | bytes 589824 | tf_op jit(solution)/shard_map/all_to_all | solution.py:502
  77.7 0.0 copy-start
  77.7 8.3 %inside.1 = f32[768,256]{1,0:T(8,128)} custom-call(bf16[768,128]{1,0:T(8,128)(2,1)} %get-tuple-element.36.rea, bf16[768,128]{1,0:T(8,128)(2,1)} %get-tuple-element.37.wri, bf16[768,256]{1,0:T(8,128)(2,1)} %get-tuple-element.38.sig, f32[16,768]{1,0:T(8,128)} %get-tuple-element.39.rows, f32[768,128]{1,0:T(8,128)} %get-tuple-element.40.cols), custom_call_target="tpu_custom_call" | custom-call | flops 1358954496 | bytes 786432 | tf_op jit(solution)/shard_map/inside/pallas_call | solution.py:504
  86.1 5.6 %all-to-all-done.2.got = bf16[16,72,128]{2,1,0:T(8,128)(2,1)S(1)} async-done(((bf16[16,72,128]{2,1,0:T(8,128)(2,1)}), bf16[16,72,128]{2,1,0:T(8,128)(2,1)S(1)}, u32[]{:S(2)}, u32[]{:S(2)}) %all-to-all-start.2) | async-done | bytes 294944 | tf_op jit(solution)/shard_map/all_to_all | solution.py:502
  91.6 0.8 chain.1
  92.4 23.3 %all_to_all.20.starts = bf16[16,32,128]{2,1,0:T(8,128)(2,1)S(1)} all-to-all(bf16[16,32,128]{2,1,0:T(8,128)(2,1)} %chain.1), channel_id=1, replica_groups=mesh['grp'=2,'sp'=16,'tp'=4,'dp'=2] {'sp'}, dimensions={0} | all-to-all | bytes 262144 | tf_op jit(solution)/shard_map/all_to_all | solution.py:528
  115.8 0.0 copy-done.1
  115.8 3.4 %finish.1.refs_0_ = bf16[768,256]{1,0:T(8,128)(2,1)} custom-call(bf16[16,32,128]{2,1,0:T(8,128)(2,1)S(1)} %all_to_all.20.starts, bf16[768,128]{1,0:T(8,128)(2,1)} %get-tuple-element.36.rea, f32[768,128]{1,0:T(8,128)} %get-tuple-element.40.cols, f32[768,256]{1,0:T(8,128)} %inside.1, bf16[768,256]{1,0:T(8,128)(2,1)} %get-tuple-element.43.gate, ...), custom_call_target="tpu_custom_call" | custom-call | tf_op jit(solution)/shard_map/finish/pallas_call | solution.py:529
  119.2 0.9 collective-permute-start.5
  120.0 0.6 collective-permute-start.4
  120.6 2.1 %collective-permute-start.3 = (bf16[768,256]{1,0:T(8,128)(2,1)}, bf16[768,256]{1,0:T(8,128)(2,1)}, u32[]{:S(2)}, u32[]{:S(2)}) collective-permute-start(bf16[768,256]{1,0:T(8,128)(2,1)} %finish.1.refs_0_), channel_id=1, source_target_pairs={{0,6},{2,0},{4,2},{6,4},{1,7},{3,1},{5,3},{7,5},{8,14},{10,8},{12,... | collective-permute-start | bytes 1179656 | tf_op jit(solution)/shard_map/ppermute | solution.py:24
  122.7 4.7 %collective-permute-start.6 = (bf16[768,256]{1,0:T(8,128)(2,1)}, bf16[768,256]{1,0:T(8,128)(2,1)}, u32[]{:S(2)}, u32[]{:S(2)}) collective-permute-start(bf16[768,256]{1,0:T(8,128)(2,1)} %finish.1.refs_0_), channel_id=1, source_target_pairs={{0,1},{1,0},{2,3},{3,2},{4,5},{5,4},{6,7},{7,6},{8,9},{9,8},{10,11... | collective-permute-start | bytes 1179656 | tf_op jit(solution)/shard_map/ppermute | solution.py:24
  127.4 0.2 collective-permute-done.5.refs_3_
  127.6 0.0 copy-start.3
  127.6 9.1 %collective-permute-start.9 = (bf16[768,256]{1,0:T(8,128)(2,1)S(1)}, bf16[768,256]{1,0:T(8,128)(2,1)}, u32[]{:S(2)}, u32[]{:S(2)}) collective-permute-start(bf16[768,256]{1,0:T(8,128)(2,1)S(1)} %collective-permute-done.5.refs_3_), channel_id=1, source_target_pairs={{0,1},{1,0},{2,3},{3,2},{4,5},{5,4},{6,7},{7,6},{8,9},{9,8},{10,11... | collective-permute-start | bytes 1179656 | tf_op jit(solution)/shard_map/ppermute | solution.py:24
  136.7 3.4 %collective-permute-done.4.refs_2_ = bf16[768,256]{1,0:T(8,128)(2,1)} collective-permute-done((bf16[768,256]{1,0:T(8,128)(2,1)}, bf16[768,256]{1,0:T(8,128)(2,1)}, u32[]{:S(2)}, u32[]{:S(2)}) %collective-permute-start.4) | collective-permute-done | bytes 393248 | tf_op jit(solution)/shard_map/ppermute | solution.py:24
  140.0 0.9 collective-permute-start.8
  140.9 0.0 collective-permute-done.3.refs_1_
  140.9 0.0 collective-permute-start.7
  140.9 0.1 stack.56.where
  141.0 0.0 collective-permute-done.6.refs_4_
  141.0 0.0 collective-permute-done.9.refs_7_
  141.0 1.6 %collective-permute-done.8.refs_6_ = bf16[768,256]{1,0:T(8,128)(2,1)} collective-permute-done((bf16[768,256]{1,0:T(8,128)(2,1)}, bf16[768,256]{1,0:T(8,128)(2,1)}, u32[]{:S(2)}, u32[]{:S(2)}) %collective-permute-start.8) | collective-permute-done | bytes 393248 | tf_op jit(solution)/shard_map/ppermute | solution.py:24
  142.6 0.6 collective-permute-done.7.refs_5_
  143.2 0.0 copy-done.3
  143.2 0.0 copy-done
  143.2 5.7 %output.1 = bf16[768,512]{1,0:T(8,128)(2,1)} custom-call(s32[10]{0:T(128)S(1)} %stack.56.where, bf16[768,256]{1,0:T(8,128)(2,1)} %finish.1.refs_0_, bf16[768,256]{1,0:T(8,128)(2,1)} %collective-permute-done.3.refs_1_, bf16[768,256]{1,0:T(8,128)(2,1)} %collective-permute-done.4.refs_2_, bf16[768,256]{1,0:T(8,128)(2,1)} %copy-done.3, ...), custom_call_target="tpu_custom_call" | custom-call | tf_op jit(solution)/shard_map/output/pallas_call | solution.py:546
Async XLA Ops:
  0.0 58.2 %copy-start.2 = (f32[4096]{0:T(1024)S(1)}, f32[4096]{0:T(1024)}, u32[]{:S(2)}) copy-start(f32[4096]{0:T(1024)} %param.28) | copy-start | bytes 49156
  2.1 56.1 %collective-permute-start = (bf16[384,4096]{1,0:T(8,128)(2,1)}, bf16[384,4096]{1,0:T(8,128)(2,1)S(1)}, u32[]{:S(2)}, u32[]{:S(2)}) collective-permute-start(bf16[384,4096]{1,0:T(8,128)(2,1)} %refs_9_), channel_id=1, source_target_pairs={{0,1},{1,0},{2,3},{3,2},{4,5},{5,4},{6,7},{7,6},{8,9},{9,8},{10,11... | collective-permute-start | bytes 9437192 | tf_op jit(solution)/shard_map/ppermute | solution.py:24
  22.5 18.9 %all-to-all-start = ((f32[16,5,512]{2,1,0:T(8,128)}), f32[16,5,512]{2,1,0:T(8,128)S(1)}, u32[]{:S(2)}, u32[]{:S(2)}) async-start(f32[16,5,512]{2,1,0:T(8,128)} %condense.1), calls=%async_computation | async-start | bytes 524288 | tf_op jit(solution)/shard_map/all_to_all | solution.py:411
  28.9 27.3 %collective-permute-start.2 = (bf16[2,4096]{1,0:T(2,128)(2,1)}, bf16[2,4096]{1,0:T(2,128)(2,1)S(1)}, u32[]{:S(2)}, u32[]{:S(2)}) collective-permute-start(bf16[2,4096]{1,0:T(2,128)(2,1)} %broadcast_select_fusion), channel_id=1, source_target_pairs={{1,8},{9,16},{8,1},{17,24},{16,9},{25,32},{24,17},{33,40},{32,25},... | collective-permute-start | bytes 49160 | tf_op jit(solution)/shard_map/ppermute | solution.py:444
  32.5 23.8 %collective-permute-start.1 = (bf16[2,4096]{1,0:T(2,128)(2,1)}, bf16[2,4096]{1,0:T(2,128)(2,1)S(1)}, u32[]{:S(2)}, u32[]{:S(2)}) collective-permute-start(bf16[2,4096]{1,0:T(2,128)(2,1)} %broadcast_select_fusion), channel_id=1, source_target_pairs={{1,9},{9,17},{8,0},{17,25},{16,8},{25,33},{24,16},{33,41},{32,24},... | collective-permute-start | bytes 49160 | tf_op jit(solution)/shard_map/ppermute | solution.py:443
  42.0 16.2 %all-to-all-start.1 = ((f32[8,4,512]{2,1,0:T(4,128)}), f32[8,4,512]{2,1,0:T(4,128)S(1)}, u32[]{:S(2)}, u32[]{:S(2)}) async-start(f32[8,4,512]{2,1,0:T(4,128)} %get-tuple-element.29), calls=%async_computation.1 | async-start | bytes 131072 | tf_op jit(solution)/shard_map/all_to_all | solution.py:428
  73.3 42.5 %copy-start.1 = (f32[256]{0:T(256)S(1)}, f32[256]{0:T(256)}, u32[]{:S(2)}) copy-start(f32[256]{0:T(256)} %param.40) | copy-start | bytes 3076
  73.3 18.4 %all-to-all-start.2 = ((bf16[16,72,128]{2,1,0:T(8,128)(2,1)}), bf16[16,72,128]{2,1,0:T(8,128)(2,1)S(1)}, u32[]{:S(2)}, u32[]{:S(2)}) async-start(bf16[16,72,128]{2,1,0:T(8,128)(2,1)} %get-tuple-element.35), calls=%async_computation.2 | async-start | bytes 589824 | tf_op jit(solution)/shard_map/all_to_all | solution.py:502
  77.7 65.5 %copy-start = (f32[1,512]{1,0:T(1,128)S(1)}, f32[1,512]{1,0:T(1,128)}, u32[]{:S(2)}) copy-start(f32[1,512]{1,0:T(1,128)} %get-tuple-element.44.refs_11_) | copy-start | bytes 6148
  119.2 8.4 %collective-permute-start.5 = (bf16[768,256]{1,0:T(8,128)(2,1)}, bf16[768,256]{1,0:T(8,128)(2,1)S(1)}, u32[]{:S(2)}, u32[]{:S(2)}) collective-permute-start(bf16[768,256]{1,0:T(8,128)(2,1)} %finish.1.refs_0_), channel_id=1, source_target_pairs={{0,4},{2,6},{4,0},{6,2},{1,5},{3,7},{5,1},{7,3},{8,12},{10,14},{12... | collective-permute-start | bytes 1179656 | tf_op jit(solution)/shard_map/ppermute | solution.py:24
  120.0 20.0 %collective-permute-start.4 = (bf16[768,256]{1,0:T(8,128)(2,1)}, bf16[768,256]{1,0:T(8,128)(2,1)}, u32[]{:S(2)}, u32[]{:S(2)}) collective-permute-start(bf16[768,256]{1,0:T(8,128)(2,1)} %finish.1.refs_0_), channel_id=1, source_target_pairs={{0,2},{2,4},{4,6},{6,0},{1,3},{3,5},{5,7},{7,1},{8,10},{10,12},{12... | collective-permute-start | bytes 1179656 | tf_op jit(solution)/shard_map/ppermute | solution.py:24
  120.6 20.3 %collective-permute-start.3 = (bf16[768,256]{1,0:T(8,128)(2,1)}, bf16[768,256]{1,0:T(8,128)(2,1)}, u32[]{:S(2)}, u32[]{:S(2)}) collective-permute-start(bf16[768,256]{1,0:T(8,128)(2,1)} %finish.1.refs_0_), channel_id=1, source_target_pairs={{0,6},{2,0},{4,2},{6,4},{1,7},{3,1},{5,3},{7,5},{8,14},{10,8},{12,... | collective-permute-start | bytes 1179656 | tf_op jit(solution)/shard_map/ppermute | solution.py:24
  122.7 18.3 %collective-permute-start.6 = (bf16[768,256]{1,0:T(8,128)(2,1)}, bf16[768,256]{1,0:T(8,128)(2,1)}, u32[]{:S(2)}, u32[]{:S(2)}) collective-permute-start(bf16[768,256]{1,0:T(8,128)(2,1)} %finish.1.refs_0_), channel_id=1, source_target_pairs={{0,1},{1,0},{2,3},{3,2},{4,5},{5,4},{6,7},{7,6},{8,9},{9,8},{10,11... | collective-permute-start | bytes 1179656 | tf_op jit(solution)/shard_map/ppermute | solution.py:24
  127.6 15.6 %copy-start.3 = (bf16[768,256]{1,0:T(8,128)(2,1)}, bf16[768,256]{1,0:T(8,128)(2,1)S(1)}, u32[]{:S(2)}) copy-start(bf16[768,256]{1,0:T(8,128)(2,1)S(1)} %collective-permute-done.5.refs_3_) | copy-start | bytes 1179652
  127.6 13.4 %collective-permute-start.9 = (bf16[768,256]{1,0:T(8,128)(2,1)S(1)}, bf16[768,256]{1,0:T(8,128)(2,1)}, u32[]{:S(2)}, u32[]{:S(2)}) collective-permute-start(bf16[768,256]{1,0:T(8,128)(2,1)S(1)} %collective-permute-done.5.refs_3_), channel_id=1, source_target_pairs={{0,1},{1,0},{2,3},{3,2},{4,5},{5,4},{6,7},{7,6},{8,9},{9,8},{10,11... | collective-permute-start | bytes 1179656 | tf_op jit(solution)/shard_map/ppermute | solution.py:24
  140.0 2.6 %collective-permute-start.8 = (bf16[768,256]{1,0:T(8,128)(2,1)}, bf16[768,256]{1,0:T(8,128)(2,1)}, u32[]{:S(2)}, u32[]{:S(2)}) collective-permute-start(bf16[768,256]{1,0:T(8,128)(2,1)} %collective-permute-done.4.refs_2_), channel_id=1, source_target_pairs={{0,1},{1,0},{2,3},{3,2},{4,5},{5,4},{6,7},{7,6},{8,9},{9,8},{10,11... | collective-permute-start | bytes 1179656 | tf_op jit(solution)/shard_map/ppermute | solution.py:24
  140.9 2.3 %collective-permute-start.7 = (bf16[768,256]{1,0:T(8,128)(2,1)}, bf16[768,256]{1,0:T(8,128)(2,1)}, u32[]{:S(2)}, u32[]{:S(2)}) collective-permute-start(bf16[768,256]{1,0:T(8,128)(2,1)} %collective-permute-done.3.refs_1_), channel_id=1, source_target_pairs={{0,1},{1,0},{2,3},{3,2},{4,5},{5,4},{6,7},{7,6},{8,9},{9,8},{10,11... | collective-permute-start | bytes 1179656 | tf_op jit(solution)/shard_map/ppermute | solution.py:24

commit v3 on v2

--- a/solution.py
+++ b/solution.py
@@ -56,7 +56,7 @@
     return ahead, behind
 
 
-def condense_body(where, cond, ctx_cond, shift, scale, gate, out, wide):
+def condense_body(where, cond, ctx_cond, shift, scale, gate, out, wide, turned):
     rows = shift.shape[0] // LANES
     acts = []
     for c, ref in enumerate((cond, ctx_cond)):
@@ -66,32 +66,35 @@
         acts.append(jnp.concatenate(picked, axis=1))
     row = lax.broadcasted_iota(jnp.int32, (8, shift.shape[0]), 0)
     acts = jnp.where(row == 0, acts[0], jnp.where(row == 1, acts[1], 0.0)).astype(BF16)
-    parts = jnp.concatenate(
-        [
-            jnp.dot(acts, shift[...], preferred_element_type=F32)[:2, :],
-            jnp.dot(acts, scale[...], preferred_element_type=F32)[:2, :],
-            jnp.dot(acts, gate[...], preferred_element_type=F32)[:1, :],
-        ],
-        axis=0,
-    )
+    at = 0
+    for weight, n in ((shift, 2), (scale, 2), (gate, 1)):
+        part = jnp.dot(acts, weight[...], preferred_element_type=F32)
+        for r in range(n):
+            for t in range(part.shape[1] // LANES):
+                turned[at : at + 1, :] = part[r : r + 1, t * LANES : (t + 1) * LANES]
+                at += 1
+    sent = turned[: out.shape[1], :].astype(BF16)
     for i in range(out.shape[0]):
-        out[i] = parts
+        out[i] = sent
 
 
 def fold_body(got, out, gate):
-    total = got[0]
+    total = got[0].astype(F32)
     for i in range(1, got.shape[0]):
-        total = total + got[i]
+        total = total + got[i].astype(F32)
+    n = out.shape[1]
     for i in range(out.shape[0]):
-        out[i] = total[: out.shape[1], :]
-    gate[...] = total[out.shape[1] :, :]
+        out[i] = total[:n, :]
+    gate[...] = jnp.concatenate(
+        [total[r : r + 1, :] for r in range(n, n + gate.shape[1] // LANES)], axis=1
+    )
 
 
 def project_body(
     flags, own, oth, ctx, same, crossed, gain, vectors, w_gate, w_sig, w_wri, w_rea,
-    w_step, taps, bias, dlog, extra,
+    w_step, sig_taps, wri_taps, rea_taps, bias, rates, extra,
     gate_out, sig_out, wri_out, rea_out, rows_out, cols_out, payload,
-    acc, squares, pad, cpad, stpad, *hiddens,
+    acc, acc_step, squares, pad, cpad, stpad, small, *hiddens,
     heads,
 ):
     k = pl.program_id(0)
@@ -110,6 +113,7 @@
     @pl.when(k == 0)
     def _():
         acc[...] = jnp.zeros_like(acc)
+        acc_step[...] = jnp.zeros_like(acc_step)
         squares[...] = jnp.zeros_like(squares)
 
     def take(hidden, values, scale, at):
@@ -123,9 +127,19 @@
 
     for c, hidden in enumerate(hiddens):
         cut = slice(c * wide, (c + 1) * wide)
-        w = jnp.concatenate([r[cut, :] for r in (w_gate, w_sig, w_wri, w_rea, w_step)], axis=1)
-        g0, b0 = gain[:, cut] * (1.0 + vectors[c, 2:3, :]), vectors[c, 0:1, :]
-        g1, b1 = gain[:, cut] * (1.0 + vectors[c, 3:4, :]), vectors[c, 1:2, :]
+        w = jnp.concatenate([r[cut, :] for r in (w_gate, w_sig, w_wri, w_rea)], axis=1)
+        for direction in range(2):
+            small[direction * heads : (direction + 1) * heads, :] = w_step[
+                direction, :, cut
+            ].astype(F32)
+        per = wide // LANES
+        b0, b1, g0, g1 = (
+            jnp.concatenate(
+                [vectors[c, r * per + t : r * per + t + 1, :] for t in range(per)], axis=1
+            )
+            for r in range(4)
+        )
+        g0, g1 = gain[:, cut] * (1.0 + g0), gain[:, cut] * (1.0 + g1)
         edges = [same[:, cut].astype(F32), crossed[:, cut].astype(F32)]
         edges_before = jnp.where(first, edges[1], edges[0])
         edges_after = jnp.where(first, edges[0], edges[1])
@@ -145,6 +159,10 @@
         take(hidden, own[:, cut].astype(F32), g0, 0)
         take(hidden, oth[:, cut].astype(F32), g0, half)
         acc[...] += jnp.dot(hidden[...], w, preferred_element_type=F32)
+        acc_step[...] += lax.dot_general(
+            hidden[...], small[...].astype(BF16), (((1,), (1,)), ((), ())),
+            preferred_element_type=F32,
+        )
 
     @pl.when(k == pl.num_programs(0) - 1)
     def _():
@@ -153,28 +171,29 @@
         prev_ok = jnp.where(flags[1] > 0, 0.0, 1.0)
         next_ok = jnp.where(flags[2] > 0, 0.0, 1.0)
         base = length + ctx_len + EDGES
-        lat_add = acc[base : base + 1, :] + acc[base + 1 : base + 2, :]
-        ctx_add = acc[base + 2 : base + 3, :] + acc[base + 3 : base + 4, :]
         scale = lax.rsqrt(
             jnp.sum(squares[...], axis=1, keepdims=True) * (1.0 / d_model) + EPSILON
         )
 
-        def values(lo, n, cols, add):
-            return rounded(acc[lo : lo + n, cols] * scale[lo : lo + n, :] + add[:, cols])
-
-        conv_cols, step_cols = slice(c0, c1), slice(c1, c1 + 2 * heads)
+        def values(lo, n, cols, is_ctx=0, source=acc):
+            at = base + 2 * is_ctx
+            add = source[at : at + 1, cols] + source[at + 1 : at + 2, cols]
+            return rounded(source[lo : lo + n, cols] * scale[lo : lo + n, :] + add)
+
+        conv_cols, step_cols = slice(c0, c1), slice(0, 2 * heads)
         for lo, off in ((0, dp * half), (half, (1 - dp) * half)):
             off = pl.multiple_of(off, half)
-            gate_out[pl.ds(off, half), :] = values(lo, half, slice(0, c0), lat_add).astype(BF16)
-            pad[pl.ds(off + 8, half), :] = values(lo, half, conv_cols, lat_add)
-            stpad[pl.ds(off, half), : 2 * heads] = values(lo, half, step_cols, lat_add)
-        base = length + ctx_len
-        pad[7:8, :] = values(base + 2, 1, conv_cols, lat_add) * prev_ok
-        pad[8 + length : 9 + length, :] = values(base + 3, 1, conv_cols, lat_add) * next_ok
-        cpad[8 : 8 + ctx_len, :] = values(length, ctx_len, conv_cols, ctx_add)
-        cpad[7:8, :] = values(base, 1, conv_cols, ctx_add) * prev_ok
-        cpad[8 + ctx_len : 9 + ctx_len, :] = values(base + 1, 1, conv_cols, ctx_add) * next_ok
-        stpad[length : length + ctx_len, : 2 * heads] = values(length, ctx_len, step_cols, ctx_add)
+            gate_out[pl.ds(off, half), :] = values(lo, half, slice(0, c0)).astype(BF16)
+            pad[pl.ds(off + 8, half), :] = values(lo, half, conv_cols)
+            stpad[pl.ds(off, half), : 2 * heads] = values(lo, half, step_cols, 0, acc_step)
+        edge = length + ctx_len
+        pad[7:8, :] = values(edge + 2, 1, conv_cols) * prev_ok
+        pad[8 + length : 9 + length, :] = values(edge + 3, 1, conv_cols) * next_ok
+        cpad[8 : 8 + ctx_len, :] = values(length, ctx_len, conv_cols, 1)
+        cpad[7:8, :] = values(edge, 1, conv_cols, 1) * prev_ok
+        cpad[8 + ctx_len : 9 + ctx_len, :] = values(edge + 1, 1, conv_cols, 1) * next_ok
+        stpad[length : length + ctx_len, : 2 * heads] = values(length, ctx_len, step_cols, 1, acc_step)
+        taps = jnp.concatenate([sig_taps[...], wri_taps[...], rea_taps[...]], axis=1)
         t0, t1, t2 = taps[0:1, :], taps[1:2, :], taps[2:3, :]
         conv = silu(
             t0 * pad[7 : 7 + length, :] + t1 * pad[8 : 8 + length, :] + t2 * pad[9 : 9 + length, :]
@@ -192,15 +211,25 @@
         sig_out[...] = sig.astype(BF16)
         wri_out[...] = wri
         rea_out[...] = rea
+        blank = jnp.zeros((LANES - ctx_len, conv_w), F32)
+        cconv = jnp.concatenate([cconv, blank], axis=0)
         csig, cwri = cconv[:, :n_sig], cconv[:, n_sig : n_sig + n_state].astype(BF16)
 
         both = 2 * heads
         turned = stpad[...].T[:both, :]
         lane = lax.broadcasted_iota(jnp.int32, turned.shape, 1)
-        z = jnp.where(lane < length + ctx_len, turned, 0.0) + bias[...]
+        which = lax.broadcasted_iota(jnp.int32, (both, 1), 0)
+        shift, rate = jnp.zeros((both, 1), F32), jnp.zeros((both, 1), F32)
+        for r in range(both):
+            d, h = divmod(r, heads)
+            shift = jnp.where(which == r, bias[d : d + 1, h : h + 1], shift)
+            rate = jnp.where(which == r, rates[d : d + 1, h : h + 1], rate)
+        z = jnp.where(lane < length + ctx_len, turned, 0.0) + shift
         step = jnp.maximum(z, 0.0) + jnp.log1p(jnp.exp(-jnp.abs(z)))
-        more = jnp.concatenate([extra[...], jnp.zeros((both, LANES), F32)], axis=1)
-        logs = -jnp.exp(dlog[...]) * step + more
+        for direction in range(2):
+            rows_out[direction * heads : (direction + 1) * heads, :] = extra[direction]
+        more = jnp.concatenate([rows_out[:both, :], jnp.zeros((both, LANES), F32)], axis=1)
+        logs = -jnp.exp(rate) * step + more
         logs = jnp.where(lane < length + ctx_len, logs, 0.0)
         lat_step, lat_log = step[:, :length], logs[:, :length]
         ctx_step, ctx_log = step[:, length:], logs[:, length:]
@@ -214,20 +243,22 @@
         ctx_w = jnp.exp(jnp.where(forward, c_total - c_ahead, c_ahead - ctx_log)) * ctx_step
         rows_out[:both, :] = cum
         rows_out[both:, :] = lat_step
-        cols = jnp.concatenate([cum, lat_w, jnp.zeros((LANES - 2 * both, length), F32)], axis=0).T
-        ctx_cols = jnp.concatenate([ctx_w, jnp.zeros((LANES - both, LANES), F32)], axis=0).T
-        cols_out[...] = cols
-        contract = (((0,), (0,)), ((), ()))
-        for direction in range(2):
-            lhs = (sig * per_head(cols, both + direction * heads, heads, width)).astype(BF16)
-            state = lax.dot_general(lhs, wri, contract, preferred_element_type=F32)
-            part = n_sig // payload.shape[0]
-            kind = direction * part
-            payload[:, kind : kind + part, :] = state.reshape(-1, part, n_state).astype(BF16)
-            lhs = csig * per_head(ctx_cols[:ctx_len, :], direction * heads, heads, width)
-            state = lax.dot_general(lhs.astype(BF16), cwri, contract, preferred_element_type=F32)
-            kind = (2 + direction) * part
-            payload[:, kind : kind + part, :] = state.reshape(-1, part, n_state).astype(BF16)
+        cols_out[...] = jnp.concatenate([cum, jnp.zeros((LANES - both, length), F32)], axis=0).T
+        part = n_sig // payload.shape[0]
+        kind = 0
+        for values_t, weights, other in ((sig.T, lat_w, wri), (csig.T, ctx_w, cwri)):
+            for direction in range(2):
+                lhs = jnp.concatenate(
+                    [
+                        values_t[h * width : (h + 1) * width, :]
+                        * weights[direction * heads + h : direction * heads + h + 1, :]
+                        for h in range(heads)
+                    ],
+                    axis=0,
+                ).astype(BF16)
+                state = jnp.dot(lhs, other, preferred_element_type=F32)
+                payload[:, kind : kind + part, :] = state.reshape(-1, part, n_state).astype(BF16)
+                kind += part
         tail = payload.shape[1] - KINDS * part
         row = lax.broadcasted_iota(jnp.int32, (tail, LANES), 0)
         pieces = []
@@ -392,13 +423,16 @@
     small = lambda n: pltpu.CompilerParams(vmem_limit_bytes=n * MIB)
     parts = pl.pallas_call(
         condense_body,
-        out_shape=shaped((n_sp, 5, cols_here), F32),
+        out_shape=shaped((n_sp, 5 * cols_here // LANES, LANES), BF16),
         grid_spec=pltpu.PrefetchScalarGridSpec(
             num_scalar_prefetch=1,
             grid=(1,),
             in_specs=[whole((d_model // LANES, LANES))] * 2 + [whole(shift_weight.shape)] * 3,
-            out_specs=whole((n_sp, 5, cols_here)),
-            scratch_shapes=[pltpu.VMEM((2 * d_model // LANES, LANES), F32)],
+            out_specs=whole((n_sp, 5 * cols_here // LANES, LANES)),
+            scratch_shapes=[
+                pltpu.VMEM((2 * d_model // LANES, LANES), F32),
+                pltpu.VMEM((8 * cols_here // LANES, LANES), F32),
+            ],
         ),
         compiler_params=small(8),
         name="condense",
@@ -409,17 +443,10 @@
     )
     latent, context, sent = lax.optimization_barrier((latent, context, parts))
     sums = lax.all_to_all(sent, "sp", split_axis=0, concat_axis=0, tiled=True)
-    taps = jnp.concatenate([signal_taps, writer_taps, reader_taps], axis=1)
-    steps = jnp.moveaxis(step_weight, 0, 1).reshape(d_model, 2 * heads)
-    extra = decay_extra.reshape(2 * heads, length)
-    bias, rates = step_bias.reshape(-1, 1), decay_log.reshape(-1, 1)
-    sums, taps, steps, extra, bias, rates = lax.optimization_barrier(
-        (sums, taps, steps, extra, bias, rates)
-    )
     vectors, gate_vec = pl.pallas_call(
         fold_body,
         out_shape=(
-            shaped((n_tp * n_dp, 4, cols_here), F32),
+            shaped((n_tp * n_dp, 4 * cols_here // LANES, LANES), F32),
             shaped((1, cols_here), F32),
         ),
         compiler_params=pltpu.CompilerParams(vmem_limit_bytes=8 * MIB),
@@ -444,7 +471,7 @@
     crossed = lax.ppermute(edge, ("sp", "dp"), pairs[1])
 
     flags = jnp.stack([dp, sp == 0, sp == n_sp - 1]).astype(jnp.int32)
-    n_all = n_gate + n_sig + 2 * n_state + 2 * heads
+    n_all = n_gate + n_sig + 2 * n_state
     n_rows = length + ctx_len + 2 * EDGES
     part = n_sig // n_sp
     tail = KINDS * PIECES
@@ -470,18 +497,21 @@
             in_specs=[
                 tile(half), tile(half), tile(ctx_len), tile(2), tile(2),
                 tile(1),
-                pl.BlockSpec((CHUNKS, 4, cols_here), lambda k, *_: (k, 0, 0)),
-                down(n_gate), down(n_sig), down(n_state), down(n_state), down(2 * heads),
-                whole((3, conv_w)), whole((2 * heads, 1)), whole((2 * heads, 1)),
-                whole((2 * heads, length)),
+                pl.BlockSpec((CHUNKS, 4 * cols_here // LANES, LANES), lambda k, *_: (k, 0, 0)),
+                down(n_gate), down(n_sig), down(n_state), down(n_state),
+                pl.BlockSpec((2, heads, k_tile), lambda k, *_: (0, 0, k)),
+                whole(signal_taps.shape), whole(writer_taps.shape), whole(reader_taps.shape),
+                whole(step_bias.shape), whole(decay_log.shape), whole(decay_extra.shape),
             ],
             out_specs=[whole(o.shape) for o in outs],
             scratch_shapes=[
                 pltpu.VMEM((n_rows, n_all), F32),
+                pltpu.VMEM((n_rows, 2 * heads), F32),
                 pltpu.VMEM((n_rows, LANES), F32),
                 pltpu.VMEM((length + 16, conv_w), F32),
                 pltpu.VMEM((ctx_len + 16, conv_w), F32),
                 pltpu.VMEM((length + LANES, LANES), F32),
+                pltpu.VMEM((2 * heads, cols_here), F32),
             ]
             + [pltpu.VMEM((n_rows, cols_here), BF16)] * CHUNKS,
         ),
@@ -494,9 +524,10 @@
         ),
         name="project",
     )(
-        flags, *placed(latent), oth, *placed(context), same, crossed, norm_gain.reshape(1, -1), vectors,
-        *placed(out_gate_weight, signal_weight, writer_weight, reader_matrix, steps),
-        taps, bias, rates, extra,
+        flags, *placed(latent), oth, *placed(context), same, crossed, *placed(norm_gain.reshape(1, -1)), vectors,
+        *placed(out_gate_weight, signal_weight, writer_weight, reader_matrix),
+        *placed(jnp.swapaxes(step_weight, 1, 2)), *placed(signal_taps, writer_taps, reader_taps),
+        *placed(step_bias, decay_log, decay_extra),
     )
 
     got = lax.all_to_all(payload, "sp", split_axis=0, concat_axis=0, tiled=True)

time: 150 us -> 142 us (0.947)
  local copies, waits for them, and re-layouts: 8.12 us -> 1.09 us
  waiting for transfers between devices: 14.2 us -> 20.4 us
  starting transfers between devices: 65.7 us -> 60.5 us
    all_to_all x1, starting transfers between devices: 11.3 us -> 6.2 us  [on_device(): lax.all_to_all(vectors, ('tp', 'dp'), split_axis=0, concat_axis=0, tiled=...]
    reshape x4 -> x0, local copies, waits for them, and re-layouts: 4.24 us -> none  [the longest x2 2.63 us: on_device(): bias, rates = (step_bias.reshape(-1, 1), decay_log.reshape(-1, 1))]
    all_to_all x1, waiting for transfers between devices: 0.83 us -> 4.06 us  [on_device(): sums = lax.all_to_all(sent, 'sp', split_axis=0, concat_axis=0, tiled=True)]
    all_to_all x1, waiting for transfers between devices: 1.98 us -> 4.77 us  [on_device(): lax.all_to_all(vectors, ('tp', 'dp'), split_axis=0, concat_axis=0, tiled=...]
    optimization_barrier x3 -> x0, local copies, waits for them, and re-layouts: 2.78 us -> none  [on_device(): lax.optimization_barrier((sums, taps, steps, extra, bias, rates))]
  transfers between devices with their start and end apart: 13 -> 13, of which waited for: 7 -> 7; matrix products, arithmetic and copies ran while one was open for 6% -> 1% of each run, Pallas kernels for 6% -> 6%
where the time goes in v3:
time: 142 us; the launch traced here: 141 us
  starting transfers between devices  60.5 us (43%)
  Pallas kernels  35.3 us (25%)
  blocking collectives  23.3 us (16%)
  waiting for transfers between devices  20.4 us (14%)
    ppermute x8, starting transfers between devices, shifted(): return lax.ppermute(x, axis, [(i, (i + by) % n) for i in range(n)])  38.3 us
    all_to_all x1, blocking collectives, on_device(): lax.all_to_all(starts, 'sp', split_axis=0, concat_axis=0, tiled=True)  23.3 us
    pallas_call x1, Pallas kernels, on_device(): pl.pallas_call(functools.partial(project_body, heads=heads), out_shape=ou...  14.4 us
    pallas_call x1, Pallas kernels, on_device(): pl.pallas_call(functools.partial(inside_body, heads=heads), out_shape=sha...  8.32 us
    all_to_all x1, starting transfers between devices, on_device(): lax.all_to_all(vectors, ('tp', 'dp'), split_axis=0, concat_axis=0, tiled=...  6.2 us
    ppermute x8, waiting for transfers between devices, shifted(): return lax.ppermute(x, axis, [(i, (i + by) % n) for i in range(n)])  6.01 us
    pallas_call x1, Pallas kernels, on_device(): pl.pallas_call(functools.partial(output_body, count=count), out_shape=sha...  5.68 us
    all_to_all x1, waiting for transfers between devices, on_device(): got = lax.all_to_all(payload, 'sp', split_axis=0, concat_axis=0, tiled=True)  5.59 us
  transfers between devices with their start and end apart: 13, of which 7 were waited for; matrix products, arithmetic and copies ran while one was open for 1% of the time, Pallas kernels for 6%

profile of v3, /device:TPU:33, one launch (start us, length us, event | category | flops | bytes accessed | tf_op | source)
XLA Modules:
  0.0 141.0 jit_solution(9719362409803878101)
XLA Ops:
  0.0 2.0 %condense.1 = bf16[16,20,128]{2,1,0:T(8,128)(2,1)} custom-call(s32[1]{0:T(128)} %bitcast.11.where, bf16[32,128]{1,0:T(8,128)(2,1)} %bitcast.18, bf16[32,128]{1,0:T(8,128)(2,1)} %bitcast.19, bf16[256,512]{1,0:T(8,128)(2,1)} %shift.1, bf16[256,512]{1,0:T(8,128)(2,1)} %scale.1, bf16[256,512]{1,0:T(8,128)(2,1)} %gate.1), custom_call_target="tpu_custom_call" | custom-call | tf_op jit(solution)/shard_map/condense/pallas_call | solution.py:424
  2.0 20.4 %collective-permute-start = (bf16[384,4096]{1,0:T(8,128)(2,1)}, bf16[384,4096]{1,0:T(8,128)(2,1)S(1)}, u32[]{:S(2)}, u32[]{:S(2)}) collective-permute-start(bf16[384,4096]{1,0:T(8,128)(2,1)} %refs_9_), channel_id=1, source_target_pairs={{0,1},{1,0},{2,3},{3,2},{4,5},{5,4},{6,7},{7,6},{8,9},{9,8},{10,11... | collective-permute-start | bytes 9437192 | tf_op jit(solution)/shard_map/ppermute | solution.py:24
  22.4 4.7 %all-to-all-start = ((bf16[16,20,128]{2,1,0:T(8,128)(2,1)}), bf16[16,20,128]{2,1,0:T(8,128)(2,1)S(1)}, u32[]{:S(2)}, u32[]{:S(2)}) async-start(bf16[16,20,128]{2,1,0:T(8,128)(2,1)} %condense.1), calls=%async_computation | async-start | bytes 196608 | tf_op jit(solution)/shard_map/all_to_all | solution.py:445
  27.2 1.0 fusion
  28.1 0.1 broadcast_select_fusion
  28.2 3.5 %collective-permute-start.2 = (bf16[2,4096]{1,0:T(2,128)(2,1)S(1)}, bf16[2,4096]{1,0:T(2,128)(2,1)S(1)}, u32[]{:S(2)}, u32[]{:S(2)}) collective-permute-start(bf16[2,4096]{1,0:T(2,128)(2,1)S(1)} %broadcast_select_fusion), channel_id=1, source_target_pairs={{1,8},{9,16},{8,1},{17,24},{16,9},{25,32},{24,17},{33,40},{32,25},... | collective-permute-start | bytes 49160 | tf_op jit(solution)/shard_map/ppermute | solution.py:471
  31.8 3.1 %collective-permute-start.1 = (bf16[2,4096]{1,0:T(2,128)(2,1)S(1)}, bf16[2,4096]{1,0:T(2,128)(2,1)S(1)}, u32[]{:S(2)}, u32[]{:S(2)}) collective-permute-start(bf16[2,4096]{1,0:T(2,128)(2,1)S(1)} %broadcast_select_fusion), channel_id=1, source_target_pairs={{1,9},{9,17},{8,0},{17,25},{16,8},{25,33},{24,16},{33,41},{32,24},... | collective-permute-start | bytes 49160 | tf_op jit(solution)/shard_map/ppermute | solution.py:470
  34.9 4.1 %all-to-all-done.got = bf16[16,20,128]{2,1,0:T(8,128)(2,1)S(1)} async-done(((bf16[16,20,128]{2,1,0:T(8,128)(2,1)}), bf16[16,20,128]{2,1,0:T(8,128)(2,1)S(1)}, u32[]{:S(2)}, u32[]{:S(2)}) %all-to-all-start) | async-done | bytes 81952 | tf_op jit(solution)/shard_map/all_to_all | solution.py:445
  39.0 0.7 fold.1
  39.6 6.2 %all-to-all-start.1 = ((f32[8,16,128]{2,1,0:T(8,128)}), f32[8,16,128]{2,1,0:T(8,128)S(1)}, u32[]{:S(2)}, u32[]{:S(2)}) async-start(f32[8,16,128]{2,1,0:T(8,128)} %get-tuple-element.22), calls=%async_computation.1 | async-start | bytes 131072 | tf_op jit(solution)/shard_map/all_to_all | solution.py:455
  45.8 0.1 pad_add_fusion.flags
  45.9 0.0 collective-permute-done.2.crossed
  45.9 0.0 collective-permute-done.1.same
  45.9 4.8 %all-to-all-done.1.vectors = f32[8,16,128]{2,1,0:T(8,128)S(1)} async-done(((f32[8,16,128]{2,1,0:T(8,128)}), f32[8,16,128]{2,1,0:T(8,128)S(1)}, u32[]{:S(2)}, u32[]{:S(2)}) %all-to-all-start.1) | async-done | bytes 65568 | tf_op jit(solution)/shard_map/all_to_all | solution.py:455
  50.7 0.0 collective-permute-done.oth.refs_10_
  50.7 14.4 %project.1 = (bf16[768,256]{1,0:T(8,128)(2,1)}, bf16[768,256]{1,0:T(8,128)(2,1)}, bf16[768,128]{1,0:T(8,128)(2,1)}, bf16[768,128]{1,0:T(8,128)(2,1)}, f32[16,768...) custom-call(s32[3]{0:T(128)S(1)} %pad_add_fusion.flags, bf16[384,4096]{1,0:T(8,128)(2,1)} %refs_9_, ...), custom_call_target="tpu_custom_call" | custom-call | flops 5234491392 | bytes 13107200 | tf_op jit(solution)/shard_map/project/pallas_call | solution.py:491
  65.1 0.0 copy-start.1
  65.1 4.6 %all-to-all-start.2 = ((bf16[16,72,128]{2,1,0:T(8,128)(2,1)}), bf16[16,72,128]{2,1,0:T(8,128)(2,1)S(1)}, u32[]{:S(2)}, u32[]{:S(2)}) async-start(bf16[16,72,128]{2,1,0:T(8,128)(2,1)} %get-tuple-element.23), calls=%async_computation.2 | async-start | bytes 589824 | tf_op jit(solution)/shard_map/all_to_all | solution.py:533
  69.7 0.0 copy-start
  69.7 8.3 %inside.1 = f32[768,256]{1,0:T(8,128)} custom-call(bf16[768,128]{1,0:T(8,128)(2,1)} %get-tuple-element.24.rea, bf16[768,128]{1,0:T(8,128)(2,1)} %get-tuple-element.25.wri, bf16[768,256]{1,0:T(8,128)(2,1)} %get-tuple-element.26.sig, f32[16,768]{1,0:T(8,128)} %get-tuple-element.27.rows, f32[768,128]{1,0:T(8,128)} %get-tuple-element.28.cols), custom_call_target="tpu_custom_call" | custom-call | flops 1358954496 | bytes 786432 | tf_op jit(solution)/shard_map/inside/pallas_call | solution.py:535
  78.0 5.6 %all-to-all-done.2.got = bf16[16,72,128]{2,1,0:T(8,128)(2,1)S(1)} async-done(((bf16[16,72,128]{2,1,0:T(8,128)(2,1)}), bf16[16,72,128]{2,1,0:T(8,128)(2,1)S(1)}, u32[]{:S(2)}, u32[]{:S(2)}) %all-to-all-start.2) | async-done | bytes 294944 | tf_op jit(solution)/shard_map/all_to_all | solution.py:533
  83.6 0.8 chain.1
  84.4 23.3 %all_to_all.20.starts = bf16[16,32,128]{2,1,0:T(8,128)(2,1)S(1)} all-to-all(bf16[16,32,128]{2,1,0:T(8,128)(2,1)} %chain.1), channel_id=1, replica_groups=mesh['grp'=2,'sp'=16,'tp'=4,'dp'=2] {'sp'}, dimensions={0} | all-to-all | bytes 262144 | tf_op jit(solution)/shard_map/all_to_all | solution.py:559
  107.7 0.0 copy-done.1
  107.7 3.4 %finish.1.refs_0_ = bf16[768,256]{1,0:T(8,128)(2,1)} custom-call(bf16[16,32,128]{2,1,0:T(8,128)(2,1)S(1)} %all_to_all.20.starts, bf16[768,128]{1,0:T(8,128)(2,1)} %get-tuple-element.24.rea, f32[768,128]{1,0:T(8,128)} %get-tuple-element.28.cols, f32[768,256]{1,0:T(8,128)} %inside.1, bf16[768,256]{1,0:T(8,128)(2,1)} %get-tuple-element.31.gate, ...), custom_call_target="tpu_custom_call" | custom-call | tf_op jit(solution)/shard_map/finish/pallas_call | solution.py:560
  111.1 0.7 collective-permute-start.5
  111.8 0.7 collective-permute-start.4
  112.6 1.9 %collective-permute-start.3 = (bf16[768,256]{1,0:T(8,128)(2,1)}, bf16[768,256]{1,0:T(8,128)(2,1)}, u32[]{:S(2)}, u32[]{:S(2)}) collective-permute-start(bf16[768,256]{1,0:T(8,128)(2,1)} %finish.1.refs_0_), channel_id=1, source_target_pairs={{0,6},{2,0},{4,2},{6,4},{1,7},{3,1},{5,3},{7,5},{8,14},{10,8},{12,... | collective-permute-start | bytes 1179656 | tf_op jit(solution)/shard_map/ppermute | solution.py:24
  114.5 4.6 %collective-permute-start.6 = (bf16[768,256]{1,0:T(8,128)(2,1)}, bf16[768,256]{1,0:T(8,128)(2,1)}, u32[]{:S(2)}, u32[]{:S(2)}) collective-permute-start(bf16[768,256]{1,0:T(8,128)(2,1)} %finish.1.refs_0_), channel_id=1, source_target_pairs={{0,1},{1,0},{2,3},{3,2},{4,5},{5,4},{6,7},{7,6},{8,9},{9,8},{10,11... | collective-permute-start | bytes 1179656 | tf_op jit(solution)/shard_map/ppermute | solution.py:24
  119.2 0.4 collective-permute-done.5.refs_3_
  119.5 0.0 copy-start.2
  119.5 9.1 %collective-permute-start.9 = (bf16[768,256]{1,0:T(8,128)(2,1)S(1)}, bf16[768,256]{1,0:T(8,128)(2,1)}, u32[]{:S(2)}, u32[]{:S(2)}) collective-permute-start(bf16[768,256]{1,0:T(8,128)(2,1)S(1)} %collective-permute-done.5.refs_3_), channel_id=1, source_target_pairs={{0,1},{1,0},{2,3},{3,2},{4,5},{5,4},{6,7},{7,6},{8,9},{9,8},{10,11... | collective-permute-start | bytes 1179656 | tf_op jit(solution)/shard_map/ppermute | solution.py:24
  128.6 3.5 %collective-permute-done.4.refs_2_ = bf16[768,256]{1,0:T(8,128)(2,1)} collective-permute-done((bf16[768,256]{1,0:T(8,128)(2,1)}, bf16[768,256]{1,0:T(8,128)(2,1)}, u32[]{:S(2)}, u32[]{:S(2)}) %collective-permute-start.4) | collective-permute-done | bytes 393248 | tf_op jit(solution)/shard_map/ppermute | solution.py:24
  132.1 0.8 collective-permute-start.8
  132.9 0.0 collective-permute-done.3.refs_1_
  132.9 0.0 collective-permute-start.7
  132.9 0.1 stack.56.where
  133.0 0.0 collective-permute-done.6.refs_4_
  133.0 0.0 collective-permute-done.9.refs_7_
  133.0 1.6 %collective-permute-done.8.refs_6_ = bf16[768,256]{1,0:T(8,128)(2,1)} collective-permute-done((bf16[768,256]{1,0:T(8,128)(2,1)}, bf16[768,256]{1,0:T(8,128)(2,1)}, u32[]{:S(2)}, u32[]{:S(2)}) %collective-permute-start.8) | collective-permute-done | bytes 393248 | tf_op jit(solution)/shard_map/ppermute | solution.py:24
  134.6 0.6 collective-permute-done.7.refs_5_
  135.1 0.0 copy-done.2
  135.1 0.0 copy-done
  135.1 5.7 %output.1 = bf16[768,512]{1,0:T(8,128)(2,1)} custom-call(s32[10]{0:T(128)S(1)} %stack.56.where, bf16[768,256]{1,0:T(8,128)(2,1)} %finish.1.refs_0_, bf16[768,256]{1,0:T(8,128)(2,1)} %collective-permute-done.3.refs_1_, bf16[768,256]{1,0:T(8,128)(2,1)} %collective-permute-done.4.refs_2_, bf16[768,256]{1,0:T(8,128)(2,1)} %copy-done.2, ...), custom_call_target="tpu_custom_call" | custom-call | tf_op jit(solution)/shard_map/output/pallas_call | solution.py:577
Async XLA Ops:
  2.0 48.7 %collective-permute-start = (bf16[384,4096]{1,0:T(8,128)(2,1)}, bf16[384,4096]{1,0:T(8,128)(2,1)S(1)}, u32[]{:S(2)}, u32[]{:S(2)}) collective-permute-start(bf16[384,4096]{1,0:T(8,128)(2,1)} %refs_9_), channel_id=1, source_target_pairs={{0,1},{1,0},{2,3},{3,2},{4,5},{5,4},{6,7},{7,6},{8,9},{9,8},{10,11... | collective-permute-start | bytes 9437192 | tf_op jit(solution)/shard_map/ppermute | solution.py:24
  22.4 16.5 %all-to-all-start = ((bf16[16,20,128]{2,1,0:T(8,128)(2,1)}), bf16[16,20,128]{2,1,0:T(8,128)(2,1)S(1)}, u32[]{:S(2)}, u32[]{:S(2)}) async-start(bf16[16,20,128]{2,1,0:T(8,128)(2,1)} %condense.1), calls=%async_computation | async-start | bytes 196608 | tf_op jit(solution)/shard_map/all_to_all | solution.py:445
  28.2 17.7 %collective-permute-start.2 = (bf16[2,4096]{1,0:T(2,128)(2,1)S(1)}, bf16[2,4096]{1,0:T(2,128)(2,1)S(1)}, u32[]{:S(2)}, u32[]{:S(2)}) collective-permute-start(bf16[2,4096]{1,0:T(2,128)(2,1)S(1)} %broadcast_select_fusion), channel_id=1, source_target_pairs={{1,8},{9,16},{8,1},{17,24},{16,9},{25,32},{24,17},{33,40},{32,25},... | collective-permute-start | bytes 49160 | tf_op jit(solution)/shard_map/ppermute | solution.py:471
  31.8 14.1 %collective-permute-start.1 = (bf16[2,4096]{1,0:T(2,128)(2,1)S(1)}, bf16[2,4096]{1,0:T(2,128)(2,1)S(1)}, u32[]{:S(2)}, u32[]{:S(2)}) collective-permute-start(bf16[2,4096]{1,0:T(2,128)(2,1)S(1)} %broadcast_select_fusion), channel_id=1, source_target_pairs={{1,9},{9,17},{8,0},{17,25},{16,8},{25,33},{24,16},{33,41},{32,24},... | collective-permute-start | bytes 49160 | tf_op jit(solution)/shard_map/ppermute | solution.py:470
  39.6 11.1 %all-to-all-start.1 = ((f32[8,16,128]{2,1,0:T(8,128)}), f32[8,16,128]{2,1,0:T(8,128)S(1)}, u32[]{:S(2)}, u32[]{:S(2)}) async-start(f32[8,16,128]{2,1,0:T(8,128)} %get-tuple-element.22), calls=%async_computation.1 | async-start | bytes 131072 | tf_op jit(solution)/shard_map/all_to_all | solution.py:455
  65.1 42.6 %copy-start.1 = (f32[256]{0:T(256)S(1)}, f32[256]{0:T(256)}, u32[]{:S(2)}) copy-start(f32[256]{0:T(256)} %param.40) | copy-start | bytes 3076
  65.1 18.5 %all-to-all-start.2 = ((bf16[16,72,128]{2,1,0:T(8,128)(2,1)}), bf16[16,72,128]{2,1,0:T(8,128)(2,1)S(1)}, u32[]{:S(2)}, u32[]{:S(2)}) async-start(bf16[16,72,128]{2,1,0:T(8,128)(2,1)} %get-tuple-element.23), calls=%async_computation.2 | async-start | bytes 589824 | tf_op jit(solution)/shard_map/all_to_all | solution.py:533
  69.7 65.4 %copy-start = (f32[1,512]{1,0:T(1,128)S(1)}, f32[1,512]{1,0:T(1,128)}, u32[]{:S(2)}) copy-start(f32[1,512]{1,0:T(1,128)} %get-tuple-element.32.refs_11_) | copy-start | bytes 6148
  111.1 8.4 %collective-permute-start.5 = (bf16[768,256]{1,0:T(8,128)(2,1)}, bf16[768,256]{1,0:T(8,128)(2,1)S(1)}, u32[]{:S(2)}, u32[]{:S(2)}) collective-permute-start(bf16[768,256]{1,0:T(8,128)(2,1)} %finish.1.refs_0_), channel_id=1, source_target_pairs={{0,4},{2,6},{4,0},{6,2},{1,5},{3,7},{5,1},{7,3},{8,12},{10,14},{12... | collective-permute-start | bytes 1179656 | tf_op jit(solution)/shard_map/ppermute | solution.py:24
  111.8 20.2 %collective-permute-start.4 = (bf16[768,256]{1,0:T(8,128)(2,1)}, bf16[768,256]{1,0:T(8,128)(2,1)}, u32[]{:S(2)}, u32[]{:S(2)}) collective-permute-start(bf16[768,256]{1,0:T(8,128)(2,1)} %finish.1.refs_0_), channel_id=1, source_target_pairs={{0,2},{2,4},{4,6},{6,0},{1,3},{3,5},{5,7},{7,1},{8,10},{10,12},{12... | collective-permute-start | bytes 1179656 | tf_op jit(solution)/shard_map/ppermute | solution.py:24
  112.6 20.3 %collective-permute-start.3 = (bf16[768,256]{1,0:T(8,128)(2,1)}, bf16[768,256]{1,0:T(8,128)(2,1)}, u32[]{:S(2)}, u32[]{:S(2)}) collective-permute-start(bf16[768,256]{1,0:T(8,128)(2,1)} %finish.1.refs_0_), channel_id=1, source_target_pairs={{0,6},{2,0},{4,2},{6,4},{1,7},{3,1},{5,3},{7,5},{8,14},{10,8},{12,... | collective-permute-start | bytes 1179656 | tf_op jit(solution)/shard_map/ppermute | solution.py:24
  114.5 18.5 %collective-permute-start.6 = (bf16[768,256]{1,0:T(8,128)(2,1)}, bf16[768,256]{1,0:T(8,128)(2,1)}, u32[]{:S(2)}, u32[]{:S(2)}) collective-permute-start(bf16[768,256]{1,0:T(8,128)(2,1)} %finish.1.refs_0_), channel_id=1, source_target_pairs={{0,1},{1,0},{2,3},{3,2},{4,5},{5,4},{6,7},{7,6},{8,9},{9,8},{10,11... | collective-permute-start | bytes 1179656 | tf_op jit(solution)/shard_map/ppermute | solution.py:24
  119.5 15.6 %copy-start.2 = (bf16[768,256]{1,0:T(8,128)(2,1)}, bf16[768,256]{1,0:T(8,128)(2,1)S(1)}, u32[]{:S(2)}) copy-start(bf16[768,256]{1,0:T(8,128)(2,1)S(1)} %collective-permute-done.5.refs_3_) | copy-start | bytes 1179652
  119.5 13.4 %collective-permute-start.9 = (bf16[768,256]{1,0:T(8,128)(2,1)S(1)}, bf16[768,256]{1,0:T(8,128)(2,1)}, u32[]{:S(2)}, u32[]{:S(2)}) collective-permute-start(bf16[768,256]{1,0:T(8,128)(2,1)S(1)} %collective-permute-done.5.refs_3_), channel_id=1, source_target_pairs={{0,1},{1,0},{2,3},{3,2},{4,5},{5,4},{6,7},{7,6},{8,9},{9,8},{10,11... | collective-permute-start | bytes 1179656 | tf_op jit(solution)/shard_map/ppermute | solution.py:24
  132.1 2.5 %collective-permute-start.8 = (bf16[768,256]{1,0:T(8,128)(2,1)}, bf16[768,256]{1,0:T(8,128)(2,1)}, u32[]{:S(2)}, u32[]{:S(2)}) collective-permute-start(bf16[768,256]{1,0:T(8,128)(2,1)} %collective-permute-done.4.refs_2_), channel_id=1, source_target_pairs={{0,1},{1,0},{2,3},{3,2},{4,5},{5,4},{6,7},{7,6},{8,9},{9,8},{10,11... | collective-permute-start | bytes 1179656 | tf_op jit(solution)/shard_map/ppermute | solution.py:24
  132.9 2.3 %collective-permute-start.7 = (bf16[768,256]{1,0:T(8,128)(2,1)}, bf16[768,256]{1,0:T(8,128)(2,1)}, u32[]{:S(2)}, u32[]{:S(2)}) collective-permute-start(bf16[768,256]{1,0:T(8,128)(2,1)} %collective-permute-done.3.refs_1_), channel_id=1, source_target_pairs={{0,1},{1,0},{2,3},{3,2},{4,5},{5,4},{6,7},{7,6},{8,9},{9,8},{10,11... | collective-permute-start | bytes 1179656 | tf_op jit(solution)/shard_map/ppermute | solution.py:24

commit v4 on v3

--- a/solution.py
+++ b/solution.py
@@ -325,7 +325,7 @@
         )
 
 
-def finish_body(starts, rea, cols, inside, gate, gain, out, *, heads):
+def finish_body(starts, rea, cols, inside, gate, gain, *outs, heads):
     spans, rows, state = starts.shape
     part = rows // 2
     n_sig = inside.shape[1]
@@ -339,16 +339,17 @@
         mixed = mixed + carried * per_head(decays, direction * heads, heads, width)
     gated = mixed * silu(gate[...].astype(F32))
     scale = lax.rsqrt(jnp.mean(gated * gated, axis=-1, keepdims=True) + EPSILON)
-    out[...] = (gated * scale * gain[...]).astype(BF16)
+    normed = (gated * scale * gain[...]).astype(BF16)
+    rows = outs[0].shape[0]
+    for r, out in enumerate(outs):
+        out[...] = normed[r * rows : (r + 1) * rows, :]
 
 
 def output_body(where, *refs, count):
-    blocks, (weight, own, oth, gate, out) = refs[:count], refs[count : count + 5]
-    left, right, rest, done, sems = refs[count + 5 :]
-    length, n = blocks[0].shape
+    pieces, (weight, own, oth, gate, out) = refs[: 2 * count], refs[2 * count : 2 * count + 5]
+    left, right, rest, done, acc, sems = refs[2 * count + 5 :]
+    half, n = pieces[0].shape
     n_out = out.shape[1]
-    half = own.shape[0]
-    parts = length // half
     column = pl.multiple_of(where[1] * n_out, n_out)
     copies = []
 
@@ -359,24 +360,30 @@
     for b in range(count):
         at = pl.multiple_of(where[2 + b] * n, n)
         start(weight.at[pl.ds(at, n), :], right.at[b * n : (b + 1) * n, :])
-        start(blocks[b].at[:half, :], left.at[:half, b * n : (b + 1) * n])
+        for p in range(2):
+            start(
+                pieces[2 * b + p],
+                left.at[p * half : (p + 1) * half, b * n : (b + 1) * n],
+            )
     start(own.at[:, pl.ds(column, n_out)], rest.at[0])
     start(oth.at[:, pl.ds(column, n_out)], rest.at[1])
-    for p in range(1, parts):
-        for b in range(count):
-            start(
-                blocks[b].at[p * half : (p + 1) * half, :],
-                left.at[p * half : (p + 1) * half, b * n : (b + 1) * n],
-            )
-    first = 2 * count + 2
-    for copy in copies[:first]:
+    groups = count // 2
+    for g in range(groups - 1):
+        for copy in copies[6 * g : 6 * g + 6]:
+            copy.wait()
+        cut = slice(2 * g * n, 2 * (g + 1) * n)
+        term = jnp.dot(left[:, cut], right[cut, :], preferred_element_type=F32)
+        if g:
+            acc[...] += term
+        else:
+            acc[...] = term
+    for copy in copies[6 * (groups - 1) :]:
         copy.wait()
+    cut = slice(2 * (groups - 1) * n, 2 * groups * n)
     writes = []
-    for p in range(parts):
-        for copy in copies[first + (p - 1) * count : first + p * count] if p else []:
-            copy.wait()
+    for p in range(2):
         rows = slice(p * half, (p + 1) * half)
-        total = jnp.dot(left[rows, :], right[...], preferred_element_type=F32)
+        total = acc[rows, :] + jnp.dot(left[rows, cut], right[cut, :], preferred_element_type=F32)
         mine = jnp.where(where[0] == p, 1.0, 0.0)
         base = rest[0].astype(F32) * mine + rest[1].astype(F32) * (1.0 - mine)
         done[rows, :] = (base + gate[...] * total).astype(BF16)
@@ -559,20 +566,29 @@
     starts = lax.all_to_all(starts, "sp", split_axis=0, concat_axis=0, tiled=True)
     normed = pl.pallas_call(
         functools.partial(finish_body, heads=heads),
-        out_shape=shaped((length, n_sig), BF16),
-        compiler_params=pltpu.CompilerParams(vmem_limit_bytes=12 * MIB),
+        out_shape=[shaped((half, n_sig), BF16)] * n_dp,
+        compiler_params=small(12),
         name="finish",
     )(starts, *placed(reader, cols, inside, gate_in), group_gain.reshape(1, -1))
+    normed = placed(*normed)
+    moved = {0: normed}
+    for by in {1, n_tp - 1}:
+        moved[by] = [shifted(piece, "tp", by) for piece in normed]
+    for by in range(2, n_tp - 1):
+        if n_tp == 4:
+            moved[by] = [shifted(moved[1][0], "tp", 1), shifted(moved[3][1], "tp", 3)]
+        else:
+            moved[by] = [shifted(piece, "tp", by) for piece in normed]
+    *held, _ = lax.optimization_barrier((*normed, moved[1][0]))
+    pieces, places = [], []
+    for by in (0, *(k for k in moved if k in (1, n_tp - 1)), *range(2, n_tp - 1)):
+        place = (tp + n_tp - by) % n_tp * n_dp
+        for blocks in (moved[by], [shifted(b, "dp", 1) for b in (moved[by] if by else held)]):
+            pieces.extend(blocks)
+        places += [place + dp, place + 1 - dp]
     at = tp * n_dp + dp
-    blocks, places = placed(normed), [at]
-    for by in (n_tp - 1, 1, *range(2, n_tp - 1)):
-        blocks.append(shifted(normed, "tp", by))
-        places.append((tp + n_tp - by) % n_tp * n_dp + dp)
-    for one, place in list(zip(blocks, places)):
-        blocks.append(shifted(one, "dp", 1))
-        places.append(place - dp + 1 - dp)
     where = jnp.stack([dp, at, *places]).astype(jnp.int32)
-    count = len(blocks)
+    count = len(places)
     anywhere = pl.BlockSpec(memory_space=pl.ANY)
     return pl.pallas_call(
         functools.partial(output_body, count=count),
@@ -580,19 +596,20 @@
         grid_spec=pltpu.PrefetchScalarGridSpec(
             num_scalar_prefetch=1,
             grid=(1,),
-            in_specs=[anywhere] * (count + 3) + [whole((1, n_out))],
+            in_specs=[anywhere] * (2 * count + 3) + [whole((1, n_out))],
             out_specs=anywhere,
             scratch_shapes=[
                 pltpu.VMEM((length, n_sig * count), BF16),
                 pltpu.VMEM((n_sig * count, n_out), BF16),
                 pltpu.VMEM((2, half, n_out), BF16),
                 pltpu.VMEM((length, n_out), BF16),
-                pltpu.SemaphoreType.DMA((n_dp * (count + 1) + count + 1,)),
+                pltpu.VMEM((length, n_out), F32),
+                pltpu.SemaphoreType.DMA((3 * count + 2,)),
             ],
         ),
         compiler_params=small(24),
         name="output",
-    )(where, *placed(*blocks), *placed(output_weight, latent), oth, gate_vec)
+    )(where, *placed(*pieces), *placed(output_weight, latent), oth, gate_vec)
 
 
 def solution(mesh):

time: 142 us -> 139 us (0.979)
    ppermute x8 -> x15, starting transfers between devices: 38.3 us -> 37.5 us  [shifted(): return lax.ppermute(x, axis, [(i, (i + by) % n) for i in range(n)])]
    ppermute x8 -> x15, waiting for transfers between devices: 6.01 us -> 5.34 us  [shifted(): return lax.ppermute(x, axis, [(i, (i + by) % n) for i in range(n)])]
  transfers between devices with their start and end apart: 13 -> 20, of which waited for: 7 -> 7; matrix products, arithmetic and copies ran while one was open for 1% -> 1% of each run, Pallas kernels for 6% -> 6%
where the time goes in v4:
time: 139 us
  starting transfers between devices  59.6 us (43%)
  Pallas kernels  34.4 us (25%)
  blocking collectives  23.3 us (17%)
  waiting for transfers between devices  19.8 us (14%)
    ppermute x15, starting transfers between devices, shifted(): return lax.ppermute(x, axis, [(i, (i + by) % n) for i in range(n)])  37.5 us
    all_to_all x1, blocking collectives, on_device(): lax.all_to_all(starts, 'sp', split_axis=0, concat_axis=0, tiled=True)  23.3 us
    pallas_call x1, Pallas kernels, on_device(): pl.pallas_call(functools.partial(project_body, heads=heads), out_shape=ou...  14.4 us
    pallas_call x1, Pallas kernels, on_device(): pl.pallas_call(functools.partial(inside_body, heads=heads), out_shape=sha...  8.32 us
    all_to_all x1, starting transfers between devices, on_device(): lax.all_to_all(vectors, ('tp', 'dp'), split_axis=0, concat_axis=0, tiled=...  6.2 us
    all_to_all x1, waiting for transfers between devices, on_device(): got = lax.all_to_all(payload, 'sp', split_axis=0, concat_axis=0, tiled=True)  5.59 us
    ppermute x15, waiting for transfers between devices, shifted(): return lax.ppermute(x, axis, [(i, (i + by) % n) for i in range(n)])  5.34 us
    pallas_call x1, Pallas kernels, on_device(): pl.pallas_call(functools.partial(output_body, count=count), out_shape=sha...  4.89 us
  transfers between devices with their start and end apart: 20, of which 7 were waited for; matrix products, arithmetic and copies ran while one was open for 1% of the time, Pallas kernels for 6%

profile of v4, /device:TPU:33, one launch (start us, length us, event | category | flops | bytes accessed | tf_op | source)
XLA Modules:
  0.0 138.8 jit_solution(6767061098936563302)
XLA Ops:
  0.0 2.0 %condense.1 = bf16[16,20,128]{2,1,0:T(8,128)(2,1)} custom-call(s32[1]{0:T(128)} %bitcast.12.where, bf16[32,128]{1,0:T(8,128)(2,1)} %bitcast.19, bf16[32,128]{1,0:T(8,128)(2,1)} %bitcast.20, bf16[256,512]{1,0:T(8,128)(2,1)} %shift.1, bf16[256,512]{1,0:T(8,128)(2,1)} %scale.1, bf16[256,512]{1,0:T(8,128)(2,1)} %gate.1), custom_call_target="tpu_custom_call" | custom-call | tf_op jit(solution)/shard_map/condense/pallas_call | solution.py:431
  2.0 20.4 %collective-permute-start = (bf16[384,4096]{1,0:T(8,128)(2,1)}, bf16[384,4096]{1,0:T(8,128)(2,1)S(1)}, u32[]{:S(2)}, u32[]{:S(2)}) collective-permute-start(bf16[384,4096]{1,0:T(8,128)(2,1)} %refs_17_), channel_id=1, source_target_pairs={{0,1},{1,0},{2,3},{3,2},{4,5},{5,4},{6,7},{7,6},{8,9},{9,8},{10,11... | collective-permute-start | bytes 9437192 | tf_op jit(solution)/shard_map/ppermute | solution.py:24
  22.4 4.7 %all-to-all-start = ((bf16[16,20,128]{2,1,0:T(8,128)(2,1)}), bf16[16,20,128]{2,1,0:T(8,128)(2,1)S(1)}, u32[]{:S(2)}, u32[]{:S(2)}) async-start(bf16[16,20,128]{2,1,0:T(8,128)(2,1)} %condense.1), calls=%async_computation | async-start | bytes 196608 | tf_op jit(solution)/shard_map/all_to_all | solution.py:452
  27.2 1.0 fusion
  28.1 0.1 broadcast_select_fusion
  28.2 3.5 %collective-permute-start.2 = (bf16[2,4096]{1,0:T(2,128)(2,1)S(1)}, bf16[2,4096]{1,0:T(2,128)(2,1)S(1)}, u32[]{:S(2)}, u32[]{:S(2)}) collective-permute-start(bf16[2,4096]{1,0:T(2,128)(2,1)S(1)} %broadcast_select_fusion), channel_id=1, source_target_pairs={{1,8},{9,16},{8,1},{17,24},{16,9},{25,32},{24,17},{33,40},{32,25},... | collective-permute-start | bytes 49160 | tf_op jit(solution)/shard_map/ppermute | solution.py:478
  31.8 3.1 %collective-permute-start.1 = (bf16[2,4096]{1,0:T(2,128)(2,1)S(1)}, bf16[2,4096]{1,0:T(2,128)(2,1)S(1)}, u32[]{:S(2)}, u32[]{:S(2)}) collective-permute-start(bf16[2,4096]{1,0:T(2,128)(2,1)S(1)} %broadcast_select_fusion), channel_id=1, source_target_pairs={{1,9},{9,17},{8,0},{17,25},{16,8},{25,33},{24,16},{33,41},{32,24},... | collective-permute-start | bytes 49160 | tf_op jit(solution)/shard_map/ppermute | solution.py:477
  34.9 4.1 %all-to-all-done.got = bf16[16,20,128]{2,1,0:T(8,128)(2,1)S(1)} async-done(((bf16[16,20,128]{2,1,0:T(8,128)(2,1)}), bf16[16,20,128]{2,1,0:T(8,128)(2,1)S(1)}, u32[]{:S(2)}, u32[]{:S(2)}) %all-to-all-start) | async-done | bytes 81952 | tf_op jit(solution)/shard_map/all_to_all | solution.py:452
  39.0 0.7 fold.1
  39.6 6.2 %all-to-all-start.1 = ((f32[8,16,128]{2,1,0:T(8,128)}), f32[8,16,128]{2,1,0:T(8,128)S(1)}, u32[]{:S(2)}, u32[]{:S(2)}) async-start(f32[8,16,128]{2,1,0:T(8,128)} %get-tuple-element.26), calls=%async_computation.1 | async-start | bytes 131072 | tf_op jit(solution)/shard_map/all_to_all | solution.py:462
  45.8 0.1 pad_add_fusion.flags
  45.9 0.0 collective-permute-done.2.crossed
  45.9 0.0 collective-permute-done.1.same
  45.9 4.8 %all-to-all-done.1.vectors = f32[8,16,128]{2,1,0:T(8,128)S(1)} async-done(((f32[8,16,128]{2,1,0:T(8,128)}), f32[8,16,128]{2,1,0:T(8,128)S(1)}, u32[]{:S(2)}, u32[]{:S(2)}) %all-to-all-start.1) | async-done | bytes 65568 | tf_op jit(solution)/shard_map/all_to_all | solution.py:462
  50.7 0.0 collective-permute-done.oth.refs_18_
  50.7 14.4 %project.1 = (bf16[768,256]{1,0:T(8,128)(2,1)}, bf16[768,256]{1,0:T(8,128)(2,1)}, bf16[768,128]{1,0:T(8,128)(2,1)}, bf16[768,128]{1,0:T(8,128)(2,1)}, f32[16,768...) custom-call(s32[3]{0:T(128)S(1)} %pad_add_fusion.flags, bf16[384,4096]{1,0:T(8,128)(2,1)} %refs_17_, ...), custom_call_target="tpu_custom_call" | custom-call | flops 5234491392 | bytes 13107200 | tf_op jit(solution)/shard_map/project/pallas_call | solution.py:498
  65.1 0.0 copy-start.1
  65.1 4.6 %all-to-all-start.2 = ((bf16[16,72,128]{2,1,0:T(8,128)(2,1)}), bf16[16,72,128]{2,1,0:T(8,128)(2,1)S(1)}, u32[]{:S(2)}, u32[]{:S(2)}) async-start(bf16[16,72,128]{2,1,0:T(8,128)(2,1)} %get-tuple-element.27), calls=%async_computation.2 | async-start | bytes 589824 | tf_op jit(solution)/shard_map/all_to_all | solution.py:540
  69.7 0.0 copy-start
  69.7 8.3 %inside.1 = f32[768,256]{1,0:T(8,128)} custom-call(bf16[768,128]{1,0:T(8,128)(2,1)} %get-tuple-element.28.rea, bf16[768,128]{1,0:T(8,128)(2,1)} %get-tuple-element.29.wri, bf16[768,256]{1,0:T(8,128)(2,1)} %get-tuple-element.30.sig, f32[16,768]{1,0:T(8,128)} %get-tuple-element.31.rows, f32[768,128]{1,0:T(8,128)} %get-tuple-element.32.cols), custom_call_target="tpu_custom_call" | custom-call | flops 1358954496 | bytes 786432 | tf_op jit(solution)/shard_map/inside/pallas_call | solution.py:542
  78.0 5.6 %all-to-all-done.2.got = bf16[16,72,128]{2,1,0:T(8,128)(2,1)S(1)} async-done(((bf16[16,72,128]{2,1,0:T(8,128)(2,1)}), bf16[16,72,128]{2,1,0:T(8,128)(2,1)S(1)}, u32[]{:S(2)}, u32[]{:S(2)}) %all-to-all-start.2) | async-done | bytes 294944 | tf_op jit(solution)/shard_map/all_to_all | solution.py:540
  83.6 0.8 chain.1
  84.4 23.3 %all_to_all.20.starts = bf16[16,32,128]{2,1,0:T(8,128)(2,1)S(1)} all-to-all(bf16[16,32,128]{2,1,0:T(8,128)(2,1)} %chain.1), channel_id=1, replica_groups=mesh['grp'=2,'sp'=16,'tp'=4,'dp'=2] {'sp'}, dimensions={0} | all-to-all | bytes 262144 | tf_op jit(solution)/shard_map/all_to_all | solution.py:566
  107.7 0.0 copy-done.1
  107.7 3.4 %finish.1 = (bf16[384,256]{1,0:T(8,128)(2,1)}, bf16[384,256]{1,0:T(8,128)(2,1)}) custom-call(bf16[16,32,128]{2,1,0:T(8,128)(2,1)S(1)} %all_to_all.20.starts, bf16[768,128]{1,0:T(8,128)(2,1)} %get-tuple-element.28.rea, f32[768,128]{1,0:T(8,128)} %get-tuple-element.32.cols, f32[768,256]{1,0:T(8,128)} %inside.1, bf16[768,256]{1,0:T(8,128)(2,1)} %get-tuple-element.35.gate, ...), custom_call_target="tpu_custom_call" | custom-call | tf_op jit(solution)/shard_map/finish/pallas_call | solution.py:567
  111.1 0.3 collective-permute-start.3
  111.4 2.4 %collective-permute-start.9 = (bf16[384,256]{1,0:T(8,128)(2,1)}, bf16[384,256]{1,0:T(8,128)(2,1)S(1)}, u32[]{:S(2)}, u32[]{:S(2)}) collective-permute-start(bf16[384,256]{1,0:T(8,128)(2,1)} %get-tuple-element.38.refs_0_), channel_id=1, source_target_pairs={{0,6},{2,0},{4,2},{6,4},{1,7},{3,1},{5,3},{7,5},{8,14},{10,8},{12,... | collective-permute-start | bytes 589832 | tf_op jit(solution)/shard_map/ppermute | solution.py:24
  113.8 0.0 collective-permute-start.10
  113.8 1.4 %collective-permute-start.6 = (bf16[384,256]{1,0:T(8,128)(2,1)}, bf16[384,256]{1,0:T(8,128)(2,1)}, u32[]{:S(2)}, u32[]{:S(2)}) collective-permute-start(bf16[384,256]{1,0:T(8,128)(2,1)} %get-tuple-element.39.refs_1_), channel_id=1, source_target_pairs={{0,2},{2,4},{4,6},{6,0},{1,3},{3,5},{5,7},{7,1},{8,10},{10,12},{12... | collective-permute-start | bytes 589832 | tf_op jit(solution)/shard_map/ppermute | solution.py:24
  115.2 1.8 %collective-permute-done.3.refs_4_ = bf16[384,256]{1,0:T(8,128)(2,1)S(1)} collective-permute-done((bf16[384,256]{1,0:T(8,128)(2,1)}, bf16[384,256]{1,0:T(8,128)(2,1)S(1)}, u32[]{:S(2)}, u32[]{:S(2)}) %collective-permute-start.3) | collective-permute-done | bytes 196640 | tf_op jit(solution)/shard_map/ppermute | solution.py:24
  117.0 0.0 collective-permute-done.9.refs_8_
  117.0 0.0 copy-start.3
  117.0 5.6 %collective-permute-start.11 = (bf16[384,256]{1,0:T(8,128)(2,1)S(1)}, bf16[384,256]{1,0:T(8,128)(2,1)S(1)}, u32[]{:S(2)}, u32[]{:S(2)}) collective-permute-start(bf16[384,256]{1,0:T(8,128)(2,1)S(1)} %collective-permute-done.9.refs_8_), channel_id=1, source_target_pairs={{0,1},{1,0},{2,3},{3,2},{4,5},{5,4},{6,7},{7,6},{8,9},{9,8},{10,11... | collective-permute-start | bytes 589832 | tf_op jit(solution)/shard_map/ppermute | solution.py:24
  122.6 0.1 collective-permute-start.4
  122.8 0.4 collective-permute-start.5
  123.2 0.0 collective-permute-done.10.refs_9_
  123.2 0.2 collective-permute-start.13
  123.4 0.0 collective-permute-done.6.refs_5_
  123.4 2.4 %collective-permute-start.14 = (bf16[384,256]{1,0:T(8,128)(2,1)}, bf16[384,256]{1,0:T(8,128)(2,1)}, u32[]{:S(2)}, u32[]{:S(2)}) collective-permute-start(bf16[384,256]{1,0:T(8,128)(2,1)} %collective-permute-done.10.refs_9_), channel_id=1, source_target_pairs={{0,6},{2,0},{4,2},{6,4},{1,7},{3,1},{5,3},{7,5},{8,14},{10,8},{12,... | collective-permute-start | bytes 589832 | tf_op jit(solution)/shard_map/ppermute | solution.py:24
  125.8 0.0 collective-permute-done.11.refs_10_
  125.8 0.0 copy-start.4
  125.8 1.6 %collective-permute-start.7 = (bf16[384,256]{1,0:T(8,128)(2,1)S(1)}, bf16[384,256]{1,0:T(8,128)(2,1)}, u32[]{:S(2)}, u32[]{:S(2)}) collective-permute-start(bf16[384,256]{1,0:T(8,128)(2,1)S(1)} %collective-permute-done.3.refs_4_), channel_id=1, source_target_pairs={{0,1},{1,0},{2,3},{3,2},{4,5},{5,4},{6,7},{7,6},{8,9},{9,8},{10,11... | collective-permute-start | bytes 589832 | tf_op jit(solution)/shard_map/ppermute | solution.py:24
  127.4 0.0 collective-permute-done.4.refs_2_
  127.4 0.0 copy-start.5
  127.4 0.1 collective-permute-start.12
  127.6 0.0 collective-permute-done.5.refs_3_
  127.6 0.4 collective-permute-start.8
  128.0 1.9 %collective-permute-done.13.refs_12_ = bf16[384,256]{1,0:T(8,128)(2,1)} collective-permute-done((bf16[384,256]{1,0:T(8,128)(2,1)S(1)}, bf16[384,256]{1,0:T(8,128)(2,1)}, u32[]{:S(2)}, u32[]{:S(2)}) %collective-permute-start.13) | collective-permute-done | bytes 196640 | tf_op jit(solution)/shard_map/ppermute | solution.py:24
  129.9 0.0 copy-done.4
  129.9 1.9 %collective-permute-start.15 = (bf16[384,256]{1,0:T(8,128)(2,1)}, bf16[384,256]{1,0:T(8,128)(2,1)}, u32[]{:S(2)}, u32[]{:S(2)}) collective-permute-start(bf16[384,256]{1,0:T(8,128)(2,1)} %collective-permute-done.13.refs_12_), channel_id=1, source_target_pairs={{0,1},{1,0},{2,3},{3,2},{4,5},{5,4},{6,7},{7,6},{8,9},{9,8},{10,11... | collective-permute-start | bytes 589832 | tf_op jit(solution)/shard_map/ppermute | solution.py:24
  131.8 0.0 copy-done.5
  131.8 0.0 collective-permute-done.14.refs_13_
  131.8 0.0 copy-done.6
  131.8 0.1 collective-permute-start.16
  132.0 0.1 stack.59.where
  132.1 0.0 collective-permute-done.7.refs_6_
  132.1 0.0 collective-permute-done.12.refs_11_
  132.1 0.0 collective-permute-done.8.refs_7_
  132.1 1.1 collective-permute-done.15.refs_14_
  133.2 0.5 collective-permute-done.16.refs_15_
  133.7 0.0 copy-done.2
  133.7 0.0 copy-done.3
  133.7 0.0 copy-done
  133.7 4.9 %output.1 = bf16[768,512]{1,0:T(8,128)(2,1)} custom-call(s32[10]{0:T(128)S(1)} %stack.59.where, bf16[384,256]{1,0:T(8,128)(2,1)} %get-tuple-element.38.refs_0_, bf16[384,256]{1,0:T(8,128)(2,1)} %get-tuple-element.39.refs_1_, bf16[384,256]{1,0:T(8,128)(2,1)} %copy-done.5, bf16[384,256]{1,0:T(8,128)(2,1)} %copy-done.6, bf16[384,256]{1,0:T(8,128)(2,1)} %copy-done.2, ...), custom_call_target="tpu_custom_call" | custom-call | tf_op jit(solution)/shard_map/output/pallas_call | solution.py:593
  (2 shorter events, 0.0 us)
Async XLA Ops:
  2.0 48.7 %collective-permute-start = (bf16[384,4096]{1,0:T(8,128)(2,1)}, bf16[384,4096]{1,0:T(8,128)(2,1)S(1)}, u32[]{:S(2)}, u32[]{:S(2)}) collective-permute-start(bf16[384,4096]{1,0:T(8,128)(2,1)} %refs_17_), channel_id=1, source_target_pairs={{0,1},{1,0},{2,3},{3,2},{4,5},{5,4},{6,7},{7,6},{8,9},{9,8},{10,11... | collective-permute-start | bytes 9437192 | tf_op jit(solution)/shard_map/ppermute | solution.py:24
  22.4 16.5 %all-to-all-start = ((bf16[16,20,128]{2,1,0:T(8,128)(2,1)}), bf16[16,20,128]{2,1,0:T(8,128)(2,1)S(1)}, u32[]{:S(2)}, u32[]{:S(2)}) async-start(bf16[16,20,128]{2,1,0:T(8,128)(2,1)} %condense.1), calls=%async_computation | async-start | bytes 196608 | tf_op jit(solution)/shard_map/all_to_all | solution.py:452
  28.2 17.7 %collective-permute-start.2 = (bf16[2,4096]{1,0:T(2,128)(2,1)S(1)}, bf16[2,4096]{1,0:T(2,128)(2,1)S(1)}, u32[]{:S(2)}, u32[]{:S(2)}) collective-permute-start(bf16[2,4096]{1,0:T(2,128)(2,1)S(1)} %broadcast_select_fusion), channel_id=1, source_target_pairs={{1,8},{9,16},{8,1},{17,24},{16,9},{25,32},{24,17},{33,40},{32,25},... | collective-permute-start | bytes 49160 | tf_op jit(solution)/shard_map/ppermute | solution.py:478
  31.8 14.1 %collective-permute-start.1 = (bf16[2,4096]{1,0:T(2,128)(2,1)S(1)}, bf16[2,4096]{1,0:T(2,128)(2,1)S(1)}, u32[]{:S(2)}, u32[]{:S(2)}) collective-permute-start(bf16[2,4096]{1,0:T(2,128)(2,1)S(1)} %broadcast_select_fusion), channel_id=1, source_target_pairs={{1,9},{9,17},{8,0},{17,25},{16,8},{25,33},{24,16},{33,41},{32,24},... | collective-permute-start | bytes 49160 | tf_op jit(solution)/shard_map/ppermute | solution.py:477
  39.6 11.1 %all-to-all-start.1 = ((f32[8,16,128]{2,1,0:T(8,128)}), f32[8,16,128]{2,1,0:T(8,128)S(1)}, u32[]{:S(2)}, u32[]{:S(2)}) async-start(f32[8,16,128]{2,1,0:T(8,128)} %get-tuple-element.26), calls=%async_computation.1 | async-start | bytes 131072 | tf_op jit(solution)/shard_map/all_to_all | solution.py:462
  65.1 42.6 %copy-start.1 = (f32[256]{0:T(256)S(1)}, f32[256]{0:T(256)}, u32[]{:S(2)}) copy-start(f32[256]{0:T(256)} %param.40) | copy-start | bytes 3076
  65.1 18.5 %all-to-all-start.2 = ((bf16[16,72,128]{2,1,0:T(8,128)(2,1)}), bf16[16,72,128]{2,1,0:T(8,128)(2,1)S(1)}, u32[]{:S(2)}, u32[]{:S(2)}) async-start(bf16[16,72,128]{2,1,0:T(8,128)(2,1)} %get-tuple-element.27), calls=%async_computation.2 | async-start | bytes 589824 | tf_op jit(solution)/shard_map/all_to_all | solution.py:540
  69.7 64.0 %copy-start = (f32[1,512]{1,0:T(1,128)S(1)}, f32[1,512]{1,0:T(1,128)}, u32[]{:S(2)}) copy-start(f32[1,512]{1,0:T(1,128)} %get-tuple-element.40.refs_19_) | copy-start | bytes 6148
  111.1 5.9 %collective-permute-start.3 = (bf16[384,256]{1,0:T(8,128)(2,1)}, bf16[384,256]{1,0:T(8,128)(2,1)S(1)}, u32[]{:S(2)}, u32[]{:S(2)}) collective-permute-start(bf16[384,256]{1,0:T(8,128)(2,1)} %get-tuple-element.38.refs_0_), channel_id=1, source_target_pairs={{0,2},{2,4},{4,6},{6,0},{1,3},{3,5},{5,7},{7,1},{8,10},{10,12},{12... | collective-permute-start | bytes 589832 | tf_op jit(solution)/shard_map/ppermute | solution.py:24
  111.4 5.7 %collective-permute-start.9 = (bf16[384,256]{1,0:T(8,128)(2,1)}, bf16[384,256]{1,0:T(8,128)(2,1)S(1)}, u32[]{:S(2)}, u32[]{:S(2)}) collective-permute-start(bf16[384,256]{1,0:T(8,128)(2,1)} %get-tuple-element.38.refs_0_), channel_id=1, source_target_pairs={{0,6},{2,0},{4,2},{6,4},{1,7},{3,1},{5,3},{7,5},{8,14},{10,8},{12,... | collective-permute-start | bytes 589832 | tf_op jit(solution)/shard_map/ppermute | solution.py:24
  113.8 9.4 %collective-permute-start.10 = (bf16[384,256]{1,0:T(8,128)(2,1)}, bf16[384,256]{1,0:T(8,128)(2,1)}, u32[]{:S(2)}, u32[]{:S(2)}) collective-permute-start(bf16[384,256]{1,0:T(8,128)(2,1)} %get-tuple-element.39.refs_1_), channel_id=1, source_target_pairs={{0,6},{2,0},{4,2},{6,4},{1,7},{3,1},{5,3},{7,5},{8,14},{10,8},{12,... | collective-permute-start | bytes 589832 | tf_op jit(solution)/shard_map/ppermute | solution.py:24
  113.8 9.6 %collective-permute-start.6 = (bf16[384,256]{1,0:T(8,128)(2,1)}, bf16[384,256]{1,0:T(8,128)(2,1)}, u32[]{:S(2)}, u32[]{:S(2)}) collective-permute-start(bf16[384,256]{1,0:T(8,128)(2,1)} %get-tuple-element.39.refs_1_), channel_id=1, source_target_pairs={{0,2},{2,4},{4,6},{6,0},{1,3},{3,5},{5,7},{7,1},{8,10},{10,12},{12... | collective-permute-start | bytes 589832 | tf_op jit(solution)/shard_map/ppermute | solution.py:24
  117.0 16.7 %copy-start.2 = (bf16[384,256]{1,0:T(8,128)(2,1)}, bf16[384,256]{1,0:T(8,128)(2,1)S(1)}, u32[]{:S(2)}) copy-start(bf16[384,256]{1,0:T(8,128)(2,1)S(1)} %collective-permute-done.3.refs_4_) | copy-start | bytes 589828
  117.0 16.7 %copy-start.3 = (bf16[384,256]{1,0:T(8,128)(2,1)}, bf16[384,256]{1,0:T(8,128)(2,1)S(1)}, u32[]{:S(2)}) copy-start(bf16[384,256]{1,0:T(8,128)(2,1)S(1)} %collective-permute-done.9.refs_8_) | copy-start | bytes 589828
  117.0 8.8 %collective-permute-start.11 = (bf16[384,256]{1,0:T(8,128)(2,1)S(1)}, bf16[384,256]{1,0:T(8,128)(2,1)S(1)}, u32[]{:S(2)}, u32[]{:S(2)}) collective-permute-start(bf16[384,256]{1,0:T(8,128)(2,1)S(1)} %collective-permute-done.9.refs_8_), channel_id=1, source_target_pairs={{0,1},{1,0},{2,3},{3,2},{4,5},{5,4},{6,7},{7,6},{8,9},{9,8},{10,11... | collective-permute-start | bytes 589832 | tf_op jit(solution)/shard_map/ppermute | solution.py:24
  122.6 4.8 %collective-permute-start.4 = (bf16[384,256]{1,0:T(8,128)(2,1)}, bf16[384,256]{1,0:T(8,128)(2,1)S(1)}, u32[]{:S(2)}, u32[]{:S(2)}) collective-permute-start(bf16[384,256]{1,0:T(8,128)(2,1)} %get-tuple-element.38.refs_0_), channel_id=1, source_target_pairs={{0,1},{1,0},{2,3},{3,2},{4,5},{5,4},{6,7},{7,6},{8,9},{9,8},{10,11... | collective-permute-start | bytes 589832 | tf_op jit(solution)/shard_map/ppermute | solution.py:24
  122.8 4.8 %collective-permute-start.5 = (bf16[384,256]{1,0:T(8,128)(2,1)}, bf16[384,256]{1,0:T(8,128)(2,1)S(1)}, u32[]{:S(2)}, u32[]{:S(2)}) collective-permute-start(bf16[384,256]{1,0:T(8,128)(2,1)} %get-tuple-element.39.refs_1_), channel_id=1, source_target_pairs={{0,1},{1,0},{2,3},{3,2},{4,5},{5,4},{6,7},{7,6},{8,9},{9,8},{10,11... | collective-permute-start | bytes 589832 | tf_op jit(solution)/shard_map/ppermute | solution.py:24
  123.2 6.7 %collective-permute-start.13 = (bf16[384,256]{1,0:T(8,128)(2,1)S(1)}, bf16[384,256]{1,0:T(8,128)(2,1)}, u32[]{:S(2)}, u32[]{:S(2)}) collective-permute-start(bf16[384,256]{1,0:T(8,128)(2,1)S(1)} %collective-permute-done.3.refs_4_), channel_id=1, source_target_pairs={{0,2},{2,4},{4,6},{6,0},{1,3},{3,5},{5,7},{7,1},{8,10},{10,12},{12... | collective-permute-start | bytes 589832 | tf_op jit(solution)/shard_map/ppermute | solution.py:24
  123.4 8.4 %collective-permute-start.14 = (bf16[384,256]{1,0:T(8,128)(2,1)}, bf16[384,256]{1,0:T(8,128)(2,1)}, u32[]{:S(2)}, u32[]{:S(2)}) collective-permute-start(bf16[384,256]{1,0:T(8,128)(2,1)} %collective-permute-done.10.refs_9_), channel_id=1, source_target_pairs={{0,6},{2,0},{4,2},{6,4},{1,7},{3,1},{5,3},{7,5},{8,14},{10,8},{12,... | collective-permute-start | bytes 589832 | tf_op jit(solution)/shard_map/ppermute | solution.py:24
  125.8 4.1 %copy-start.4 = (bf16[384,256]{1,0:T(8,128)(2,1)}, bf16[384,256]{1,0:T(8,128)(2,1)S(1)}, u32[]{:S(2)}) copy-start(bf16[384,256]{1,0:T(8,128)(2,1)S(1)} %collective-permute-done.11.refs_10_) | copy-start | bytes 589828
  125.8 6.3 %collective-permute-start.7 = (bf16[384,256]{1,0:T(8,128)(2,1)S(1)}, bf16[384,256]{1,0:T(8,128)(2,1)}, u32[]{:S(2)}, u32[]{:S(2)}) collective-permute-start(bf16[384,256]{1,0:T(8,128)(2,1)S(1)} %collective-permute-done.3.refs_4_), channel_id=1, source_target_pairs={{0,1},{1,0},{2,3},{3,2},{4,5},{5,4},{6,7},{7,6},{8,9},{9,8},{10,11... | collective-permute-start | bytes 589832 | tf_op jit(solution)/shard_map/ppermute | solution.py:24
  127.4 4.3 %copy-start.5 = (bf16[384,256]{1,0:T(8,128)(2,1)}, bf16[384,256]{1,0:T(8,128)(2,1)S(1)}, u32[]{:S(2)}) copy-start(bf16[384,256]{1,0:T(8,128)(2,1)S(1)} %collective-permute-done.4.refs_2_) | copy-start | bytes 589828
  127.4 4.7 %collective-permute-start.12 = (bf16[384,256]{1,0:T(8,128)(2,1)}, bf16[384,256]{1,0:T(8,128)(2,1)}, u32[]{:S(2)}, u32[]{:S(2)}) collective-permute-start(bf16[384,256]{1,0:T(8,128)(2,1)} %collective-permute-done.10.refs_9_), channel_id=1, source_target_pairs={{0,1},{1,0},{2,3},{3,2},{4,5},{5,4},{6,7},{7,6},{8,9},{9,8},{10,11... | collective-permute-start | bytes 589832 | tf_op jit(solution)/shard_map/ppermute | solution.py:24
  127.6 4.2 %copy-start.6 = (bf16[384,256]{1,0:T(8,128)(2,1)}, bf16[384,256]{1,0:T(8,128)(2,1)S(1)}, u32[]{:S(2)}) copy-start(bf16[384,256]{1,0:T(8,128)(2,1)S(1)} %collective-permute-done.5.refs_3_) | copy-start | bytes 589828
  127.6 4.5 %collective-permute-start.8 = (bf16[384,256]{1,0:T(8,128)(2,1)}, bf16[384,256]{1,0:T(8,128)(2,1)}, u32[]{:S(2)}, u32[]{:S(2)}) collective-permute-start(bf16[384,256]{1,0:T(8,128)(2,1)} %collective-permute-done.6.refs_5_), channel_id=1, source_target_pairs={{0,1},{1,0},{2,3},{3,2},{4,5},{5,4},{6,7},{7,6},{8,9},{9,8},{10,11... | collective-permute-start | bytes 589832 | tf_op jit(solution)/shard_map/ppermute | solution.py:24
  129.9 3.3 %collective-permute-start.15 = (bf16[384,256]{1,0:T(8,128)(2,1)}, bf16[384,256]{1,0:T(8,128)(2,1)}, u32[]{:S(2)}, u32[]{:S(2)}) collective-permute-start(bf16[384,256]{1,0:T(8,128)(2,1)} %collective-permute-done.13.refs_12_), channel_id=1, source_target_pairs={{0,1},{1,0},{2,3},{3,2},{4,5},{5,4},{6,7},{7,6},{8,9},{9,8},{10,11... | collective-permute-start | bytes 589832 | tf_op jit(solution)/shard_map/ppermute | solution.py:24
  131.8 1.9 %collective-permute-start.16 = (bf16[384,256]{1,0:T(8,128)(2,1)}, bf16[384,256]{1,0:T(8,128)(2,1)}, u32[]{:S(2)}, u32[]{:S(2)}) collective-permute-start(bf16[384,256]{1,0:T(8,128)(2,1)} %collective-permute-done.14.refs_13_), channel_id=1, source_target_pairs={{0,1},{1,0},{2,3},{3,2},{4,5},{5,4},{6,7},{7,6},{8,9},{9,8},{10,11... | collective-permute-start | bytes 589832 | tf_op jit(solution)/shard_map/ppermute | solution.py:24
